TPU v7x, 128 devices: a whole 4x4x4 slice. The times are simulated.
128 devices in a mesh: kv: 16 (over z, y), tp: 8 (over x, core).
Axes of the slice: x: 4, y: 4, z: 4, core: 2. Of those that a mesh axis runs over, the one named last changes fastest.
Arguments:
- tokens: bfloat16 [128, 4096], P(None, 'kv'), may hold values from -8 to 8
- attn_gain: float32 [4096], P('kv'), may hold values from 0.1 to 1.9
- w_query: bfloat16 [4096, 2048], P('kv', 'tp'), may hold values from -0.09375 to 0.09375
- w_key: bfloat16 [4096, 2048], P('kv', 'tp'), may hold values from -0.09375 to 0.09375
- w_value: bfloat16 [4096, 4096], P('kv', 'tp'), may hold values from -0.09375 to 0.09375
- w_outgate: bfloat16 [4096, 4096], P('kv', 'tp'), may hold values from -0.09375 to 0.09375
- w_gates: bfloat16 [4096, 16], replicated, may hold values from -0.029907227 to 0.029907227
- forget_bias: float32 [8], replicated, may hold values from -1 to 3
- state_c: float32 [128, 8, 512, 256], P('kv', 'tp'), may hold values from -6 to 6
- state_n: float32 [128, 8, 256], P('kv', 'tp'), may hold values from -6 to 6
- state_m: float32 [128, 8], P('kv', 'tp'), may hold values from -2 to 0.5
- w_output: bfloat16 [4096, 4096], P('tp', 'kv'), may hold values from -0.09375 to 0.09375
- mlp_gain: float32 [4096], P('kv'), may hold values from 0.1 to 1.9
- w_gateff: bfloat16 [4096, 11008], P('kv', 'tp'), may hold values from -0.09375 to 0.09375
- w_upff: bfloat16 [4096, 11008], P('kv', 'tp'), may hold values from -0.09375 to 0.09375
- w_downff: bfloat16 [11008, 4096], P('tp', 'kv'), may hold values from -0.0546875 to 0.0546875
Outputs:
- mixed: bfloat16 [128, 4096], P(None, 'kv')
- new_c: float32 [128, 8, 512, 256], P('kv', 'tp')
- new_n: float32 [128, 8, 256], P('kv', 'tp')
- new_m: float32 [128, 8], P('kv', 'tp')
All inputs are finite; a program needn't handle non-finite values.
Results may differ from a plain program's by a relative error of at most 0.0083.
Values may be sent and summed in bfloat16 or wider, within the bound.
No kernel may reach another device: no remote copies, remote signals or barrier semaphores. Data moves between devices by JAX's collectives and lax.ppermute only.
A program may use at most 64 MiB of HBM per device.

v0:
```python
import jax
import jax.numpy as jnp
from jax import lax
from jax.sharding import PartitionSpec as P

norm_floor = 1e-05


def in_blocks(value, dim, length):
    dims = value.shape
    pieces = value.reshape(*dims[:dim], length, dims[dim] // length, *dims[dim + 1 :])
    return jnp.moveaxis(pieces, dim, 0)


def sum_at_owner(value, axis, dim):
    pieces = in_blocks(value, dim, lax.axis_size(axis))
    arrived = lax.all_to_all(pieces, axis, split_axis=0, concat_axis=0, tiled=True)
    return arrived.astype(jnp.float32).sum(axis=0)


def shortened(value):

    def short(part):
        return part.astype(jnp.bfloat16) if part.dtype == jnp.float32 else part

    return jax.tree.map(short, value)


def sent_to_all(value, axis):
    copies = jnp.broadcast_to(value, (lax.axis_size(axis), *value.shape))
    return lax.all_to_all(copies, axis, split_axis=0, concat_axis=0, tiled=True)


def joined_along(pieces, dim):
    pieces = jnp.moveaxis(pieces, 0, dim)
    dims = pieces.shape
    return pieces.reshape(*dims[:dim], dims[dim] * dims[dim + 1], *dims[dim + 2 :])


def collect(value, axis, dim):
    pieces = sent_to_all(value, axis)
    return joined_along(pieces, dim)


def taken_together(value, axis):
    everything = sent_to_all(value, axis)
    return jnp.sum(everything.astype(jnp.float32), axis=0)


def over_copies(value, axis):
    return sent_to_all(value, axis).sum(axis=0)


def per_device(
    tokens,
    attn_gain,
    w_query,
    w_key,
    w_value,
    w_outgate,
    w_gates,
    forget_bias,
    state_c,
    state_n,
    state_m,
    w_output,
    mlp_gain,
    w_gateff,
    w_upff,
    w_downff,
):
    kv_count = lax.axis_size("kv")
    kv_at = lax.axis_index("kv")
    tp_at = lax.axis_index("tp")
    batch = tokens.shape[0]
    width_dev = tokens.shape[1]
    width_all = width_dev * kv_count
    rows = batch // kv_count
    heads_dev = state_c.shape[1]
    heads_all = forget_bias.shape[0]
    value_size = state_c.shape[2]
    query_size = state_c.shape[3]
    tok_float = tokens.astype(jnp.float32)
    squares_one = jnp.sum(tok_float * tok_float, axis=1)
    normed_one = (tok_float * attn_gain).astype(jnp.bfloat16)
    query_width = heads_dev * query_size
    value_width = heads_dev * value_size
    stacked = jnp.concatenate([w_query, w_key, w_value, w_outgate], axis=1)
    proj_part = jnp.dot(normed_one, stacked, preferred_element_type=jnp.float32)
    gate_rows = lax.dynamic_slice_in_dim(w_gates, kv_at * width_dev, width_dev, 0)
    gate_part = jnp.dot(normed_one, gate_rows, preferred_element_type=jnp.float32)
    extra_one = (squares_one,)
    summed_one = jax.tree.map(
        lambda part: sum_at_owner(part, "kv", 0), shortened((proj_part, gate_part) + extra_one)
    )
    rows_one = summed_one[2]
    scale_one = lax.rsqrt(rows_one / width_all + norm_floor)[:, None]
    proj_rows = summed_one[0] * scale_one
    gate_all = summed_one[1] * scale_one
    query = (proj_rows[:, :query_width] * query_size ** (-0.5)).reshape(rows, heads_dev, query_size)
    key_vec = proj_rows[:, query_width : 2 * query_width].reshape(rows, heads_dev, query_size)
    value = proj_rows[:, 2 * query_width : 2 * query_width + value_width].reshape(
        rows, heads_dev, value_size
    )
    out_pre = proj_rows[:, 2 * query_width + value_width :].reshape(rows, heads_dev, value_size)
    log_input = lax.dynamic_slice_in_dim(gate_all, tp_at * heads_dev, heads_dev, 1)
    forget_pre = lax.dynamic_slice_in_dim(gate_all, heads_all + tp_at * heads_dev, heads_dev, 1)
    bias_dev = lax.dynamic_slice_in_dim(forget_bias, tp_at * heads_dev, heads_dev, 0)
    log_forget = jax.nn.log_sigmoid(forget_pre + bias_dev)
    carried = log_forget + state_m
    new_m = jnp.maximum(carried, log_input)
    keep = jnp.exp(carried - new_m)
    admit = jnp.exp(log_input - new_m)
    new_c = (
        keep[:, :, None, None] * state_c
        + admit[:, :, None, None] * value[:, :, :, None] * key_vec[:, :, None, :]
    )
    new_n = keep[:, :, None] * state_n + admit[:, :, None] * key_vec
    numer = jnp.einsum("bhvd,bhd->bhv", new_c, query, precision=lax.Precision.HIGHEST)
    denom = jnp.maximum(jnp.abs(jnp.sum(new_n * query, axis=-1)), jnp.exp(-new_m))
    head_out = (
        (jax.nn.sigmoid(out_pre) * numer / denom[:, :, None])
        .reshape(rows, value_width)
        .astype(jnp.bfloat16)
    )
    attn_part = jnp.dot(collect(head_out, "kv", 0), w_output, preferred_element_type=jnp.float32)
    attn_mix = taken_together(attn_part.astype(jnp.bfloat16), "tp").astype(jnp.float32)
    middle = (tok_float + attn_mix).astype(jnp.bfloat16)
    mid_float = middle.astype(jnp.float32)
    squares_two = jnp.sum(mid_float * mid_float, axis=1)
    normed_two = (mid_float * mlp_gain).astype(jnp.bfloat16)
    gate_ff = jnp.dot(normed_two, w_gateff, preferred_element_type=jnp.float32)
    up_ff = jnp.dot(normed_two, w_upff, preferred_element_type=jnp.float32)
    extra_two = (squares_two,)
    summed_two = jax.tree.map(
        lambda part: sum_at_owner(part, "kv", 0), shortened((gate_ff, up_ff) + extra_two)
    )
    rows_two = summed_two[2]
    scale_two = lax.rsqrt(rows_two / width_all + norm_floor)[:, None]
    hidden_ff = (jax.nn.silu(summed_two[0] * scale_two) * (summed_two[1] * scale_two)).astype(
        jnp.bfloat16
    )
    down_part = jnp.dot(collect(hidden_ff, "kv", 0), w_downff, preferred_element_type=jnp.float32)
    down_sum = over_copies(down_part, "tp")
    mixed = (mid_float + down_sum).astype(jnp.bfloat16)
    return (mixed, new_c, new_n, new_m)


def solution(mesh):
    placed = (
        P(None, "kv"),
        P("kv"),
        P("kv", "tp"),
        P("kv", "tp"),
        P("kv", "tp"),
        P("kv", "tp"),
        P(),
        P(),
        P("kv", "tp", None, None),
        P("kv", "tp", None),
        P("kv", "tp"),
        P("tp", "kv"),
        P("kv"),
        P("kv", "tp"),
        P("kv", "tp"),
        P("tp", "kv"),
    )
    return jax.shard_map(
        per_device,
        mesh=mesh,
        in_specs=placed,
        out_specs=(P(None, "kv"), P("kv", "tp", None, None), P("kv", "tp", None), P("kv", "tp")),
        check_vma=False,
    )
```

profile of v0, /device:TPU:1, one launch (start us, length us, event | category | flops | bytes accessed | tf_op | source)
XLA Modules:
  0.0 150.8 jit_solution(17463970850615773686)
XLA Ops:
  0.7 1.0 fusion.13
  2.4 8.6 %all-to-all-start.1 = ((bf16[16,1,8]{2,1,0:T(2,128)(2,1)}), bf16[16,1,8]{2,1,0:T(2,128)(2,1)S(1)}, u32[]{:S(2)}, u32[]{:S(2)}) async-start(bf16[16,1,8]{2,1,0:T(2,128)(2,1)} %convert_element_type.114), calls=%async_computation.1 | async-start | bytes 16384 | tf_op jit(solution)/shard_map/all_to_all | solution.py:17
  11.7 1.0 convolution_convert_fusion.4
  12.7 2.2 %fusion.2 = bf16[16,8,1536]{2,1,0:T(8,128)(2,1)} fusion(bf16[256,512]{1,0:T(8,128)(2,1)} %param.21, bf16[256,512]{1,0:T(8,128)(2,1)} %param.20, bf16[256,256]{1,0:T(8,128)(2,1)} %param.19, bf16[256,256]{1,0:T(8,128)(2,1)} %param.18, bf16[128,256]{1,0:T(8,128)(2,1)} %param.16, f32[256]{0:T(256)} %param.17), kind=kOutput, calls=%fused_computation.6 | convolution fusion | flops 104103936 | bytes 1246208 | tf_op jit(solution)/shard_map/dot_general | solution.py:89
  15.6 1.2 dynamic_slice.14
  17.3 6.2 %all-to-all-start.2 = ((bf16[16,8,16]{2,1,0:T(8,128)(2,1)}), bf16[16,8,16]{2,1,0:T(8,128)(2,1)S(1)}, u32[]{:S(2)}, u32[]{:S(2)}) async-start(bf16[16,8,16]{2,1,0:T(8,128)(2,1)} %bitcast.1), calls=%async_computation.2 | async-start | bytes 65536 | tf_op jit(solution)/shard_map/all_to_all | solution.py:17
  23.6 6.4 %all-to-all-done.2 = bf16[16,8,16]{2,1,0:T(8,128)(2,1)S(1)} async-done(((bf16[16,8,16]{2,1,0:T(8,128)(2,1)}), bf16[16,8,16]{2,1,0:T(8,128)(2,1)S(1)}, u32[]{:S(2)}, u32[]{:S(2)}) %all-to-all-start.2) | async-done | bytes 4128 | tf_op jit(solution)/shard_map/all_to_all | solution.py:17
  30.0 3.6 %all-to-all-start = ((bf16[16,8,1536]{2,1,0:T(8,128)(2,1)}), bf16[16,8,1536]{2,1,0:T(8,128)(2,1)S(1)}, u32[]{:S(2)}, u32[]{:S(2)}) async-start(bf16[16,8,1536]{2,1,0:T(8,128)(2,1)} %fusion.2), calls=%async_computation | async-start | bytes 786432 | tf_op jit(solution)/shard_map/all_to_all | solution.py:17
  34.5 7.2 %all-to-all-done = bf16[16,8,1536]{2,1,0:T(8,128)(2,1)S(1)} async-done(((bf16[16,8,1536]{2,1,0:T(8,128)(2,1)}), bf16[16,8,1536]{2,1,0:T(8,128)(2,1)S(1)}, u32[]{:S(2)}, u32[]{:S(2)}) %all-to-all-start) | async-done | bytes 393248 | tf_op jit(solution)/shard_map/all_to_all | solution.py:17
  42.9 2.6 %multiply_add_fusion = f32[8,1,512,256]{3,2,1,0:T(8,128)S(1)} fusion(f32[8,1,512,256]{3,2,1,0:T(8,128)} %param.24, f32[8,256]{1,0:T(8,128)S(1)} %get-tuple-element.26, f32[8,512]{1,0:T(8,128)S(1)} %slice_multiply_fusion, f32[8]{0:T(128)S(1)} %get-tuple-element.16), kind=kLoop, calls=%fused_computation.2 | loop fusion | flops 3145728 | bytes 8413216 | tf_op jit(solution)/shard_map/add | solution.py:115
  45.6 2.0 %copy-done.1 = f32[8,1,512,256]{3,2,1,0:T(8,128)} copy-done((f32[8,1,512,256]{3,2,1,0:T(8,128)}, f32[8,1,512,256]{3,2,1,0:T(8,128)S(1)}, u32[]{:S(2)}) %copy-start.1) | copy-done | bytes 4194328
  47.6 3.6 %fusion = f32[8,1,512]{2,1,0:T(1,128)S(1)} fusion(f32[8,1,512,256]{3,2,1,0:T(8,128)S(1)} %multiply_add_fusion, f32[8,256,1]{1,0,2:T(8,128)S(1)} %get-tuple-element.24), kind=kOutput, calls=%fused_computation | convolution fusion | flops 12582912 | bytes 4218880 | tf_op jit(solution)/shard_map/bhvd,bhd->bhv/dot_general | solution.py:119
  51.3 9.6 %all_to_all.52 = bf16[16,8,512]{2,1,0:T(8,128)(2,1)S(1)} all-to-all(bf16[16,8,512]{2,1,0:T(8,128)(2,1)S(1)} %broadcast_in_dim.8), channel_id=1, replica_groups=mesh['kv'=16,'tp'=8] {'kv'}, dimensions={0} | all-to-all | bytes 262144 | tf_op jit(solution)/shard_map/all_to_all | solution.py:31
  61.1 18.5 %all_to_all.53 = bf16[8,128,256]{2,1,0:T(8,128)(2,1)S(1)} all-to-all(bf16[8,128,256]{2,1,0:T(8,128)(2,1)S(1)} %broadcast_in_dim.9), channel_id=1, replica_groups=mesh['kv'=16,'tp'=8] {'tp'}, dimensions={0} | all-to-all | bytes 1048576 | tf_op jit(solution)/shard_map/all_to_all | solution.py:31
  80.6 3.5 %all-to-all-start.6 = ((bf16[16,1,8]{2,1,0:T(2,128)(2,1)}), bf16[16,1,8]{2,1,0:T(2,128)(2,1)S(1)}, u32[]{:S(2)}, u32[]{:S(2)}) async-start(bf16[16,1,8]{2,1,0:T(2,128)(2,1)} %convert_element_type.115), calls=%async_computation.6 | async-start | bytes 16384 | tf_op jit(solution)/shard_map/all_to_all | solution.py:17
  85.3 5.0 %all-to-all-done.6 = bf16[16,1,8]{2,1,0:T(2,128)(2,1)S(1)} async-done(((bf16[16,1,8]{2,1,0:T(2,128)(2,1)}), bf16[16,1,8]{2,1,0:T(2,128)(2,1)S(1)}, u32[]{:S(2)}, u32[]{:S(2)}) %all-to-all-start.6) | async-done | bytes 288 | tf_op jit(solution)/shard_map/all_to_all | solution.py:17
  90.3 3.5 %all-to-all-start.7 = ((bf16[16,8,1376]{2,1,0:T(8,128)(2,1)}), bf16[16,8,1376]{2,1,0:T(8,128)(2,1)S(1)}, u32[]{:S(2)}, u32[]{:S(2)}) async-start(bf16[16,8,1376]{2,1,0:T(8,128)(2,1)} %bitcast.10), calls=%async_computation.7 | async-start | bytes 720896 | tf_op jit(solution)/shard_map/all_to_all | solution.py:17
  95.2 6.8 %all-to-all-done.7 = bf16[16,8,1376]{2,1,0:T(8,128)(2,1)S(1)} async-done(((bf16[16,8,1376]{2,1,0:T(8,128)(2,1)}), bf16[16,8,1376]{2,1,0:T(8,128)(2,1)S(1)}, u32[]{:S(2)}, u32[]{:S(2)}) %all-to-all-start.7) | async-done | bytes 352288 | tf_op jit(solution)/shard_map/all_to_all | solution.py:17
  102.0 3.5 %all-to-all-start.5 = ((bf16[16,8,1376]{2,1,0:T(8,128)(2,1)}), bf16[16,8,1376]{2,1,0:T(8,128)(2,1)S(1)}, u32[]{:S(2)}, u32[]{:S(2)}) async-start(bf16[16,8,1376]{2,1,0:T(8,128)(2,1)} %bitcast.9), calls=%async_computation.5 | async-start | bytes 720896 | tf_op jit(solution)/shard_map/all_to_all | solution.py:17
  105.6 8.1 %all-to-all-done.5 = bf16[16,8,1376]{2,1,0:T(8,128)(2,1)S(1)} async-done(((bf16[16,8,1376]{2,1,0:T(8,128)(2,1)}), bf16[16,8,1376]{2,1,0:T(8,128)(2,1)S(1)}, u32[]{:S(2)}, u32[]{:S(2)}) %all-to-all-start.5) | async-done | bytes 352288 | tf_op jit(solution)/shard_map/all_to_all | solution.py:17
  113.9 10.7 %all_to_all.54 = bf16[16,8,1376]{2,1,0:T(8,128)(2,1)S(1)} all-to-all(bf16[16,8,1376]{2,1,0:T(8,128)(2,1)S(1)} %broadcast_in_dim.10), channel_id=1, replica_groups=mesh['kv'=16,'tp'=8] {'kv'}, dimensions={0} | all-to-all | bytes 704512 | tf_op jit(solution)/shard_map/all_to_all | solution.py:31
  124.8 1.1 broadcast_in_dim.11
  125.9 9.2 %all-to-all-start.9 = ((f32[8,128,256]{2,1,0:T(8,128)}), f32[8,128,256]{2,1,0:T(8,128)S(1)}, u32[]{:S(2)}, u32[]{:S(2)}) async-start(f32[8,128,256]{2,1,0:T(8,128)} %broadcast_in_dim.11), calls=%async_computation.9 | async-start | bytes 2097152 | tf_op jit(solution)/shard_map/all_to_all | solution.py:31
  135.7 14.4 %all-to-all-done.9 = f32[8,128,256]{2,1,0:T(8,128)S(1)} async-done(((f32[8,128,256]{2,1,0:T(8,128)}), f32[8,128,256]{2,1,0:T(8,128)S(1)}, u32[]{:S(2)}, u32[]{:S(2)}) %all-to-all-start.9) | async-done | bytes 1048608 | tf_op jit(solution)/shard_map/all_to_all | solution.py:31
  (53 shorter events, 10.4 us)
Async XLA Ops:
  0.6 83.4 %copy-start = (bf16[256,1376]{0,1:T(8,128)(2,1)S(1)}, bf16[256,1376]{0,1:T(8,128)(2,1)}, u32[]{:S(2)}) copy-start(bf16[256,1376]{0,1:T(8,128)(2,1)} %param.30) | copy-start | bytes 2113540
  0.6 41.4 %copy-start.6 = (f32[8,1,256]{2,1,0:T(1,128)S(1)}, f32[8,1,256]{2,1,0:T(1,128)}, u32[]{:S(2)}) copy-start(f32[8,1,256]{2,1,0:T(1,128)} %param.25) | copy-start | bytes 24580
  2.4 15.0 %all-to-all-start.1 = ((bf16[16,1,8]{2,1,0:T(2,128)(2,1)}), bf16[16,1,8]{2,1,0:T(2,128)(2,1)S(1)}, u32[]{:S(2)}, u32[]{:S(2)}) async-start(bf16[16,1,8]{2,1,0:T(2,128)(2,1)} %convert_element_type.114), calls=%async_computation.1 | async-start | bytes 16384 | tf_op jit(solution)/shard_map/all_to_all | solution.py:17
  17.3 12.6 %all-to-all-start.2 = ((bf16[16,8,16]{2,1,0:T(8,128)(2,1)}), bf16[16,8,16]{2,1,0:T(8,128)(2,1)S(1)}, u32[]{:S(2)}, u32[]{:S(2)}) async-start(bf16[16,8,16]{2,1,0:T(8,128)(2,1)} %bitcast.1), calls=%async_computation.2 | async-start | bytes 65536 | tf_op jit(solution)/shard_map/all_to_all | solution.py:17
  30.0 11.8 %all-to-all-start = ((bf16[16,8,1536]{2,1,0:T(8,128)(2,1)}), bf16[16,8,1536]{2,1,0:T(8,128)(2,1)S(1)}, u32[]{:S(2)}, u32[]{:S(2)}) async-start(bf16[16,8,1536]{2,1,0:T(8,128)(2,1)} %fusion.2), calls=%async_computation | async-start | bytes 786432 | tf_op jit(solution)/shard_map/all_to_all | solution.py:17
  45.5 2.0 %copy-start.1 = (f32[8,1,512,256]{3,2,1,0:T(8,128)}, f32[8,1,512,256]{3,2,1,0:T(8,128)S(1)}, u32[]{:S(2)}) copy-start(f32[8,1,512,256]{3,2,1,0:T(8,128)S(1)} %multiply_add_fusion) | copy-start | bytes 12582916
  45.6 15.3 %copy-start.4 = (bf16[512,256]{1,0:T(8,128)(2,1)S(1)}, bf16[512,256]{1,0:T(8,128)(2,1)}, u32[]{:S(2)}) copy-start(bf16[512,256]{1,0:T(8,128)(2,1)} %param.27) | copy-start | bytes 786436
  45.6 34.2 %copy-start.5 = (bf16[128,256]{1,0:T(8,128)(2,1)S(1)}, bf16[128,256]{1,0:T(8,128)(2,1)}, u32[]{:S(2)}) copy-start(bf16[128,256]{1,0:T(8,128)(2,1)} %param.16) | copy-start | bytes 196612
  45.6 38.5 %copy-start.7 = (f32[256]{0:T(256)S(1)}, f32[256]{0:T(256)}, u32[]{:S(2)}) copy-start(f32[256]{0:T(256)} %param.28) | copy-start | bytes 3076
  47.6 46.3 %copy-start.2 = (bf16[256,1376]{0,1:T(8,128)(2,1)S(1)}, bf16[256,1376]{0,1:T(8,128)(2,1)}, u32[]{:S(2)}) copy-start(bf16[256,1376]{0,1:T(8,128)(2,1)} %param.29) | copy-start | bytes 2113540
  79.7 44.9 %copy-start.3 = (bf16[1376,256]{1,0:T(8,128)(2,1)S(1)}, bf16[1376,256]{1,0:T(8,128)(2,1)}, u32[]{:S(2)}) copy-start(bf16[1376,256]{1,0:T(8,128)(2,1)} %param.31) | copy-start | bytes 2113540
  80.6 9.8 %all-to-all-start.6 = ((bf16[16,1,8]{2,1,0:T(2,128)(2,1)}), bf16[16,1,8]{2,1,0:T(2,128)(2,1)S(1)}, u32[]{:S(2)}, u32[]{:S(2)}) async-start(bf16[16,1,8]{2,1,0:T(2,128)(2,1)} %convert_element_type.115), calls=%async_computation.6 | async-start | bytes 16384 | tf_op jit(solution)/shard_map/all_to_all | solution.py:17
  90.3 11.7 %all-to-all-start.7 = ((bf16[16,8,1376]{2,1,0:T(8,128)(2,1)}), bf16[16,8,1376]{2,1,0:T(8,128)(2,1)S(1)}, u32[]{:S(2)}, u32[]{:S(2)}) async-start(bf16[16,8,1376]{2,1,0:T(8,128)(2,1)} %bitcast.10), calls=%async_computation.7 | async-start | bytes 720896 | tf_op jit(solution)/shard_map/all_to_all | solution.py:17
  102.0 11.7 %all-to-all-start.5 = ((bf16[16,8,1376]{2,1,0:T(8,128)(2,1)}), bf16[16,8,1376]{2,1,0:T(8,128)(2,1)S(1)}, u32[]{:S(2)}, u32[]{:S(2)}) async-start(bf16[16,8,1376]{2,1,0:T(8,128)(2,1)} %bitcast.9), calls=%async_computation.5 | async-start | bytes 720896 | tf_op jit(solution)/shard_map/all_to_all | solution.py:17
  125.9 24.2 %all-to-all-start.9 = ((f32[8,128,256]{2,1,0:T(8,128)}), f32[8,128,256]{2,1,0:T(8,128)S(1)}, u32[]{:S(2)}, u32[]{:S(2)}) async-start(f32[8,128,256]{2,1,0:T(8,128)} %broadcast_in_dim.11), calls=%async_computation.9 | async-start | bytes 2097152 | tf_op jit(solution)/shard_map/all_to_all | solution.py:31
where the time goes:
time: 152 us; the launch traced here: 151 us
  waiting for transfers between devices  48.4 us (32%)
  blocking collectives  38.8 us (26%)
  starting transfers between devices  38.1 us (25%)
  local copies, waits for them, and re-layouts  9.79 us (6%)
  matrix products  7.97 us (5%)
  other arithmetic  6.94 us (5%)
    all_to_all x3, blocking collectives, sent_to_all(): return lax.all_to_all(copies, axis, split_axis=0, concat_axis=0, tiled=True)  38.8 us
    all_to_all x6, waiting for transfers between devices, sum_at_owner(): lax.all_to_all(pieces, axis, split_axis=0, concat_axis=0, tiled=True)  34 us
    all_to_all x6, starting transfers between devices, sum_at_owner(): lax.all_to_all(pieces, axis, split_axis=0, concat_axis=0, tiled=True)  28.9 us
    all_to_all x1, waiting for transfers between devices, sent_to_all(): return lax.all_to_all(copies, axis, split_axis=0, concat_axis=0, tiled=True)  14.4 us
    all_to_all x1, starting transfers between devices, sent_to_all(): return lax.all_to_all(copies, axis, split_axis=0, concat_axis=0, tiled=True)  9.19 us
    convert_element_type x5, local copies, waits for them, and re-layouts, short(): return part.astype(jnp.bfloat16) if part.dtype == jnp.float32 else part  3.98 us
    dot_general x1, matrix products, per_device(): jnp.einsum('bhvd,bhd->bhv', new_c, query, precision=lax.Precision.HIGHEST)  3.63 us
    unnamed x18, local copies, waits for them, and re-layouts  3.33 us
  transfers between devices with their start and end apart: 7, of which 7 were waited for; matrix products, arithmetic and copies ran while one was open for 7% of the time, Pallas kernels for 0%

commit v1 on v0

v1 whole, which is shorter than its diff:
```python
import jax
import jax.numpy as jnp
from jax import lax
from jax.sharding import Mesh, PartitionSpec as P

norm_floor = 1e-05
lanes = 128


def exchange(value, axis):
    return lax.all_to_all(value, axis, split_axis=0, concat_axis=0, tiled=True)


def sent_to_all(value, axis):
    copies = jnp.broadcast_to(value, (lax.axis_size(axis), *value.shape))
    return exchange(copies, axis)


def split_pair(value):
    high = value.astype(jnp.bfloat16)
    low = (value - high.astype(jnp.float32)).astype(jnp.bfloat16)
    return high, low


def pad_to(value, width):
    return jnp.pad(value, ((0, 0), (0, width - value.shape[1])))


def shifted(value, axis, step):
    size = lax.axis_size(axis)
    return lax.ppermute(value, axis, [(i, (i + step) % size) for i in range(size)])


def summed_over_tp(part):
    mine = part.astype(jnp.bfloat16)
    theirs = shifted(mine, "core", 1)
    pair = (mine.astype(jnp.float32) + theirs.astype(jnp.float32)).astype(jnp.bfloat16)
    size = lax.axis_size("x")
    parts = [pair] + [shifted(pair, "x", step) for step in range(1, size)]
    parts = [p.astype(jnp.float32) for p in parts]
    while len(parts) > 1:
        half = len(parts) // 2
        parts = [parts[i] + parts[i + half] for i in range(half)]
    return parts[0]


def per_device(
    tokens,
    attn_gain,
    w_query,
    w_key,
    w_value,
    w_outgate,
    w_gates,
    forget_bias,
    state_c,
    state_n,
    state_m,
    w_output,
    mlp_gain,
    w_gateff,
    w_upff,
    w_downff,
):
    kv = ("z", "y")
    kv_count = lax.axis_size(kv)
    kv_at = lax.axis_index(kv)
    tp_at = lax.axis_index(("x", "core"))
    batch = tokens.shape[0]
    width_dev = tokens.shape[1]
    width_all = width_dev * kv_count
    rows = batch // kv_count
    heads_dev = state_c.shape[1]
    heads_all = forget_bias.shape[0]
    value_size = state_c.shape[2]
    query_size = state_c.shape[3]
    query_width = heads_dev * query_size
    value_width = heads_dev * value_size
    proj_width = 2 * query_width + 2 * value_width
    gates = 2 * heads_all

    tok_float = tokens.astype(jnp.float32)
    squares_one = jnp.sum(tok_float * tok_float, axis=1, keepdims=True)
    normed_one = (tok_float * attn_gain).astype(jnp.bfloat16)
    stacked = jnp.concatenate([w_query, w_key, w_value, w_outgate], axis=1)
    proj_part = jnp.dot(normed_one, stacked, preferred_element_type=jnp.float32)
    gate_rows = lax.dynamic_slice_in_dim(w_gates, kv_at * width_dev, width_dev, 0)
    gate_part = jnp.dot(normed_one, gate_rows, preferred_element_type=jnp.float32)
    extra = jnp.concatenate([gate_part, squares_one], axis=1)
    extra_width = gates + 1
    high, low = split_pair(extra)
    sent = jnp.concatenate(
        [proj_part.astype(jnp.bfloat16), pad_to(jnp.concatenate([high, low], axis=1), lanes)], axis=1
    )
    arrived = exchange(sent.reshape(kv_count, rows, proj_width + lanes), kv)
    summed = arrived.astype(jnp.float32).sum(axis=0)
    extra_sum = (
        summed[:, proj_width : proj_width + extra_width]
        + summed[:, proj_width + extra_width : proj_width + 2 * extra_width]
    )
    scale_one = lax.rsqrt(extra_sum[:, gates] / width_all + norm_floor)[:, None]
    proj_rows = summed[:, :proj_width] * scale_one
    gate_all = extra_sum[:, :gates] * scale_one
    query = (proj_rows[:, :query_width] * query_size ** (-0.5)).reshape(rows, heads_dev, query_size)
    key_vec = proj_rows[:, query_width : 2 * query_width].reshape(rows, heads_dev, query_size)
    value = proj_rows[:, 2 * query_width : 2 * query_width + value_width].reshape(
        rows, heads_dev, value_size
    )
    out_pre = proj_rows[:, 2 * query_width + value_width :].reshape(rows, heads_dev, value_size)
    log_input = lax.dynamic_slice_in_dim(gate_all, tp_at * heads_dev, heads_dev, 1)
    forget_pre = lax.dynamic_slice_in_dim(gate_all, heads_all + tp_at * heads_dev, heads_dev, 1)
    bias_dev = lax.dynamic_slice_in_dim(forget_bias, tp_at * heads_dev, heads_dev, 0)
    log_forget = jax.nn.log_sigmoid(forget_pre + bias_dev)
    carried = log_forget + state_m
    new_m = jnp.maximum(carried, log_input)
    keep = jnp.exp(carried - new_m)
    admit = jnp.exp(log_input - new_m)
    new_c = (
        keep[:, :, None, None] * state_c
        + admit[:, :, None, None] * value[:, :, :, None] * key_vec[:, :, None, :]
    )
    new_n = keep[:, :, None] * state_n + admit[:, :, None] * key_vec
    numer = jnp.einsum("bhvd,bhd->bhv", new_c, query, precision=lax.Precision.HIGHEST)
    denom = jnp.maximum(jnp.abs(jnp.sum(new_n * query, axis=-1)), jnp.exp(-new_m))
    head_out = (
        (jax.nn.sigmoid(out_pre) * numer / denom[:, :, None])
        .reshape(rows, value_width)
        .astype(jnp.bfloat16)
    )
    heads_rows = sent_to_all(head_out, kv).reshape(batch, value_width)
    attn_part = jnp.dot(heads_rows, w_output, preferred_element_type=jnp.float32)
    attn_mix = summed_over_tp(attn_part)
    middle = (tok_float + attn_mix).astype(jnp.bfloat16)
    mid_float = middle.astype(jnp.float32)
    squares_two = jnp.sum(mid_float * mid_float, axis=1, keepdims=True)
    normed_two = (mid_float * mlp_gain).astype(jnp.bfloat16)
    gate_ff = jnp.dot(normed_two, w_gateff, preferred_element_type=jnp.float32)
    up_ff = jnp.dot(normed_two, w_upff, preferred_element_type=jnp.float32)
    hidden_dev = w_gateff.shape[1]
    hidden_pad = -(-(hidden_dev + 2) // lanes) * lanes
    high, low = split_pair(squares_two)
    sent = jnp.concatenate(
        [
            pad_to(gate_ff.astype(jnp.bfloat16), hidden_pad),
            pad_to(jnp.concatenate([up_ff.astype(jnp.bfloat16), high, low], axis=1), hidden_pad),
        ],
        axis=1,
    )
    arrived = exchange(sent.reshape(kv_count, rows, 2 * hidden_pad), kv)
    summed = arrived.astype(jnp.float32).sum(axis=0)
    at = hidden_pad + hidden_dev
    rows_two = summed[:, at : at + 1] + summed[:, at + 1 : at + 2]
    scale_two = lax.rsqrt(rows_two / width_all + norm_floor)
    hidden_ff = (
        jax.nn.silu(summed[:, :hidden_dev] * scale_two)
        * (summed[:, hidden_pad : hidden_pad + hidden_dev] * scale_two)
    ).astype(jnp.bfloat16)
    hidden_rows = sent_to_all(hidden_ff, kv).reshape(batch, hidden_dev)
    down_part = jnp.dot(hidden_rows, w_downff, preferred_element_type=jnp.float32)
    mixed = (mid_float + summed_over_tp(down_part)).astype(jnp.bfloat16)
    return (mixed, new_c, new_n, new_m)


def solution(mesh):
    kv = ("z", "y")
    tp = ("x", "core")
    cores = 2
    tp_size = mesh.shape["tp"]
    fine = Mesh(
        mesh.devices.reshape(4, mesh.shape["kv"] // 4, tp_size // cores, cores), kv + tp
    )
    placed = (
        P(None, kv),
        P(kv),
        P(kv, tp),
        P(kv, tp),
        P(kv, tp),
        P(kv, tp),
        P(),
        P(),
        P(kv, tp, None, None),
        P(kv, tp, None),
        P(kv, tp),
        P(tp, kv),
        P(kv),
        P(kv, tp),
        P(kv, tp),
        P(tp, kv),
    )
    return jax.shard_map(
        per_device,
        mesh=fine,
        in_specs=placed,
        out_specs=(P(None, kv), P(kv, tp, None, None), P(kv, tp, None), P(kv, tp)),
        check_vma=False,
    )
```

time: 152 us -> 96.6 us (0.64)
  waiting for transfers between devices: 48.4 us -> 18.5 us
  starting transfers between devices: 38.1 us -> 23 us
  local copies, waits for them, and re-layouts: 9.79 us -> 3.37 us
  blocking collectives: 38.8 us -> 35.7 us
    all_to_all x7 -> x1, waiting for transfers between devices: 48.4 us -> 8.9 us  [exchange(): return lax.all_to_all(value, axis, split_axis=0, concat_axis=0, tiled=True)]
    all_to_all x7 -> x1, starting transfers between devices: 38.1 us -> 8.58 us  [exchange(): return lax.all_to_all(value, axis, split_axis=0, concat_axis=0, tiled=True)]
    ppermute x0 -> x8, starting transfers between devices: none -> 14.4 us  [shifted(): lax.ppermute(value, axis, [(i, (i + step) % size) for i in range(size)])]
    ppermute x0 -> x8, waiting for transfers between devices: none -> 9.57 us  [shifted(): lax.ppermute(value, axis, [(i, (i + step) % size) for i in range(size)])]
    convert_element_type x5 -> x0, local copies, waits for them, and re-layouts: 3.98 us -> none  [short(): return part.astype(jnp.bfloat16) if part.dtype == jnp.float32 else part]
    all_to_all x3, blocking collectives: 38.8 us -> 35.7 us  [exchange(): return lax.all_to_all(value, axis, split_axis=0, concat_axis=0, tiled=True)]
    unnamed x18 -> x23, local copies, waits for them, and re-layouts: 3.33 us -> 1.34 us
  transfers between devices with their start and end apart: 7 -> 9, of which waited for: 7 -> 6; matrix products, arithmetic and copies ran while one was open for 7% -> 2% of each run, Pallas kernels for 0% -> 0%
where the time goes in v1:
time: 96.6 us; the launch traced here: 96.2 us
  blocking collectives  35.7 us (37%)
  starting transfers between devices  23 us (24%)
  waiting for transfers between devices  18.5 us (19%)
  other arithmetic  7.56 us (8%)
  matrix products  7.2 us (7%)
  local copies, waits for them, and re-layouts  3.37 us (3%)
    all_to_all x3, blocking collectives, exchange(): return lax.all_to_all(value, axis, split_axis=0, concat_axis=0, tiled=True)  35.7 us
    ppermute x8, starting transfers between devices, shifted(): lax.ppermute(value, axis, [(i, (i + step) % size) for i in range(size)])  14.4 us
    ppermute x8, waiting for transfers between devices, shifted(): lax.ppermute(value, axis, [(i, (i + step) % size) for i in range(size)])  9.57 us
    all_to_all x1, waiting for transfers between devices, exchange(): return lax.all_to_all(value, axis, split_axis=0, concat_axis=0, tiled=True)  8.9 us
    all_to_all x1, starting transfers between devices, exchange(): return lax.all_to_all(value, axis, split_axis=0, concat_axis=0, tiled=True)  8.58 us
    dot_general x1, matrix products, per_device(): jnp.einsum('bhvd,bhd->bhv', new_c, query, precision=lax.Precision.HIGHEST)  3.63 us
    add x1, other arithmetic, per_device(): keep[:, :, None, None] * state_c  2.6 us
  transfers between devices with their start and end apart: 9, of which 6 were waited for; matrix products, arithmetic and copies ran while one was open for 2% of the time, Pallas kernels for 0%

profile of v1, /device:TPU:1, one launch (start us, length us, event | category | flops | bytes accessed | tf_op | source)
XLA Modules:
  0.0 96.2 jit_solution(11965617885612960155)
XLA Ops:
  0.7 1.0 %fusion.17 = f32[128]{0:T(128)S(1)} fusion(bf16[128,256]{1,0:T(8,128)(2,1)} %param.16), kind=kLoop, calls=%fused_computation.34 | loop fusion | flops 98176 | bytes 66048 | tf_op jit(solution)/shard_map/reduce_sum | solution.py:83
  1.7 1.0 %fusion.25 = f32[128,16]{0,1:T(8,128)S(1)} fusion(bf16[128,256]{1,0:T(8,128)(2,1)} %param.16, f32[256]{0:T(256)} %param.17, bf16[4096,16]{0,1:T(8,128)(2,1)} %param.22, s32[]{:T(128)S(6)} %select_n.17), kind=kOutput, calls=%fused_computation.42 | convolution fusion | flops 1146880 | bytes 82948 | tf_op jit(solution)/shard_map/dot_general | solution.py:88
  2.8 1.4 %convolution_convert_fusion.2 = bf16[128,1536]{1,0:T(8,128)(2,1)S(1)} fusion(bf16[256,512]{1,0:T(8,128)(2,1)} %param.21, bf16[256,512]{1,0:T(8,128)(2,1)} %param.20, bf16[256,256]{1,0:T(8,128)(2,1)} %param.19, bf16[256,256]{1,0:T(8,128)(2,1)} %param.18, bf16[128,256]{1,0:T(8,128)(2,1)} %param.16, f32[256]{0:T(256)} %param.17), kind=kOutput, calls=%fused_computation.5 | convolution fusion | flops 104103936 | bytes 1246208 | tf_op jit(solution)/shard_map/dot_general | solution.py:86
  4.3 0.8 fusion.14
  5.1 8.6 %all-to-all-start = ((bf16[16,8,1664]{2,1,0:T(8,128)(2,1)}), bf16[16,8,1664]{2,1,0:T(8,128)(2,1)S(1)}, u32[]{:S(2)}, u32[]{:S(2)}) async-start(bf16[16,8,1664]{2,1,0:T(8,128)(2,1)} %fusion.14), calls=%async_computation | async-start | bytes 851968 | tf_op jit(solution)/shard_map/all_to_all | solution.py:11
  14.4 8.9 %all-to-all-done = bf16[16,8,1664]{2,1,0:T(8,128)(2,1)S(1)} async-done(((bf16[16,8,1664]{2,1,0:T(8,128)(2,1)}), bf16[16,8,1664]{2,1,0:T(8,128)(2,1)S(1)}, u32[]{:S(2)}, u32[]{:S(2)}) %all-to-all-start) | async-done | bytes 426016 | tf_op jit(solution)/shard_map/all_to_all | solution.py:11
  23.8 0.9 exponential_reduce_fusion.1
  25.1 2.6 %multiply_add_fusion = f32[8,1,512,256]{3,2,1,0:T(8,128)S(1)} fusion(f32[8,1,512,256]{3,2,1,0:T(8,128)} %param.24, f32[8,256]{1,0:T(8,128)S(1)} %get-tuple-element.28, f32[8,512]{1,0:T(8,128)S(1)} %slice_multiply_fusion.3, f32[8]{0:T(128)S(1)} %get-tuple-element.20), kind=kLoop, calls=%fused_computation.2 | loop fusion | flops 3145728 | bytes 8413216 | tf_op jit(solution)/shard_map/add | solution.py:119
  27.8 3.6 %fusion = f32[8,1,512]{2,1,0:T(1,128)S(1)} fusion(f32[8,1,512,256]{3,2,1,0:T(8,128)S(1)} %multiply_add_fusion, f32[8,256,1]{1,0,2:T(8,128)S(1)} %get-tuple-element.27), kind=kOutput, calls=%fused_computation | convolution fusion | flops 12582912 | bytes 4218880 | tf_op jit(solution)/shard_map/bhvd,bhd->bhv/dot_general | solution.py:123
  31.5 9.9 %all_to_all.20 = bf16[16,8,512]{2,1,0:T(8,128)(2,1)S(1)} all-to-all(bf16[16,8,512]{2,1,0:T(8,128)(2,1)S(1)} %broadcast_in_dim.7), channel_id=1, replica_groups=mesh['z'=4,'y'=4,'x'=4,'core'=2] {'z','y'}, dimensions={0} | all-to-all | bytes 262144 | tf_op jit(solution)/shard_map/all_to_all | solution.py:11
  41.7 3.0 %collective-permute-start = (bf16[128,256]{1,0:T(8,128)(2,1)S(1)}, bf16[128,256]{1,0:T(8,128)(2,1)S(1)}, u32[]{:S(2)}, u32[]{:S(2)}) collective-permute-start(bf16[128,256]{1,0:T(8,128)(2,1)S(1)} %convolution_convert_fusion.4), channel_id=1, source_target_pairs={{0,1},{1,0},{2,3},{3,2},{4,5},{5,4},{6,7},{7,6},{8,9},{9,8},{10,11... | collective-permute-start | bytes 196616 | tf_op jit(solution)/shard_map/ppermute | solution.py:31
  44.7 0.9 collective-permute-done
  45.6 2.5 %collective-permute-start.3 = (bf16[128,256]{1,0:T(8,128)(2,1)S(1)}, bf16[128,256]{1,0:T(8,128)(2,1)S(1)}, u32[]{:S(2)}, u32[]{:S(2)}) collective-permute-start(bf16[128,256]{1,0:T(8,128)(2,1)S(1)} %add_convert_fusion.1), channel_id=1, source_target_pairs={{0,6},{2,0},{4,2},{6,4},{1,7},{3,1},{5,3},{7,5},{8,14},{10,8},{12,... | collective-permute-start | bytes 196616 | tf_op jit(solution)/shard_map/ppermute | solution.py:31
  48.2 1.7 %collective-permute-start.1 = (bf16[128,256]{1,0:T(8,128)(2,1)S(1)}, bf16[128,256]{1,0:T(8,128)(2,1)S(1)}, u32[]{:S(2)}, u32[]{:S(2)}) collective-permute-start(bf16[128,256]{1,0:T(8,128)(2,1)S(1)} %add_convert_fusion.1), channel_id=1, source_target_pairs={{0,4},{2,6},{4,0},{6,2},{1,5},{3,7},{5,1},{7,3},{8,12},{10,14},{12... | collective-permute-start | bytes 196616 | tf_op jit(solution)/shard_map/ppermute | solution.py:31
  49.9 3.0 %collective-permute-done.2 = bf16[128,256]{1,0:T(8,128)(2,1)S(1)} collective-permute-done((bf16[128,256]{1,0:T(8,128)(2,1)S(1)}, bf16[128,256]{1,0:T(8,128)(2,1)S(1)}, u32[]{:S(2)}, u32[]{:S(2)}) %collective-permute-start.2) | collective-permute-done | bytes 65568 | tf_op jit(solution)/shard_map/ppermute | solution.py:31
  52.9 0.9 collective-permute-done.1
  54.7 0.9 concatenate.22
  55.9 14.8 %all_to_all.21 = bf16[16,8,2816]{2,1,0:T(8,128)(2,1)S(1)} all-to-all(bf16[16,8,2816]{2,1,0:T(8,128)(2,1)S(1)} %bitcast.40), channel_id=1, replica_groups=mesh['z'=4,'y'=4,'x'=4,'core'=2] {'z','y'}, dimensions={0} | all-to-all | bytes 1441792 | tf_op jit(solution)/shard_map/all_to_all | solution.py:11
  71.2 11.0 %all_to_all.22 = bf16[16,8,1376]{2,1,0:T(8,128)(2,1)S(1)} all-to-all(bf16[16,8,1376]{2,1,0:T(8,128)(2,1)S(1)} %broadcast_in_dim.8), channel_id=1, replica_groups=mesh['z'=4,'y'=4,'x'=4,'core'=2] {'z','y'}, dimensions={0} | all-to-all | bytes 704512 | tf_op jit(solution)/shard_map/all_to_all | solution.py:11
  82.4 4.1 %collective-permute-start.4 = (bf16[128,256]{1,0:T(8,128)(2,1)S(1)}, bf16[128,256]{1,0:T(8,128)(2,1)S(1)}, u32[]{:S(2)}, u32[]{:S(2)}) collective-permute-start(bf16[128,256]{1,0:T(8,128)(2,1)S(1)} %convolution_convert_fusion.3), channel_id=1, source_target_pairs={{0,1},{1,0},{2,3},{3,2},{4,5},{5,4},{6,7},{7,6},{8,9},{9,8},{10,11... | collective-permute-start | bytes 196616 | tf_op jit(solution)/shard_map/ppermute | solution.py:31
  86.5 0.9 collective-permute-done.4
  87.4 1.7 %collective-permute-start.7 = (bf16[128,256]{1,0:T(8,128)(2,1)S(1)}, bf16[128,256]{1,0:T(8,128)(2,1)S(1)}, u32[]{:S(2)}, u32[]{:S(2)}) collective-permute-start(bf16[128,256]{1,0:T(8,128)(2,1)S(1)} %add_convert_fusion), channel_id=1, source_target_pairs={{0,6},{2,0},{4,2},{6,4},{1,7},{3,1},{5,3},{7,5},{8,14},{10,8},{12,... | collective-permute-start | bytes 196616 | tf_op jit(solution)/shard_map/ppermute | solution.py:31
  89.2 1.3 %collective-permute-start.5 = (bf16[128,256]{1,0:T(8,128)(2,1)S(1)}, bf16[128,256]{1,0:T(8,128)(2,1)S(1)}, u32[]{:S(2)}, u32[]{:S(2)}) collective-permute-start(bf16[128,256]{1,0:T(8,128)(2,1)S(1)} %add_convert_fusion), channel_id=1, source_target_pairs={{0,4},{2,6},{4,0},{6,2},{1,5},{3,7},{5,1},{7,3},{8,12},{10,14},{12... | collective-permute-start | bytes 196616 | tf_op jit(solution)/shard_map/ppermute | solution.py:31
  91.6 3.9 %collective-permute-done.6 = bf16[128,256]{1,0:T(8,128)(2,1)S(1)} collective-permute-done((bf16[128,256]{1,0:T(8,128)(2,1)S(1)}, bf16[128,256]{1,0:T(8,128)(2,1)S(1)}, u32[]{:S(2)}, u32[]{:S(2)}) %collective-permute-start.6) | collective-permute-done | bytes 65568 | tf_op jit(solution)/shard_map/ppermute | solution.py:31
  (62 shorter events, 5.9 us)
Async XLA Ops:
  0.6 53.3 %copy-start = (bf16[256,1376]{0,1:T(8,128)(2,1)S(1)}, bf16[256,1376]{0,1:T(8,128)(2,1)}, u32[]{:S(2)}) copy-start(bf16[256,1376]{0,1:T(8,128)(2,1)} %param.30) | copy-start | bytes 2113540
  4.3 9.4 %copy-start.8 = (f32[8,1]{0,1:T(1,128)S(1)}, f32[8,1]{0,1:T(1,128)}, u32[]{:S(2)}) copy-start(f32[8,1]{0,1:T(1,128)} %param.26) | copy-start | bytes 100
  4.3 9.5 %copy-start.9 = (f32[8]{0:T(128)S(1)}, f32[8]{0:T(128)}, u32[]{:S(2)}) copy-start(f32[8]{0:T(128)} %param.23) | copy-start | bytes 100
  4.3 20.4 %copy-start.6 = (f32[8,1,256]{2,1,0:T(1,128)S(1)}, f32[8,1,256]{2,1,0:T(1,128)}, u32[]{:S(2)}) copy-start(f32[8,1,256]{2,1,0:T(1,128)} %param.25) | copy-start | bytes 24580
  5.1 18.2 %all-to-all-start = ((bf16[16,8,1664]{2,1,0:T(8,128)(2,1)}), bf16[16,8,1664]{2,1,0:T(8,128)(2,1)S(1)}, u32[]{:S(2)}, u32[]{:S(2)}) async-start(bf16[16,8,1664]{2,1,0:T(8,128)(2,1)} %fusion.14), calls=%async_computation | async-start | bytes 851968 | tf_op jit(solution)/shard_map/all_to_all | solution.py:11
  27.8 3.7 %copy-start.1 = (f32[8,1,512,256]{3,2,1,0:T(8,128)}, f32[8,1,512,256]{3,2,1,0:T(8,128)S(1)}, u32[]{:S(2)}) copy-start(f32[8,1,512,256]{3,2,1,0:T(8,128)S(1)} %multiply_add_fusion) | copy-start | bytes 12582916
  27.8 13.7 %copy-start.5 = (bf16[512,256]{1,0:T(8,128)(2,1)S(1)}, bf16[512,256]{1,0:T(8,128)(2,1)}, u32[]{:S(2)}) copy-start(bf16[512,256]{1,0:T(8,128)(2,1)} %param.27) | copy-start | bytes 786436
  27.8 26.0 %copy-start.4 = (bf16[128,256]{1,0:T(8,128)(2,1)S(1)}, bf16[128,256]{1,0:T(8,128)(2,1)}, u32[]{:S(2)}) copy-start(bf16[128,256]{1,0:T(8,128)(2,1)} %param.16) | copy-start | bytes 196612
  27.8 26.2 %copy-start.7 = (f32[256]{0:T(256)S(1)}, f32[256]{0:T(256)}, u32[]{:S(2)}) copy-start(f32[256]{0:T(256)} %param.28) | copy-start | bytes 3076
  31.4 22.9 %copy-start.2 = (bf16[256,1376]{0,1:T(8,128)(2,1)S(1)}, bf16[256,1376]{0,1:T(8,128)(2,1)}, u32[]{:S(2)}) copy-start(bf16[256,1376]{0,1:T(8,128)(2,1)} %param.29) | copy-start | bytes 2113540
  41.7 3.9 %collective-permute-start = (bf16[128,256]{1,0:T(8,128)(2,1)S(1)}, bf16[128,256]{1,0:T(8,128)(2,1)S(1)}, u32[]{:S(2)}, u32[]{:S(2)}) collective-permute-start(bf16[128,256]{1,0:T(8,128)(2,1)S(1)} %convolution_convert_fusion.4), channel_id=1, source_target_pairs={{0,1},{1,0},{2,3},{3,2},{4,5},{5,4},{6,7},{7,6},{8,9},{9,8},{10,11... | collective-permute-start | bytes 196616 | tf_op jit(solution)/shard_map/ppermute | solution.py:31
  45.6 4.3 %collective-permute-start.3 = (bf16[128,256]{1,0:T(8,128)(2,1)S(1)}, bf16[128,256]{1,0:T(8,128)(2,1)S(1)}, u32[]{:S(2)}, u32[]{:S(2)}) collective-permute-start(bf16[128,256]{1,0:T(8,128)(2,1)S(1)} %add_convert_fusion.1), channel_id=1, source_target_pairs={{0,6},{2,0},{4,2},{6,4},{1,7},{3,1},{5,3},{7,5},{8,14},{10,8},{12,... | collective-permute-start | bytes 196616 | tf_op jit(solution)/shard_map/ppermute | solution.py:31
  48.2 4.7 %collective-permute-start.2 = (bf16[128,256]{1,0:T(8,128)(2,1)S(1)}, bf16[128,256]{1,0:T(8,128)(2,1)S(1)}, u32[]{:S(2)}, u32[]{:S(2)}) collective-permute-start(bf16[128,256]{1,0:T(8,128)(2,1)S(1)} %add_convert_fusion.1), channel_id=1, source_target_pairs={{0,2},{2,4},{4,6},{6,0},{1,3},{3,5},{5,7},{7,1},{8,10},{10,12},{12... | collective-permute-start | bytes 196616 | tf_op jit(solution)/shard_map/ppermute | solution.py:31
  48.2 5.6 %collective-permute-start.1 = (bf16[128,256]{1,0:T(8,128)(2,1)S(1)}, bf16[128,256]{1,0:T(8,128)(2,1)S(1)}, u32[]{:S(2)}, u32[]{:S(2)}) collective-permute-start(bf16[128,256]{1,0:T(8,128)(2,1)S(1)} %add_convert_fusion.1), channel_id=1, source_target_pairs={{0,4},{2,6},{4,0},{6,2},{1,5},{3,7},{5,1},{7,3},{8,12},{10,14},{12... | collective-permute-start | bytes 196616 | tf_op jit(solution)/shard_map/ppermute | solution.py:31
  55.9 26.2 %copy-start.3 = (bf16[1376,256]{1,0:T(8,128)(2,1)S(1)}, bf16[1376,256]{1,0:T(8,128)(2,1)}, u32[]{:S(2)}) copy-start(bf16[1376,256]{1,0:T(8,128)(2,1)} %param.31) | copy-start | bytes 2113540
  82.4 5.0 %collective-permute-start.4 = (bf16[128,256]{1,0:T(8,128)(2,1)S(1)}, bf16[128,256]{1,0:T(8,128)(2,1)S(1)}, u32[]{:S(2)}, u32[]{:S(2)}) collective-permute-start(bf16[128,256]{1,0:T(8,128)(2,1)S(1)} %convolution_convert_fusion.3), channel_id=1, source_target_pairs={{0,1},{1,0},{2,3},{3,2},{4,5},{5,4},{6,7},{7,6},{8,9},{9,8},{10,11... | collective-permute-start | bytes 196616 | tf_op jit(solution)/shard_map/ppermute | solution.py:31
  87.4 4.2 %collective-permute-start.7 = (bf16[128,256]{1,0:T(8,128)(2,1)S(1)}, bf16[128,256]{1,0:T(8,128)(2,1)S(1)}, u32[]{:S(2)}, u32[]{:S(2)}) collective-permute-start(bf16[128,256]{1,0:T(8,128)(2,1)S(1)} %add_convert_fusion), channel_id=1, source_target_pairs={{0,6},{2,0},{4,2},{6,4},{1,7},{3,1},{5,3},{7,5},{8,14},{10,8},{12,... | collective-permute-start | bytes 196616 | tf_op jit(solution)/shard_map/ppermute | solution.py:31
  89.2 6.3 %collective-permute-start.6 = (bf16[128,256]{1,0:T(8,128)(2,1)S(1)}, bf16[128,256]{1,0:T(8,128)(2,1)S(1)}, u32[]{:S(2)}, u32[]{:S(2)}) collective-permute-start(bf16[128,256]{1,0:T(8,128)(2,1)S(1)} %add_convert_fusion), channel_id=1, source_target_pairs={{0,2},{2,4},{4,6},{6,0},{1,3},{3,5},{5,7},{7,1},{8,10},{10,12},{12... | collective-permute-start | bytes 196616 | tf_op jit(solution)/shard_map/ppermute | solution.py:31
  89.2 6.3 %collective-permute-start.5 = (bf16[128,256]{1,0:T(8,128)(2,1)S(1)}, bf16[128,256]{1,0:T(8,128)(2,1)S(1)}, u32[]{:S(2)}, u32[]{:S(2)}) collective-permute-start(bf16[128,256]{1,0:T(8,128)(2,1)S(1)} %add_convert_fusion), channel_id=1, source_target_pairs={{0,4},{2,6},{4,0},{6,2},{1,5},{3,7},{5,1},{7,3},{8,12},{10,14},{12... | collective-permute-start | bytes 196616 | tf_op jit(solution)/shard_map/ppermute | solution.py:31

commit v2 on v1

v2 whole, which is shorter than its diff:
```python
import functools

import jax
import jax.numpy as jnp
from jax import lax
from jax.experimental import pallas as pl
from jax.experimental.pallas import tpu as pltpu
from jax.sharding import Mesh, PartitionSpec as P

norm_floor = 1e-05
lanes = 128
kv = ("z", "y")
tp = ("x", "core")
vmem = pl.BlockSpec(memory_space=pltpu.VMEM)
smem = pl.BlockSpec(memory_space=pltpu.SMEM)
anywhere = pl.BlockSpec(memory_space=pl.ANY)
low_at = 32
nt_dims = (((1,), (1,)), ((), ()))


def params(mib):
    return pltpu.CompilerParams(vmem_limit_bytes=mib << 20)


def cost(flops, moved):
    return pl.CostEstimate(flops=flops, bytes_accessed=moved, transcendentals=0)


def index_of(axes):
    at = 0
    for axis in axes:
        at = at * lax.axis_size(axis) + lax.axis_index(axis)
    return at


def lane_ids(shape):
    return lax.broadcasted_iota(jnp.int32, shape, len(shape) - 1)


def row_ids(shape):
    return lax.broadcasted_iota(jnp.int32, shape, 0)


def split_pair(value):
    high = value.astype(jnp.bfloat16)
    low = (value - high.astype(jnp.float32)).astype(jnp.bfloat16)
    return high, low


def exchange(value, axis):
    return lax.all_to_all(value, axis, split_axis=0, concat_axis=0, tiled=True)


def sent_to_all(value, axis):
    copies = jnp.broadcast_to(value, (lax.axis_size(axis), *value.shape))
    return exchange(copies, axis)


def shifted(value, axis, step):
    size = lax.axis_size(axis)
    return lax.ppermute(value, axis, [(i, (i + step) % size) for i in range(size)])


def over_tp(part):
    mine = part.astype(jnp.bfloat16)
    theirs = shifted(mine, "core", 1)
    pair = (mine.astype(jnp.float32) + theirs.astype(jnp.float32)).astype(jnp.bfloat16)
    return [pair] + [shifted(pair, "x", step) for step in range(1, lax.axis_size("x"))]


def in_order(terms):
    terms = [term.astype(jnp.float32) for term in terms]
    while len(terms) > 1:
        half = len(terms) // 2
        terms = [terms[i] + terms[i + half] for i in range(half)]
    return terms[0]


def project_kernel(
    tokens, gain_in, w_query, w_key, w_value, w_outgate, gates_t, sent, tok, gain, weights, gate_rows, sems
):
    width = tok.shape[1]
    gates = gates_t.shape[0]
    moves = [(tokens, tok), (gain_in, gain)]
    at = 0
    for source in (w_query, w_key, w_value, w_outgate):
        columns = source.shape[1]
        moves.append((source, weights.at[:, pl.ds(at, columns)]))
        at += columns
    mine = pl.ds(pl.multiple_of(index_of(kv) * width, width), width)
    for row in (0, low_at):
        moves.append((gates_t.at[:, mine], gate_rows.at[pl.ds(row, gates), :]))
    copies = [pltpu.make_async_copy(*move, sems.at[i]) for i, move in enumerate(moves)]
    for copy in copies:
        copy.start()
    for start, end in ((gates, low_at), (low_at + gates, lanes)):
        gate_rows[start:end, :] = jnp.zeros((end - start, width), gate_rows.dtype)
    for copy in copies[:2]:
        copy.wait()
    values = tok[...].astype(jnp.float32)
    squares = jnp.sum(values * values, axis=1, keepdims=True)
    normed = (values * gain[...]).astype(jnp.bfloat16)
    for copy in copies[2:]:
        copy.wait()
    product = jnp.dot(normed, weights[...], preferred_element_type=jnp.float32)
    sent[:, :at] = product.astype(jnp.bfloat16)
    extra = lax.dot_general(normed, gate_rows[...], nt_dims, preferred_element_type=jnp.float32)
    lane = lane_ids(extra.shape)
    extra = jnp.where((lane == gates) | (lane == low_at + gates), squares, extra)
    high, low = split_pair(extra)
    sent[:, at:] = jnp.where(lane < low_at, high.astype(jnp.float32), low.astype(jnp.float32)).astype(
        jnp.bfloat16
    )


def shorten_kernel(state, short):
    short[0] = state[0, 0].astype(jnp.bfloat16)


def cell_kernel(
    width_all, arrived, state_short, state_n, state_m, bias, sent, to_write, value_out, new_n, new_m
):
    rows = arrived.shape[1]
    value_size, query_size = state_short.shape[1:]
    proj_width = 2 * query_size + 2 * value_size
    heads = bias.shape[0]
    total = arrived[0].astype(jnp.float32)
    for i in range(1, arrived.shape[0]):
        total = total + arrived[i].astype(jnp.float32)
    extra = total[:, proj_width:]
    lane = lane_ids(extra.shape)

    def column(at):
        picked = jnp.where((lane == at) | (lane == at + low_at), extra, 0.0)
        return jnp.sum(picked, axis=1, keepdims=True)

    head = index_of(tp)
    scale = lax.rsqrt(column(2 * heads) / width_all + norm_floor)
    log_input = column(head) * scale
    forget_pre = column(heads + head) * scale + bias[head]
    log_forget = jnp.minimum(forget_pre, 0.0) - jnp.log(1.0 + jnp.exp(-jnp.abs(forget_pre)))
    square = (rows, rows)
    diagonal = row_ids(square) == lane_ids(square)
    old_m = jnp.sum(jnp.where(diagonal, jnp.broadcast_to(state_m[...], square), 0.0), axis=1, keepdims=True)
    carried = log_forget + old_m
    top = jnp.maximum(carried, log_input)
    keep = jnp.exp(carried - top)
    admit = jnp.exp(log_input - top)
    query = total[:, :query_size] * (scale * query_size ** (-0.5))
    key_in = total[:, query_size : 2 * query_size] * (scale * admit)
    value = total[:, 2 * query_size : 2 * query_size + value_size] * scale
    out_pre = total[:, 2 * query_size + value_size : proj_width] * scale
    later_n = keep * state_n[...].reshape(rows, query_size) + key_in
    normalizer = jnp.sum(later_n * query, axis=1, keepdims=True)
    denom = jnp.maximum(jnp.abs(normalizer), jnp.exp(-top))
    match = jnp.sum(key_in * query, axis=1, keepdims=True)
    q_high, q_low = split_pair(query)
    both = jnp.concatenate([q_high.astype(jnp.float32), q_low.astype(jnp.float32)], axis=0)
    row = row_ids(both.shape)
    reads = jnp.zeros((2 * rows, value_size), jnp.float32)
    for b in range(rows):
        one = jnp.where((row == b) | (row == b + rows), both, 0.0).astype(jnp.bfloat16)
        reads += lax.dot_general(one, state_short[b], nt_dims, preferred_element_type=jnp.float32)
    numer = keep * (reads[:rows] + reads[rows:]) + match * value
    head_out = numer / ((1.0 + jnp.exp(-out_pre)) * denom)
    short = head_out.astype(jnp.bfloat16)
    for i in range(sent.shape[0]):
        sent[i] = short
    to_write[:, :lanes] = jnp.broadcast_to(keep, (rows, lanes))
    to_write[:, lanes:] = key_in
    value_out[...] = value
    new_n[...] = later_n.reshape(new_n.shape)
    new_m[...] = jnp.sum(jnp.where(diagonal, jnp.broadcast_to(top, square), 0.0), axis=0, keepdims=True)


def write_kernel(to_write, value, state, new_c):
    b = pl.program_id(0)
    across = value[...].T
    picked = jnp.where(lane_ids(across.shape) == b, across, 0.0)
    down = jnp.sum(picked, axis=1, keepdims=True)
    packed = to_write[...]
    mine = jnp.sum(jnp.where(row_ids(packed.shape) == b, packed, 0.0), axis=0, keepdims=True)
    keep = mine[:, :1]
    key_in = mine[:, lanes:]
    new_c[0, 0] = keep * state[0, 0] + down * key_in


def widen_kernel(term_0, term_1, term_2, term_3, tok, gain, gate_t, up_t, sent, middle):
    attn_mix = in_order([term[...] for term in (term_0, term_1, term_2, term_3)])
    mid = (tok[...].astype(jnp.float32) + attn_mix).astype(jnp.bfloat16)
    middle[...] = mid
    mid_float = mid.astype(jnp.float32)
    squares = jnp.sum(mid_float * mid_float, axis=1, keepdims=True)
    normed = (mid_float * gain[...]).astype(jnp.bfloat16)
    hidden = gate_t.shape[0]
    half = sent.shape[1] // 2
    rest = half - hidden
    high, low = split_pair(squares)
    lane = lane_ids((tok.shape[0], rest))
    stats = jnp.where(
        lane == 0, high.astype(jnp.float32), jnp.where(lane == 1, low.astype(jnp.float32), 0.0)
    )
    for at, weight, tail in ((0, gate_t, jnp.zeros_like(stats)), (half, up_t, stats)):
        product = lax.dot_general(normed, weight[...], nt_dims, preferred_element_type=jnp.float32)
        whole = jnp.concatenate([product, tail], axis=1)
        sent[:, at : at + half] = whole.astype(jnp.bfloat16)


def per_device(
    tokens,
    attn_gain,
    w_query,
    w_key,
    w_value,
    w_outgate,
    w_gates,
    forget_bias,
    state_c,
    state_n,
    state_m,
    w_output,
    mlp_gain,
    w_gateff,
    w_upff,
    w_downff,
):
    kv_count = lax.axis_size(kv)
    batch, width_dev = tokens.shape
    width_all = width_dev * kv_count
    rows = batch // kv_count
    heads_all = forget_bias.shape[0]
    _, _, value_size, query_size = state_c.shape
    proj_width = 2 * query_size + 2 * value_size
    f32, bf16 = jnp.float32, jnp.bfloat16

    sent = pl.pallas_call(
        project_kernel,
        out_shape=jax.ShapeDtypeStruct((batch, proj_width + lanes), bf16),
        in_specs=[anywhere] * 7,
        out_specs=vmem,
        scratch_shapes=[
            pltpu.VMEM((batch, width_dev), bf16),
            pltpu.VMEM((1, width_dev), f32),
            pltpu.VMEM((width_dev, proj_width), bf16),
            pltpu.VMEM((lanes, width_dev), bf16),
            pltpu.SemaphoreType.DMA((8,)),
        ],
        cost_estimate=cost(2 * batch * width_dev * proj_width, 2 * width_dev * proj_width),
        name="project",
    )(tokens, attn_gain.reshape(1, width_dev), w_query, w_key, w_value, w_outgate, w_gates.T)
    state_short = pl.pallas_call(
        shorten_kernel,
        out_shape=jax.ShapeDtypeStruct((rows, value_size, query_size), bf16),
        grid=(rows,),
        in_specs=[pl.BlockSpec((1, 1, value_size, query_size), lambda b: (b, 0, 0, 0))],
        out_specs=pl.BlockSpec((1, value_size, query_size), lambda b: (b, 0, 0)),
        cost_estimate=cost(10**9, 6 * rows * value_size * query_size),
        name="shorten_state",
    )(state_c)
    arrived = exchange(sent.reshape(kv_count, rows, proj_width + lanes), kv)
    head_copies, to_write, value, new_n, new_m = pl.pallas_call(
        functools.partial(cell_kernel, width_all),
        out_shape=(
            jax.ShapeDtypeStruct((kv_count, rows, value_size), bf16),
            jax.ShapeDtypeStruct((rows, lanes + query_size), f32),
            jax.ShapeDtypeStruct((rows, value_size), f32),
            jax.ShapeDtypeStruct((rows, 1, query_size), f32),
            jax.ShapeDtypeStruct((1, rows), f32),
        ),
        in_specs=[vmem] * 4 + [smem],
        out_specs=[vmem] * 5,
        compiler_params=params(8),
        cost_estimate=cost(10**8, 4 * rows * value_size * query_size),
        name="cell",
    )(arrived, state_short, state_n, state_m.reshape(1, rows), forget_bias)
    block = pl.BlockSpec((1, 1, value_size, query_size), lambda b: (b, 0, 0, 0))
    new_c = pl.pallas_call(
        write_kernel,
        out_shape=jax.ShapeDtypeStruct(state_c.shape, f32),
        grid=(rows,),
        in_specs=[
            pl.BlockSpec((rows, lanes + query_size), lambda b: (0, 0)),
            pl.BlockSpec((rows, value_size), lambda b: (0, 0)),
            block,
        ],
        out_specs=block,
        cost_estimate=cost(10**9, 8 * rows * value_size * query_size),
        name="write_state",
    )(to_write, value, state_c)
    heads_rows = exchange(head_copies, kv).reshape(batch, value_size)
    attn_part = jnp.dot(heads_rows, w_output, preferred_element_type=f32)
    hidden_dev = w_gateff.shape[1]
    hidden_pad = -(-(hidden_dev + 2) // lanes) * lanes
    sent, middle = pl.pallas_call(
        widen_kernel,
        out_shape=(
            jax.ShapeDtypeStruct((batch, 2 * hidden_pad), bf16),
            jax.ShapeDtypeStruct((batch, width_dev), bf16),
        ),
        in_specs=[vmem] * 8,
        out_specs=[vmem] * 2,
        compiler_params=params(8),
        cost_estimate=cost(4 * batch * width_dev * hidden_dev, 4 * width_dev * hidden_dev),
        name="widen",
    )(
        *over_tp(attn_part),
        tokens,
        mlp_gain.reshape(1, width_dev),
        w_gateff.T,
        w_upff.T,
    )
    mid_float = middle.astype(f32)
    arrived = exchange(sent.reshape(kv_count, rows, 2 * hidden_pad), kv)
    summed = arrived.astype(jnp.float32).sum(axis=0)
    at = hidden_pad + hidden_dev
    rows_two = summed[:, at : at + 1] + summed[:, at + 1 : at + 2]
    scale_two = lax.rsqrt(rows_two / width_all + norm_floor)
    hidden_ff = (
        jax.nn.silu(summed[:, :hidden_dev] * scale_two)
        * (summed[:, hidden_pad : hidden_pad + hidden_dev] * scale_two)
    ).astype(jnp.bfloat16)
    hidden_rows = sent_to_all(hidden_ff, kv).reshape(batch, hidden_dev)
    down_part = jnp.dot(hidden_rows, w_downff, preferred_element_type=jnp.float32)
    mixed = (mid_float + in_order(over_tp(down_part))).astype(jnp.bfloat16)
    return (mixed, new_c, new_n, new_m.reshape(rows, 1))


def solution(mesh):
    cores = 2
    tp_size = mesh.shape["tp"]
    fine = Mesh(
        mesh.devices.reshape(4, mesh.shape["kv"] // 4, tp_size // cores, cores), kv + tp
    )
    placed = (
        P(None, kv),
        P(kv),
        P(kv, tp),
        P(kv, tp),
        P(kv, tp),
        P(kv, tp),
        P(),
        P(),
        P(kv, tp, None, None),
        P(kv, tp, None),
        P(kv, tp),
        P(tp, kv),
        P(kv),
        P(kv, tp),
        P(kv, tp),
        P(tp, kv),
    )
    return jax.shard_map(
        per_device,
        mesh=fine,
        in_specs=placed,
        out_specs=(P(None, kv), P(kv, tp, None, None), P(kv, tp, None), P(kv, tp)),
        check_vma=False,
    )
```

time: 96.6 us -> 91.7 us (0.949)
  Pallas kernels: 0 us -> 18.4 us
  waiting for transfers between devices: 18.5 us -> 10.4 us
  matrix products: 7.2 us -> 0.46 us
  other arithmetic: 7.56 us -> 1.1 us
  starting transfers between devices: 23 us -> 21 us
    pallas_call x0 -> x5, Pallas kernels: none -> 18.4 us  [the longest x1 7.63 us: per_device(): pl.pallas_call(write_kernel, out_shape=jax.ShapeDtypeStruct(state_c.shape...]
    dot_general x6 -> x1, matrix products: 6.93 us -> 0.19 us  [per_device(): attn_part = jnp.dot(heads_rows, w_output, preferred_element_type=f32)]
    all_to_all x1, waiting for transfers between devices: 8.9 us -> 3.31 us  [exchange(): return lax.all_to_all(value, axis, split_axis=0, concat_axis=0, tiled=True)]
    add x2 -> x0, other arithmetic: 2.68 us -> none  [the longest x1 2.6 us: per_device(): keep[:, :, None, None] * state_c]
    ppermute x8, waiting for transfers between devices: 9.57 us -> 7.06 us  [shifted(): lax.ppermute(value, axis, [(i, (i + step) % size) for i in range(size)])]
    ppermute x8, starting transfers between devices: 14.4 us -> 12.4 us  [shifted(): lax.ppermute(value, axis, [(i, (i + step) % size) for i in range(size)])]
    unnamed x23 -> x24, local copies, waits for them, and re-layouts: 1.34 us -> 2.84 us
    reduce_sum x3 -> x0, other arithmetic: 1.33 us -> none  [the longest x1 1.01 us: per_device(): squares_one = jnp.sum(tok_float * tok_float, axis=1, keepdims=True)]
  transfers between devices with their start and end apart: 9 -> 9, of which waited for: 6 -> 6; matrix products, arithmetic and copies ran while one was open for 2% -> 0% of each run, Pallas kernels for 0% -> 15%
where the time goes in v2:
time: 91.7 us; the launch traced here: 91 us
  blocking collectives  36 us (39%)
  starting transfers between devices  21 us (23%)
  Pallas kernels  18.4 us (20%)
  waiting for transfers between devices  10.4 us (11%)
  local copies, waits for them, and re-layouts  2.87 us (3%)
  other arithmetic  1.1 us (1%)
    all_to_all x3, blocking collectives, exchange(): return lax.all_to_all(value, axis, split_axis=0, concat_axis=0, tiled=True)  36 us
    ppermute x8, starting transfers between devices, shifted(): lax.ppermute(value, axis, [(i, (i + step) % size) for i in range(size)])  12.4 us
    all_to_all x1, starting transfers between devices, exchange(): return lax.all_to_all(value, axis, split_axis=0, concat_axis=0, tiled=True)  8.6 us
    pallas_call x1, Pallas kernels, per_device(): pl.pallas_call(write_kernel, out_shape=jax.ShapeDtypeStruct(state_c.shape...  7.63 us
    ppermute x8, waiting for transfers between devices, shifted(): lax.ppermute(value, axis, [(i, (i + step) % size) for i in range(size)])  7.06 us
    pallas_call x1, Pallas kernels, per_device(): pl.pallas_call(shorten_kernel, out_shape=jax.ShapeDtypeStruct((rows, valu...  6.21 us
    all_to_all x1, waiting for transfers between devices, exchange(): return lax.all_to_all(value, axis, split_axis=0, concat_axis=0, tiled=True)  3.31 us
    unnamed x24, local copies, waits for them, and re-layouts  2.84 us
  transfers between devices with their start and end apart: 9, of which 6 were waited for; matrix products, arithmetic and copies ran while one was open for 0% of the time, Pallas kernels for 15%

profile of v2, /device:TPU:1, one launch (start us, length us, event | category | flops | bytes accessed | tf_op | source)
XLA Modules:
  0.0 91.0 jit_solution(11901431885630944411)
XLA Ops:
  0.7 2.4 %project.1 = bf16[128,1664]{1,0:T(8,128)(2,1)} custom-call(bf16[128,256]{1,0:T(8,128)(2,1)} %tok.1, f32[1,256]{1,0:T(1,128)} %bitcast.24, bf16[256,256]{1,0:T(8,128)(2,1)} %w_query.1, bf16[256,256]{1,0:T(8,128)(2,1)} %w_key.1, bf16[256,512]{1,0:T(8,128)(2,1)} %w_value.1, bf16[256,512]{1,0:T(8,128)(2,1)} %w_outgate.1, bf16[16,4096]{1,0:T(8,128)(2,1)} %bitcast.23), custom_call_target="tpu_custom_call" | custom-call | flops 100663296 | bytes 786432 | tf_op jit(solution)/shard_map/project/pallas_call | solution.py:236
  3.1 8.6 %all-to-all-start = ((bf16[16,8,1664]{2,1,0:T(8,128)(2,1)}), bf16[16,8,1664]{2,1,0:T(8,128)(2,1)S(1)}, u32[]{:S(2)}, u32[]{:S(2)}) async-start(bf16[16,8,1664]{2,1,0:T(8,128)(2,1)} %bitcast.22), calls=%async_computation | async-start | bytes 851968 | tf_op jit(solution)/shard_map/all_to_all | solution.py:51
  11.8 6.2 %shorten_state.1.state_short = bf16[8,512,256]{2,1,0:T(8,128)(2,1)} custom-call(f32[8,1,512,256]{3,2,1,0:T(8,128)} %state.3), custom_call_target="tpu_custom_call" | custom-call | flops 1000000000 | bytes 6291456 | tf_op jit(solution)/shard_map/shorten_state/pallas_call | solution.py:251
  18.0 3.3 %all-to-all-done.arrived = bf16[16,8,1664]{2,1,0:T(8,128)(2,1)S(1)} async-done(((bf16[16,8,1664]{2,1,0:T(8,128)(2,1)}), bf16[16,8,1664]{2,1,0:T(8,128)(2,1)S(1)}, u32[]{:S(2)}, u32[]{:S(2)}) %all-to-all-start) | async-done | bytes 426016 | tf_op jit(solution)/shard_map/all_to_all | solution.py:51
  21.3 1.6 %copy-done.1 = bf16[8,512,256]{2,1,0:T(8,128)(2,1)S(1)} copy-done((bf16[8,512,256]{2,1,0:T(8,128)(2,1)S(1)}, bf16[8,512,256]{2,1,0:T(8,128)(2,1)}, u32[]{:S(2)}) %copy-start.1) | copy-done | bytes 2097176
  22.9 1.6 %cell.1 = (bf16[16,8,512]{2,1,0:T(8,128)(2,1)S(1)}, f32[8,384]{1,0:T(8,128)S(1)}, f32[8,512]{1,0:T(8,128)S(1)}, f32[8,1,256]{2,1,0:T(1,128)}, f32[1,8]{1,0:T(1,128)}) custom-call(bf16[16,8,1664]{2,1,0:T(8,128)(2,1)S(1)} %all-to-all-done.arrived, bf16[8,512,256]{2,1,0:T(8,128)(2,1)S(1)} %copy-done.1, f32[8,1,256]{2,1,0:T(1,128)S(1)} %copy-done.7, ...), custom_call_target="tpu_custom_call" | custom-call | flops 100000000 | bytes 4194304 | tf_op jit(solution)/shard_map/cell/pallas_call | solution.py:261
  24.5 0.6 copy-done.5
  25.1 0.6 copy-done.6
  25.7 10.0 %all_to_all.20 = bf16[16,8,512]{2,1,0:T(8,128)(2,1)S(1)} all-to-all(bf16[16,8,512]{2,1,0:T(8,128)(2,1)S(1)} %get-tuple-element.11), channel_id=1, replica_groups=mesh['z'=4,'y'=4,'x'=4,'core'=2] {'z','y'}, dimensions={0} | all-to-all | bytes 262144 | tf_op jit(solution)/shard_map/all_to_all | solution.py:51
  35.8 2.8 %collective-permute-start = (bf16[128,256]{1,0:T(8,128)(2,1)S(1)}, bf16[128,256]{1,0:T(8,128)(2,1)S(1)}, u32[]{:S(2)}, u32[]{:S(2)}) collective-permute-start(bf16[128,256]{1,0:T(8,128)(2,1)S(1)} %convolution_convert_fusion.1), channel_id=1, source_target_pairs={{0,1},{1,0},{2,3},{3,2},{4,5},{5,4},{6,7},{7,6},{8,9},{9,8},{10,11... | collective-permute-start | bytes 196616 | tf_op jit(solution)/shard_map/ppermute | solution.py:61
  38.7 0.9 collective-permute-done
  39.6 2.5 %collective-permute-start.3 = (bf16[128,256]{1,0:T(8,128)(2,1)S(1)}, bf16[128,256]{1,0:T(8,128)(2,1)S(1)}, u32[]{:S(2)}, u32[]{:S(2)}) collective-permute-start(bf16[128,256]{1,0:T(8,128)(2,1)S(1)} %add_convert_fusion.2.term_0), channel_id=1, source_target_pairs={{0,6},{2,0},{4,2},{6,4},{1,7},{3,1},{5,3},{7,5},{8,14},{10,8},{12,... | collective-permute-start | bytes 196616 | tf_op jit(solution)/shard_map/ppermute | solution.py:61
  42.6 0.6 collective-permute-start.1
  43.5 3.3 %collective-permute-done.2.term_2 = bf16[128,256]{1,0:T(8,128)(2,1)S(1)} collective-permute-done((bf16[128,256]{1,0:T(8,128)(2,1)S(1)}, bf16[128,256]{1,0:T(8,128)(2,1)S(1)}, u32[]{:S(2)}, u32[]{:S(2)}) %collective-permute-start.2) | collective-permute-done | bytes 65568 | tf_op jit(solution)/shard_map/ppermute | solution.py:61
  46.8 1.7 %collective-permute-done.1.term_1 = bf16[128,256]{1,0:T(8,128)(2,1)S(1)} collective-permute-done((bf16[128,256]{1,0:T(8,128)(2,1)S(1)}, bf16[128,256]{1,0:T(8,128)(2,1)S(1)}, u32[]{:S(2)}, u32[]{:S(2)}) %collective-permute-start.1) | collective-permute-done | bytes 65568 | tf_op jit(solution)/shard_map/ppermute | solution.py:61
  48.5 0.6 widen.1
  49.1 15.0 %all_to_all.21 = bf16[16,8,2816]{2,1,0:T(8,128)(2,1)S(1)} all-to-all(bf16[16,8,2816]{2,1,0:T(8,128)(2,1)S(1)} %bitcast.17), channel_id=1, replica_groups=mesh['z'=4,'y'=4,'x'=4,'core'=2] {'z','y'}, dimensions={0} | all-to-all | bytes 1441792 | tf_op jit(solution)/shard_map/all_to_all | solution.py:51
  64.5 11.1 %all_to_all.22 = bf16[16,8,1376]{2,1,0:T(8,128)(2,1)S(1)} all-to-all(bf16[16,8,1376]{2,1,0:T(8,128)(2,1)S(1)} %broadcast_in_dim.3), channel_id=1, replica_groups=mesh['z'=4,'y'=4,'x'=4,'core'=2] {'z','y'}, dimensions={0} | all-to-all | bytes 704512 | tf_op jit(solution)/shard_map/all_to_all | solution.py:51
  75.9 3.6 %collective-permute-start.4 = (bf16[128,256]{1,0:T(8,128)(2,1)S(1)}, bf16[128,256]{1,0:T(8,128)(2,1)S(1)}, u32[]{:S(2)}, u32[]{:S(2)}) collective-permute-start(bf16[128,256]{1,0:T(8,128)(2,1)S(1)} %convolution_convert_fusion), channel_id=1, source_target_pairs={{0,1},{1,0},{2,3},{3,2},{4,5},{5,4},{6,7},{7,6},{8,9},{9,8},{10,11... | collective-permute-start | bytes 196616 | tf_op jit(solution)/shard_map/ppermute | solution.py:61
  79.5 0.9 collective-permute-done.4
  80.5 1.5 %collective-permute-start.6 = (bf16[128,256]{1,0:T(8,128)(2,1)S(1)}, bf16[128,256]{1,0:T(8,128)(2,1)S(1)}, u32[]{:S(2)}, u32[]{:S(2)}) collective-permute-start(bf16[128,256]{1,0:T(8,128)(2,1)S(1)} %add_convert_fusion.1), channel_id=1, source_target_pairs={{0,2},{2,4},{4,6},{6,0},{1,3},{3,5},{5,7},{7,1},{8,10},{10,12},{12... | collective-permute-start | bytes 196616 | tf_op jit(solution)/shard_map/ppermute | solution.py:61
  81.9 0.7 collective-permute-start.5
  82.7 7.6 %write_state.1 = f32[8,1,512,256]{3,2,1,0:T(8,128)} custom-call(f32[8,384]{1,0:T(8,128)} %copy-done.6, f32[8,512]{1,0:T(8,128)} %copy-done.5, f32[8,1,512,256]{3,2,1,0:T(8,128)} %state.3), custom_call_target="tpu_custom_call" | custom-call | flops 1000000000 | bytes 8388608 | tf_op jit(solution)/shard_map/write_state/pallas_call | solution.py:277
  90.3 0.7 add_convert_fusion
  (35 shorter events, 1.8 us)
Async XLA Ops:
  0.6 74.9 %copy-start = (bf16[1376,256]{1,0:T(8,128)(2,1)S(1)}, bf16[1376,256]{1,0:T(8,128)(2,1)}, u32[]{:S(2)}) copy-start(bf16[1376,256]{1,0:T(8,128)(2,1)} %param.31) | copy-start | bytes 2113540
  0.7 20.6 %copy-start.7 = (f32[8,1,256]{2,1,0:T(1,128)S(1)}, f32[8,1,256]{2,1,0:T(1,128)}, u32[]{:S(2)}) copy-start(f32[8,1,256]{2,1,0:T(1,128)} %state_n.1) | copy-start | bytes 24580
  0.7 20.6 %copy-start.9 = (f32[8,1]{0,1:T(1,128)S(1)}, f32[8,1]{0,1:T(1,128)}, u32[]{:S(2)}) copy-start(f32[8,1]{0,1:T(1,128)} %param.26) | copy-start | bytes 100
  0.7 20.6 %copy-start.10 = (f32[8]{0:T(128)S(1)}, f32[8]{0:T(128)}, u32[]{:S(2)}) copy-start(f32[8]{0:T(128)} %bias.1) | copy-start | bytes 100
  3.1 18.2 %all-to-all-start = ((bf16[16,8,1664]{2,1,0:T(8,128)(2,1)}), bf16[16,8,1664]{2,1,0:T(8,128)(2,1)S(1)}, u32[]{:S(2)}, u32[]{:S(2)}) async-start(bf16[16,8,1664]{2,1,0:T(8,128)(2,1)} %bitcast.22), calls=%async_computation | async-start | bytes 851968 | tf_op jit(solution)/shard_map/all_to_all | solution.py:51
  11.7 23.9 %copy-start.11 = (bf16[512,256]{1,0:T(8,128)(2,1)S(1)}, bf16[512,256]{1,0:T(8,128)(2,1)}, u32[]{:S(2)}) copy-start(bf16[512,256]{1,0:T(8,128)(2,1)} %param.27) | copy-start | bytes 786436
  11.7 36.8 %copy-start.2 = (bf16[256,1376]{0,1:T(8,128)(2,1)S(1)}, bf16[256,1376]{0,1:T(8,128)(2,1)}, u32[]{:S(2)}) copy-start(bf16[256,1376]{0,1:T(8,128)(2,1)} %param.29) | copy-start | bytes 2113540
  11.7 36.8 %copy-start.3 = (bf16[256,1376]{0,1:T(8,128)(2,1)S(1)}, bf16[256,1376]{0,1:T(8,128)(2,1)}, u32[]{:S(2)}) copy-start(bf16[256,1376]{0,1:T(8,128)(2,1)} %param.30) | copy-start | bytes 2113540
  11.7 36.8 %copy-start.4 = (bf16[128,256]{1,0:T(8,128)(2,1)S(1)}, bf16[128,256]{1,0:T(8,128)(2,1)}, u32[]{:S(2)}) copy-start(bf16[128,256]{1,0:T(8,128)(2,1)} %tok.1) | copy-start | bytes 196612
  11.7 36.8 %copy-start.8 = (f32[256]{0:T(256)S(1)}, f32[256]{0:T(256)}, u32[]{:S(2)}) copy-start(f32[256]{0:T(256)} %param.28) | copy-start | bytes 3076
  21.3 1.6 %copy-start.1 = (bf16[8,512,256]{2,1,0:T(8,128)(2,1)S(1)}, bf16[8,512,256]{2,1,0:T(8,128)(2,1)}, u32[]{:S(2)}) copy-start(bf16[8,512,256]{2,1,0:T(8,128)(2,1)} %shorten_state.1.state_short) | copy-start | bytes 6291460
  24.5 0.6 copy-start.5
  25.1 0.6 copy-start.6
  35.8 3.7 %collective-permute-start = (bf16[128,256]{1,0:T(8,128)(2,1)S(1)}, bf16[128,256]{1,0:T(8,128)(2,1)S(1)}, u32[]{:S(2)}, u32[]{:S(2)}) collective-permute-start(bf16[128,256]{1,0:T(8,128)(2,1)S(1)} %convolution_convert_fusion.1), channel_id=1, source_target_pairs={{0,1},{1,0},{2,3},{3,2},{4,5},{5,4},{6,7},{7,6},{8,9},{9,8},{10,11... | collective-permute-start | bytes 196616 | tf_op jit(solution)/shard_map/ppermute | solution.py:61
  39.6 3.9 %collective-permute-start.3 = (bf16[128,256]{1,0:T(8,128)(2,1)S(1)}, bf16[128,256]{1,0:T(8,128)(2,1)S(1)}, u32[]{:S(2)}, u32[]{:S(2)}) collective-permute-start(bf16[128,256]{1,0:T(8,128)(2,1)S(1)} %add_convert_fusion.2.term_0), channel_id=1, source_target_pairs={{0,6},{2,0},{4,2},{6,4},{1,7},{3,1},{5,3},{7,5},{8,14},{10,8},{12,... | collective-permute-start | bytes 196616 | tf_op jit(solution)/shard_map/ppermute | solution.py:61
  42.1 4.7 %collective-permute-start.2 = (bf16[128,256]{1,0:T(8,128)(2,1)S(1)}, bf16[128,256]{1,0:T(8,128)(2,1)S(1)}, u32[]{:S(2)}, u32[]{:S(2)}) collective-permute-start(bf16[128,256]{1,0:T(8,128)(2,1)S(1)} %add_convert_fusion.2.term_0), channel_id=1, source_target_pairs={{0,4},{2,6},{4,0},{6,2},{1,5},{3,7},{5,1},{7,3},{8,12},{10,14},{12... | collective-permute-start | bytes 196616 | tf_op jit(solution)/shard_map/ppermute | solution.py:61
  42.6 5.9 %collective-permute-start.1 = (bf16[128,256]{1,0:T(8,128)(2,1)S(1)}, bf16[128,256]{1,0:T(8,128)(2,1)S(1)}, u32[]{:S(2)}, u32[]{:S(2)}) collective-permute-start(bf16[128,256]{1,0:T(8,128)(2,1)S(1)} %add_convert_fusion.2.term_0), channel_id=1, source_target_pairs={{0,2},{2,4},{4,6},{6,0},{1,3},{3,5},{5,7},{7,1},{8,10},{10,12},{12... | collective-permute-start | bytes 196616 | tf_op jit(solution)/shard_map/ppermute | solution.py:61
  75.9 4.5 %collective-permute-start.4 = (bf16[128,256]{1,0:T(8,128)(2,1)S(1)}, bf16[128,256]{1,0:T(8,128)(2,1)S(1)}, u32[]{:S(2)}, u32[]{:S(2)}) collective-permute-start(bf16[128,256]{1,0:T(8,128)(2,1)S(1)} %convolution_convert_fusion), channel_id=1, source_target_pairs={{0,1},{1,0},{2,3},{3,2},{4,5},{5,4},{6,7},{7,6},{8,9},{9,8},{10,11... | collective-permute-start | bytes 196616 | tf_op jit(solution)/shard_map/ppermute | solution.py:61
  80.4 9.9 %collective-permute-start.7 = (bf16[128,256]{1,0:T(8,128)(2,1)S(1)}, bf16[128,256]{1,0:T(8,128)(2,1)S(1)}, u32[]{:S(2)}, u32[]{:S(2)}) collective-permute-start(bf16[128,256]{1,0:T(8,128)(2,1)S(1)} %add_convert_fusion.1), channel_id=1, source_target_pairs={{0,6},{2,0},{4,2},{6,4},{1,7},{3,1},{5,3},{7,5},{8,14},{10,8},{12,... | collective-permute-start | bytes 196616 | tf_op jit(solution)/shard_map/ppermute | solution.py:61
  80.5 9.8 %collective-permute-start.6 = (bf16[128,256]{1,0:T(8,128)(2,1)S(1)}, bf16[128,256]{1,0:T(8,128)(2,1)S(1)}, u32[]{:S(2)}, u32[]{:S(2)}) collective-permute-start(bf16[128,256]{1,0:T(8,128)(2,1)S(1)} %add_convert_fusion.1), channel_id=1, source_target_pairs={{0,2},{2,4},{4,6},{6,0},{1,3},{3,5},{5,7},{7,1},{8,10},{10,12},{12... | collective-permute-start | bytes 196616 | tf_op jit(solution)/shard_map/ppermute | solution.py:61
  81.9 8.4 %collective-permute-start.5 = (bf16[128,256]{1,0:T(8,128)(2,1)S(1)}, bf16[128,256]{1,0:T(8,128)(2,1)S(1)}, u32[]{:S(2)}, u32[]{:S(2)}) collective-permute-start(bf16[128,256]{1,0:T(8,128)(2,1)S(1)} %add_convert_fusion.1), channel_id=1, source_target_pairs={{0,4},{2,6},{4,0},{6,2},{1,5},{3,7},{5,1},{7,3},{8,12},{10,14},{12... | collective-permute-start | bytes 196616 | tf_op jit(solution)/shard_map/ppermute | solution.py:61

commit v3 on v2

--- a/solution.py
+++ b/solution.py
@@ -13,7 +13,7 @@
 tp = ("x", "core")
 vmem = pl.BlockSpec(memory_space=pltpu.VMEM)
 smem = pl.BlockSpec(memory_space=pltpu.SMEM)
-anywhere = pl.BlockSpec(memory_space=pl.ANY)
+hbm = pl.BlockSpec(memory_space=pltpu.HBM)
 low_at = 32
 nt_dims = (((1,), (1,)), ((), ()))
 
@@ -113,8 +113,16 @@
     )
 
 
-def shorten_kernel(state, short):
-    short[0] = state[0, 0].astype(jnp.bfloat16)
+def shorten_kernel(state, weight, short, near, held, sems):
+    count = held.shape[0]
+    copies = [pltpu.make_async_copy(state.at[b, 0], held.at[b], sems.at[b]) for b in range(count)]
+    copies.append(pltpu.make_async_copy(weight, near, sems.at[count]))
+    for copy in copies:
+        copy.start()
+    for b in range(count):
+        copies[b].wait()
+        short[b] = held[b].astype(jnp.bfloat16)
+    copies[count].wait()
 
 
 def cell_kernel(
@@ -173,19 +181,36 @@
     new_m[...] = jnp.sum(jnp.where(diagonal, jnp.broadcast_to(top, square), 0.0), axis=0, keepdims=True)
 
 
-def write_kernel(to_write, value, state, new_c):
-    b = pl.program_id(0)
+def write_kernel(first, to_write, value, state, *refs):
+    new_c, order, held, sems_in, sems_out = refs[-5:]
+    order[...] = jnp.zeros_like(order)
+    count = held.shape[0]
+    into = [
+        pltpu.make_async_copy(state.at[first + b, 0], held.at[b], sems_in.at[b])
+        for b in range(count)
+    ]
+    out = [
+        pltpu.make_async_copy(held.at[b], new_c.at[first + b, 0], sems_out.at[b])
+        for b in range(count)
+    ]
+    for copy in into:
+        copy.start()
     across = value[...].T
-    picked = jnp.where(lane_ids(across.shape) == b, across, 0.0)
-    down = jnp.sum(picked, axis=1, keepdims=True)
-    packed = to_write[...]
-    mine = jnp.sum(jnp.where(row_ids(packed.shape) == b, packed, 0.0), axis=0, keepdims=True)
-    keep = mine[:, :1]
-    key_in = mine[:, lanes:]
-    new_c[0, 0] = keep * state[0, 0] + down * key_in
-
-
-def widen_kernel(term_0, term_1, term_2, term_3, tok, gain, gate_t, up_t, sent, middle):
+    for b in range(count):
+        row = first + b
+        down = across[:, row : row + 1]
+        keep = to_write[row : row + 1, :1]
+        key_in = to_write[row : row + 1, lanes:]
+        into[b].wait()
+        held[b] = keep * held[b] + down * key_in
+        out[b].start()
+    for copy in out:
+        copy.wait()
+
+
+def widen_kernel(
+    term_0, term_1, term_2, term_3, tok, gain, gate_t, up_t, order, sent, middle
+):
     attn_mix = in_order([term[...] for term in (term_0, term_1, term_2, term_3)])
     mid = (tok[...].astype(jnp.float32) + attn_mix).astype(jnp.bfloat16)
     middle[...] = mid
@@ -236,7 +261,7 @@
     sent = pl.pallas_call(
         project_kernel,
         out_shape=jax.ShapeDtypeStruct((batch, proj_width + lanes), bf16),
-        in_specs=[anywhere] * 7,
+        in_specs=[hbm] * 7,
         out_specs=vmem,
         scratch_shapes=[
             pltpu.VMEM((batch, width_dev), bf16),
@@ -245,18 +270,26 @@
             pltpu.VMEM((lanes, width_dev), bf16),
             pltpu.SemaphoreType.DMA((8,)),
         ],
+        compiler_params=params(60),
         cost_estimate=cost(2 * batch * width_dev * proj_width, 2 * width_dev * proj_width),
         name="project",
     )(tokens, attn_gain.reshape(1, width_dev), w_query, w_key, w_value, w_outgate, w_gates.T)
-    state_short = pl.pallas_call(
+    state_short, w_output_near = pl.pallas_call(
         shorten_kernel,
-        out_shape=jax.ShapeDtypeStruct((rows, value_size, query_size), bf16),
-        grid=(rows,),
-        in_specs=[pl.BlockSpec((1, 1, value_size, query_size), lambda b: (b, 0, 0, 0))],
-        out_specs=pl.BlockSpec((1, value_size, query_size), lambda b: (b, 0, 0)),
+        out_shape=(
+            jax.ShapeDtypeStruct((rows, value_size, query_size), bf16),
+            jax.ShapeDtypeStruct(w_output.shape, w_output.dtype),
+        ),
+        in_specs=[hbm, hbm],
+        out_specs=(vmem, vmem),
+        scratch_shapes=[
+            pltpu.VMEM((rows, value_size, query_size), f32),
+            pltpu.SemaphoreType.DMA((rows + 1,)),
+        ],
+        compiler_params=params(49),
         cost_estimate=cost(10**9, 6 * rows * value_size * query_size),
         name="shorten_state",
-    )(state_c)
+    )(state_c, w_output)
     arrived = exchange(sent.reshape(kv_count, rows, proj_width + lanes), kv)
     head_copies, to_write, value, new_n, new_m = pl.pallas_call(
         functools.partial(cell_kernel, width_all),
@@ -273,22 +306,32 @@
         cost_estimate=cost(10**8, 4 * rows * value_size * query_size),
         name="cell",
     )(arrived, state_short, state_n, state_m.reshape(1, rows), forget_bias)
-    block = pl.BlockSpec((1, 1, value_size, query_size), lambda b: (b, 0, 0, 0))
-    new_c = pl.pallas_call(
-        write_kernel,
-        out_shape=jax.ShapeDtypeStruct(state_c.shape, f32),
-        grid=(rows,),
-        in_specs=[
-            pl.BlockSpec((rows, lanes + query_size), lambda b: (0, 0)),
-            pl.BlockSpec((rows, value_size), lambda b: (0, 0)),
-            block,
-        ],
-        out_specs=block,
-        cost_estimate=cost(10**9, 8 * rows * value_size * query_size),
-        name="write_state",
-    )(to_write, value, state_c)
+    half_rows = rows // 2
+
+    def written(first, *begun):
+        return pl.pallas_call(
+            functools.partial(write_kernel, first),
+            out_shape=(
+                jax.ShapeDtypeStruct(state_c.shape, f32),
+                jax.ShapeDtypeStruct((8, lanes), f32),
+            ),
+            in_specs=[vmem, vmem, hbm] + [hbm] * len(begun),
+            out_specs=(hbm, vmem),
+            input_output_aliases={3: 0} if begun else {},
+            scratch_shapes=[
+                pltpu.VMEM((half_rows, value_size, query_size), f32),
+                pltpu.SemaphoreType.DMA((half_rows,)),
+                pltpu.SemaphoreType.DMA((half_rows,)),
+            ],
+            compiler_params=params(50),
+            cost_estimate=cost(10**9, 4 * rows * value_size * query_size),
+            name="write_state",
+        )(to_write, value, state_c, *begun)
+
+    begun_c, order = written(0)
+    new_c, _ = written(half_rows, begun_c)
     heads_rows = exchange(head_copies, kv).reshape(batch, value_size)
-    attn_part = jnp.dot(heads_rows, w_output, preferred_element_type=f32)
+    attn_part = jnp.dot(heads_rows, w_output_near, preferred_element_type=f32)
     hidden_dev = w_gateff.shape[1]
     hidden_pad = -(-(hidden_dev + 2) // lanes) * lanes
     sent, middle = pl.pallas_call(
@@ -297,7 +340,7 @@
             jax.ShapeDtypeStruct((batch, 2 * hidden_pad), bf16),
             jax.ShapeDtypeStruct((batch, width_dev), bf16),
         ),
-        in_specs=[vmem] * 8,
+        in_specs=[vmem] * 9,
         out_specs=[vmem] * 2,
         compiler_params=params(8),
         cost_estimate=cost(4 * batch * width_dev * hidden_dev, 4 * width_dev * hidden_dev),
@@ -308,6 +351,7 @@
         mlp_gain.reshape(1, width_dev),
         w_gateff.T,
         w_upff.T,
+        order,
     )
     mid_float = middle.astype(f32)
     arrived = exchange(sent.reshape(kv_count, rows, 2 * hidden_pad), kv)

time: 91.7 us -> 87.7 us (0.956)
  Pallas kernels: 18.4 us -> 12.5 us
  waiting for transfers between devices: 10.4 us -> 11.6 us
    pallas_call x2 -> x3, Pallas kernels: 13.8 us -> 7.96 us  [the longest x2 5.71 us: written(): pl.pallas_call(functools.partial(write_kernel, first), out_shape=(jax.Sha...]
    all_to_all x1, waiting for transfers between devices: 3.31 us -> 6.36 us  [exchange(): return lax.all_to_all(value, axis, split_axis=0, concat_axis=0, tiled=True)]
    ppermute x8, waiting for transfers between devices: 7.06 us -> 5.2 us  [shifted(): lax.ppermute(value, axis, [(i, (i + step) % size) for i in range(size)])]
    unnamed x24 -> x18, local copies, waits for them, and re-layouts: 2.84 us -> 3.09 us
  transfers between devices with their start and end apart: 9 -> 9, of which waited for: 6 -> 6; matrix products, arithmetic and copies ran while one was open for 0% -> 0% of each run, Pallas kernels for 15% -> 9%
where the time goes in v3:
time: 87.7 us; the launch traced here: 86.5 us
  blocking collectives  35.8 us (41%)
  starting transfers between devices  21.2 us (24%)
  Pallas kernels  12.5 us (14%)
  waiting for transfers between devices  11.6 us (13%)
  local copies, waits for them, and re-layouts  3.12 us (4%)
  other arithmetic  1.1 us (1%)
    all_to_all x3, blocking collectives, exchange(): return lax.all_to_all(value, axis, split_axis=0, concat_axis=0, tiled=True)  35.8 us
    ppermute x8, starting transfers between devices, shifted(): lax.ppermute(value, axis, [(i, (i + step) % size) for i in range(size)])  12.6 us
    all_to_all x1, starting transfers between devices, exchange(): return lax.all_to_all(value, axis, split_axis=0, concat_axis=0, tiled=True)  8.6 us
    all_to_all x1, waiting for transfers between devices, exchange(): return lax.all_to_all(value, axis, split_axis=0, concat_axis=0, tiled=True)  6.36 us
    pallas_call x2, Pallas kernels, written(): pl.pallas_call(functools.partial(write_kernel, first), out_shape=(jax.Sha...  5.71 us
    ppermute x8, waiting for transfers between devices, shifted(): lax.ppermute(value, axis, [(i, (i + step) % size) for i in range(size)])  5.2 us
    unnamed x18, local copies, waits for them, and re-layouts  3.09 us
    pallas_call x1, Pallas kernels, per_device(): pl.pallas_call(project_kernel, out_shape=jax.ShapeDtypeStruct((batch, pro...  2.4 us
  transfers between devices with their start and end apart: 9, of which 6 were waited for; matrix products, arithmetic and copies ran while one was open for 0% of the time, Pallas kernels for 9%

profile of v3, /device:TPU:1, one launch (start us, length us, event | category | flops | bytes accessed | tf_op | source)
XLA Modules:
  0.0 86.5 jit_solution(17224114617653059522)
XLA Ops:
  0.6 2.4 %project.1 = bf16[128,1664]{1,0:T(8,128)(2,1)} custom-call(bf16[128,256]{1,0:T(8,128)(2,1)} %tok.1, f32[1,256]{1,0:T(1,128)} %bitcast.24, bf16[256,256]{1,0:T(8,128)(2,1)} %w_query.1, bf16[256,256]{1,0:T(8,128)(2,1)} %w_key.1, bf16[256,512]{1,0:T(8,128)(2,1)} %w_value.1, bf16[256,512]{1,0:T(8,128)(2,1)} %w_outgate.1, bf16[16,4096]{1,0:T(8,128)(2,1)} %bitcast.23), custom_call_target="tpu_custom_call" | custom-call | flops 100663296 | bytes 786432 | tf_op jit(solution)/shard_map/project/pallas_call | solution.py:261
  3.1 8.6 %all-to-all-start = ((bf16[16,8,1664]{2,1,0:T(8,128)(2,1)}), bf16[16,8,1664]{2,1,0:T(8,128)(2,1)S(1)}, u32[]{:S(2)}, u32[]{:S(2)}) async-start(bf16[16,8,1664]{2,1,0:T(8,128)(2,1)} %bitcast.22), calls=%async_computation | async-start | bytes 851968 | tf_op jit(solution)/shard_map/all_to_all | solution.py:51
  11.7 0.9 %copy-done.3 = bf16[512,256]{1,0:T(8,128)(2,1)S(1)} copy-done((bf16[512,256]{1,0:T(8,128)(2,1)S(1)}, bf16[512,256]{1,0:T(8,128)(2,1)}, u32[]{:S(2)}) %copy-start.3) | copy-done | bytes 262168
  12.6 2.3 %shorten_state.1 = (bf16[8,512,256]{2,1,0:T(8,128)(2,1)S(1)}, bf16[512,256]{1,0:T(8,128)(2,1)S(1)}) custom-call(f32[8,1,512,256]{3,2,1,0:T(8,128)} %state.5, bf16[512,256]{1,0:T(8,128)(2,1)S(1)} %copy-done.3), custom_call_target="tpu_custom_call" | custom-call | flops 1000000000 | bytes 6291456 | tf_op jit(solution)/shard_map/shorten_state/pallas_call | solution.py:277
  14.9 6.4 %all-to-all-done.arrived = bf16[16,8,1664]{2,1,0:T(8,128)(2,1)S(1)} async-done(((bf16[16,8,1664]{2,1,0:T(8,128)(2,1)}), bf16[16,8,1664]{2,1,0:T(8,128)(2,1)S(1)}, u32[]{:S(2)}, u32[]{:S(2)}) %all-to-all-start) | async-done | bytes 426016 | tf_op jit(solution)/shard_map/all_to_all | solution.py:51
  21.2 0.8 copy-done.5
  22.1 0.7 copy-done.7
  23.4 1.6 %cell.1 = (bf16[16,8,512]{2,1,0:T(8,128)(2,1)S(1)}, f32[8,384]{1,0:T(8,128)S(1)}, f32[8,512]{1,0:T(8,128)S(1)}, f32[8,1,256]{2,1,0:T(1,128)}, f32[1,8]{1,0:T(1,128)}) custom-call(bf16[16,8,1664]{2,1,0:T(8,128)(2,1)S(1)} %all-to-all-done.arrived, bf16[8,512,256]{2,1,0:T(8,128)(2,1)S(1)} %get-tuple-element.16.state_short, f32[8,1,256]{2,1,0:T(1,128)S(1)} %copy-done.5, ...), custom_call_target="tpu_custom_call" | custom-call | flops 100000000 | bytes 4194304 | tf_op jit(solution)/shard_map/cell/pallas_call | solution.py:294
  24.9 9.8 %all_to_all.20 = bf16[16,8,512]{2,1,0:T(8,128)(2,1)S(1)} all-to-all(bf16[16,8,512]{2,1,0:T(8,128)(2,1)S(1)} %get-tuple-element.17), channel_id=1, replica_groups=mesh['z'=4,'y'=4,'x'=4,'core'=2] {'z','y'}, dimensions={0} | all-to-all | bytes 262144 | tf_op jit(solution)/shard_map/all_to_all | solution.py:51
  34.9 3.0 %collective-permute-start = (bf16[128,256]{1,0:T(8,128)(2,1)S(1)}, bf16[128,256]{1,0:T(8,128)(2,1)S(1)}, u32[]{:S(2)}, u32[]{:S(2)}) collective-permute-start(bf16[128,256]{1,0:T(8,128)(2,1)S(1)} %convolution_convert_fusion.1), channel_id=1, source_target_pairs={{0,1},{1,0},{2,3},{3,2},{4,5},{5,4},{6,7},{7,6},{8,9},{9,8},{10,11... | collective-permute-start | bytes 196616 | tf_op jit(solution)/shard_map/ppermute | solution.py:61
  37.9 0.9 %collective-permute-done = bf16[128,256]{1,0:T(8,128)(2,1)S(1)} collective-permute-done((bf16[128,256]{1,0:T(8,128)(2,1)S(1)}, bf16[128,256]{1,0:T(8,128)(2,1)S(1)}, u32[]{:S(2)}, u32[]{:S(2)}) %collective-permute-start) | collective-permute-done | bytes 65568 | tf_op jit(solution)/shard_map/ppermute | solution.py:61
  38.8 2.5 %collective-permute-start.3 = (bf16[128,256]{1,0:T(8,128)(2,1)S(1)}, bf16[128,256]{1,0:T(8,128)(2,1)S(1)}, u32[]{:S(2)}, u32[]{:S(2)}) collective-permute-start(bf16[128,256]{1,0:T(8,128)(2,1)S(1)} %add_convert_fusion.2.term_0), channel_id=1, source_target_pairs={{0,6},{2,0},{4,2},{6,4},{1,7},{3,1},{5,3},{7,5},{8,14},{10,8},{12,... | collective-permute-start | bytes 196616 | tf_op jit(solution)/shard_map/ppermute | solution.py:61
  42.5 2.6 %write_state.2 = (f32[8,1,512,256]{3,2,1,0:T(8,128)}, f32[8,128]{1,0:T(8,128)S(1)}) custom-call(f32[8,384]{1,0:T(8,128)S(1)} %get-tuple-element.19.to_write, f32[8,512]{1,0:T(8,128)S(1)} %get-tuple-element.20.value, f32[8,1,512,256]{3,2,1,0:T(8,128)} %state.5), custom_call_target="tpu_custom_call" | custom-call | flops 1000000000 | bytes 4194304 | tf_op jit(solution)/shard_map/write_state/pallas_call | solution.py:312
  45.1 1.0 %collective-permute-done.2.term_2 = bf16[128,256]{1,0:T(8,128)(2,1)S(1)} collective-permute-done((bf16[128,256]{1,0:T(8,128)(2,1)S(1)}, bf16[128,256]{1,0:T(8,128)(2,1)S(1)}, u32[]{:S(2)}, u32[]{:S(2)}) %collective-permute-start.2) | collective-permute-done | bytes 65568 | tf_op jit(solution)/shard_map/ppermute | solution.py:61
  46.1 1.7 %collective-permute-done.1.term_1 = bf16[128,256]{1,0:T(8,128)(2,1)S(1)} collective-permute-done((bf16[128,256]{1,0:T(8,128)(2,1)S(1)}, bf16[128,256]{1,0:T(8,128)(2,1)S(1)}, u32[]{:S(2)}, u32[]{:S(2)}) %collective-permute-start.1) | collective-permute-done | bytes 65568 | tf_op jit(solution)/shard_map/ppermute | solution.py:61
  48.4 15.0 %all_to_all.21 = bf16[16,8,2816]{2,1,0:T(8,128)(2,1)S(1)} all-to-all(bf16[16,8,2816]{2,1,0:T(8,128)(2,1)S(1)} %bitcast.17), channel_id=1, replica_groups=mesh['z'=4,'y'=4,'x'=4,'core'=2] {'z','y'}, dimensions={0} | all-to-all | bytes 1441792 | tf_op jit(solution)/shard_map/all_to_all | solution.py:51
  63.8 11.1 %all_to_all.22 = bf16[16,8,1376]{2,1,0:T(8,128)(2,1)S(1)} all-to-all(bf16[16,8,1376]{2,1,0:T(8,128)(2,1)S(1)} %broadcast_in_dim.3), channel_id=1, replica_groups=mesh['z'=4,'y'=4,'x'=4,'core'=2] {'z','y'}, dimensions={0} | all-to-all | bytes 704512 | tf_op jit(solution)/shard_map/all_to_all | solution.py:51
  75.1 3.6 %collective-permute-start.4 = (bf16[128,256]{1,0:T(8,128)(2,1)S(1)}, bf16[128,256]{1,0:T(8,128)(2,1)S(1)}, u32[]{:S(2)}, u32[]{:S(2)}) collective-permute-start(bf16[128,256]{1,0:T(8,128)(2,1)S(1)} %convolution_convert_fusion), channel_id=1, source_target_pairs={{0,1},{1,0},{2,3},{3,2},{4,5},{5,4},{6,7},{7,6},{8,9},{9,8},{10,11... | collective-permute-start | bytes 196616 | tf_op jit(solution)/shard_map/ppermute | solution.py:61
  78.8 0.9 %collective-permute-done.4 = bf16[128,256]{1,0:T(8,128)(2,1)S(1)} collective-permute-done((bf16[128,256]{1,0:T(8,128)(2,1)S(1)}, bf16[128,256]{1,0:T(8,128)(2,1)S(1)}, u32[]{:S(2)}, u32[]{:S(2)}) %collective-permute-start.4) | collective-permute-done | bytes 65568 | tf_op jit(solution)/shard_map/ppermute | solution.py:61
  79.8 1.5 %collective-permute-start.6 = (bf16[128,256]{1,0:T(8,128)(2,1)S(1)}, bf16[128,256]{1,0:T(8,128)(2,1)S(1)}, u32[]{:S(2)}, u32[]{:S(2)}) collective-permute-start(bf16[128,256]{1,0:T(8,128)(2,1)S(1)} %add_convert_fusion.1), channel_id=1, source_target_pairs={{0,2},{2,4},{4,6},{6,0},{1,3},{3,5},{5,7},{7,1},{8,10},{10,12},{12... | collective-permute-start | bytes 196616 | tf_op jit(solution)/shard_map/ppermute | solution.py:61
  81.2 0.7 collective-permute-start.5
  81.9 3.1 %write_state.3 = (f32[8,1,512,256]{3,2,1,0:T(8,128)}, f32[8,128]{1,0:T(8,128)}) custom-call(f32[8,384]{1,0:T(8,128)S(1)} %get-tuple-element.19.to_write, f32[8,512]{1,0:T(8,128)S(1)} %get-tuple-element.20.value, f32[8,1,512,256]{3,2,1,0:T(8,128)} %state.5, f32[8,1,512,256]{3,2,1,0:T(8,128)} %get-tuple-element.24.refs_0_), custom_call_target="tpu_custom_call", output_to_operand_aliasing={{0}: (3, {})} | custom-call | flops 1000000000 | bytes 4194304 | tf_op jit(solution)/shard_map/write_state/pallas_call | solution.py:312
  85.1 0.7 collective-permute-done.5
  85.8 0.7 add_convert_fusion
  (30 shorter events, 3.4 us)
Async XLA Ops:
  0.6 74.2 %copy-start = (bf16[1376,256]{1,0:T(8,128)(2,1)S(1)}, bf16[1376,256]{1,0:T(8,128)(2,1)}, u32[]{:S(2)}) copy-start(bf16[1376,256]{1,0:T(8,128)(2,1)} %param.31) | copy-start | bytes 2113540
  3.1 18.2 %all-to-all-start = ((bf16[16,8,1664]{2,1,0:T(8,128)(2,1)}), bf16[16,8,1664]{2,1,0:T(8,128)(2,1)S(1)}, u32[]{:S(2)}, u32[]{:S(2)}) async-start(bf16[16,8,1664]{2,1,0:T(8,128)(2,1)} %bitcast.22), calls=%async_computation | async-start | bytes 851968 | tf_op jit(solution)/shard_map/all_to_all | solution.py:51
  11.7 1.0 %copy-start.3 = (bf16[512,256]{1,0:T(8,128)(2,1)S(1)}, bf16[512,256]{1,0:T(8,128)(2,1)}, u32[]{:S(2)}) copy-start(bf16[512,256]{1,0:T(8,128)(2,1)} %weight.1) | copy-start | bytes 786436
  14.9 32.9 %copy-start.4 = (bf16[128,256]{1,0:T(8,128)(2,1)S(1)}, bf16[128,256]{1,0:T(8,128)(2,1)}, u32[]{:S(2)}) copy-start(bf16[128,256]{1,0:T(8,128)(2,1)} %tok.1) | copy-start | bytes 196612
  21.2 26.5 %copy-start.1 = (bf16[256,1376]{0,1:T(8,128)(2,1)S(1)}, bf16[256,1376]{0,1:T(8,128)(2,1)}, u32[]{:S(2)}) copy-start(bf16[256,1376]{0,1:T(8,128)(2,1)} %param.29) | copy-start | bytes 2113540
  21.2 26.5 %copy-start.2 = (bf16[256,1376]{0,1:T(8,128)(2,1)S(1)}, bf16[256,1376]{0,1:T(8,128)(2,1)}, u32[]{:S(2)}) copy-start(bf16[256,1376]{0,1:T(8,128)(2,1)} %param.30) | copy-start | bytes 2113540
  21.2 0.8 copy-start.5
  22.1 0.7 copy-start.7
  22.7 0.7 copy-start.8
  23.4 24.4 %copy-start.6 = (f32[256]{0:T(256)S(1)}, f32[256]{0:T(256)}, u32[]{:S(2)}) copy-start(f32[256]{0:T(256)} %param.28) | copy-start | bytes 3076
  34.9 3.9 %collective-permute-start = (bf16[128,256]{1,0:T(8,128)(2,1)S(1)}, bf16[128,256]{1,0:T(8,128)(2,1)S(1)}, u32[]{:S(2)}, u32[]{:S(2)}) collective-permute-start(bf16[128,256]{1,0:T(8,128)(2,1)S(1)} %convolution_convert_fusion.1), channel_id=1, source_target_pairs={{0,1},{1,0},{2,3},{3,2},{4,5},{5,4},{6,7},{7,6},{8,9},{9,8},{10,11... | collective-permute-start | bytes 196616 | tf_op jit(solution)/shard_map/ppermute | solution.py:61
  38.8 6.2 %collective-permute-start.3 = (bf16[128,256]{1,0:T(8,128)(2,1)S(1)}, bf16[128,256]{1,0:T(8,128)(2,1)S(1)}, u32[]{:S(2)}, u32[]{:S(2)}) collective-permute-start(bf16[128,256]{1,0:T(8,128)(2,1)S(1)} %add_convert_fusion.2.term_0), channel_id=1, source_target_pairs={{0,6},{2,0},{4,2},{6,4},{1,7},{3,1},{5,3},{7,5},{8,14},{10,8},{12,... | collective-permute-start | bytes 196616 | tf_op jit(solution)/shard_map/ppermute | solution.py:61
  41.4 4.7 %collective-permute-start.2 = (bf16[128,256]{1,0:T(8,128)(2,1)S(1)}, bf16[128,256]{1,0:T(8,128)(2,1)S(1)}, u32[]{:S(2)}, u32[]{:S(2)}) collective-permute-start(bf16[128,256]{1,0:T(8,128)(2,1)S(1)} %add_convert_fusion.2.term_0), channel_id=1, source_target_pairs={{0,4},{2,6},{4,0},{6,2},{1,5},{3,7},{5,1},{7,3},{8,12},{10,14},{12... | collective-permute-start | bytes 196616 | tf_op jit(solution)/shard_map/ppermute | solution.py:61
  41.9 5.9 %collective-permute-start.1 = (bf16[128,256]{1,0:T(8,128)(2,1)S(1)}, bf16[128,256]{1,0:T(8,128)(2,1)S(1)}, u32[]{:S(2)}, u32[]{:S(2)}) collective-permute-start(bf16[128,256]{1,0:T(8,128)(2,1)S(1)} %add_convert_fusion.2.term_0), channel_id=1, source_target_pairs={{0,2},{2,4},{4,6},{6,0},{1,3},{3,5},{5,7},{7,1},{8,10},{10,12},{12... | collective-permute-start | bytes 196616 | tf_op jit(solution)/shard_map/ppermute | solution.py:61
  75.1 4.5 %collective-permute-start.4 = (bf16[128,256]{1,0:T(8,128)(2,1)S(1)}, bf16[128,256]{1,0:T(8,128)(2,1)S(1)}, u32[]{:S(2)}, u32[]{:S(2)}) collective-permute-start(bf16[128,256]{1,0:T(8,128)(2,1)S(1)} %convolution_convert_fusion), channel_id=1, source_target_pairs={{0,1},{1,0},{2,3},{3,2},{4,5},{5,4},{6,7},{7,6},{8,9},{9,8},{10,11... | collective-permute-start | bytes 196616 | tf_op jit(solution)/shard_map/ppermute | solution.py:61
  79.7 5.4 %collective-permute-start.7 = (bf16[128,256]{1,0:T(8,128)(2,1)S(1)}, bf16[128,256]{1,0:T(8,128)(2,1)S(1)}, u32[]{:S(2)}, u32[]{:S(2)}) collective-permute-start(bf16[128,256]{1,0:T(8,128)(2,1)S(1)} %add_convert_fusion.1), channel_id=1, source_target_pairs={{0,6},{2,0},{4,2},{6,4},{1,7},{3,1},{5,3},{7,5},{8,14},{10,8},{12,... | collective-permute-start | bytes 196616 | tf_op jit(solution)/shard_map/ppermute | solution.py:61
  79.8 5.4 %collective-permute-start.6 = (bf16[128,256]{1,0:T(8,128)(2,1)S(1)}, bf16[128,256]{1,0:T(8,128)(2,1)S(1)}, u32[]{:S(2)}, u32[]{:S(2)}) collective-permute-start(bf16[128,256]{1,0:T(8,128)(2,1)S(1)} %add_convert_fusion.1), channel_id=1, source_target_pairs={{0,2},{2,4},{4,6},{6,0},{1,3},{3,5},{5,7},{7,1},{8,10},{10,12},{12... | collective-permute-start | bytes 196616 | tf_op jit(solution)/shard_map/ppermute | solution.py:61
  81.2 4.6 %collective-permute-start.5 = (bf16[128,256]{1,0:T(8,128)(2,1)S(1)}, bf16[128,256]{1,0:T(8,128)(2,1)S(1)}, u32[]{:S(2)}, u32[]{:S(2)}) collective-permute-start(bf16[128,256]{1,0:T(8,128)(2,1)S(1)} %add_convert_fusion.1), channel_id=1, source_target_pairs={{0,4},{2,6},{4,0},{6,2},{1,5},{3,7},{5,1},{7,3},{8,12},{10,14},{12... | collective-permute-start | bytes 196616 | tf_op jit(solution)/shard_map/ppermute | solution.py:61

commit v4 on v3

--- a/solution.py
+++ b/solution.py
@@ -7,12 +7,12 @@
 from jax.experimental.pallas import tpu as pltpu
 from jax.sharding import Mesh, PartitionSpec as P
 
+
 norm_floor = 1e-05
 lanes = 128
 kv = ("z", "y")
 tp = ("x", "core")
 vmem = pl.BlockSpec(memory_space=pltpu.VMEM)
-smem = pl.BlockSpec(memory_space=pltpu.SMEM)
 hbm = pl.BlockSpec(memory_space=pltpu.HBM)
 low_at = 32
 nt_dims = (((1,), (1,)), ((), ()))
@@ -65,7 +65,10 @@
     mine = part.astype(jnp.bfloat16)
     theirs = shifted(mine, "core", 1)
     pair = (mine.astype(jnp.float32) + theirs.astype(jnp.float32)).astype(jnp.bfloat16)
-    return [pair] + [shifted(pair, "x", step) for step in range(1, lax.axis_size("x"))]
+    terms = [pair]
+    for step in range(1, lax.axis_size("x")):
+        terms.append(shifted(pair, "x", step))
+    return terms
 
 
 def in_order(terms):
@@ -113,25 +116,36 @@
     )
 
 
-def shorten_kernel(state, weight, short, near, held, sems):
-    count = held.shape[0]
-    copies = [pltpu.make_async_copy(state.at[b, 0], held.at[b], sems.at[b]) for b in range(count)]
-    copies.append(pltpu.make_async_copy(weight, near, sems.at[count]))
+def near_kernel(
+    state, n_in, m_in, bias_in, short, packed, held, state_n, state_m, bias, sems
+):
+    rows, _, query_size = held.shape
+    moves = [(state.at[b, 0], held.at[b]) for b in range(rows)]
+    moves += [(n_in, state_n), (m_in, state_m), (bias_in, bias)]
+    copies = [pltpu.make_async_copy(*move, sems.at[i]) for i, move in enumerate(moves)]
     for copy in copies:
         copy.start()
-    for b in range(count):
+    for copy in copies[rows:]:
+        copy.wait()
+    square = (rows, rows)
+    diagonal = row_ids(square) == lane_ids(square)
+    old_m = jnp.where(diagonal, jnp.broadcast_to(state_m[...], square), 0.0)
+    old_m = jnp.sum(old_m, axis=1, keepdims=True)
+    mine = lane_ids(bias.shape) == index_of(tp)
+    bias_here = jnp.sum(jnp.where(mine, bias[...], 0.0), axis=1, keepdims=True)
+    packed[:, :query_size] = state_n[...].reshape(rows, query_size)
+    packed[:, query_size:] = jnp.where(lane_ids((rows, lanes)) == 0, old_m, bias_here)
+    for b in range(rows):
         copies[b].wait()
         short[b] = held[b].astype(jnp.bfloat16)
-    copies[count].wait()
 
 
 def cell_kernel(
-    width_all, arrived, state_short, state_n, state_m, bias, sent, to_write, value_out, new_n, new_m
+    width_all, heads, arrived, state_short, packed, sent, to_write, value_out
 ):
     rows = arrived.shape[1]
     value_size, query_size = state_short.shape[1:]
     proj_width = 2 * query_size + 2 * value_size
-    heads = bias.shape[0]
     total = arrived[0].astype(jnp.float32)
     for i in range(1, arrived.shape[0]):
         total = total + arrived[i].astype(jnp.float32)
@@ -145,11 +159,9 @@
     head = index_of(tp)
     scale = lax.rsqrt(column(2 * heads) / width_all + norm_floor)
     log_input = column(head) * scale
-    forget_pre = column(heads + head) * scale + bias[head]
+    old_m = packed[:, query_size : query_size + 1]
+    forget_pre = column(heads + head) * scale + packed[:, query_size + 1 : query_size + 2]
     log_forget = jnp.minimum(forget_pre, 0.0) - jnp.log(1.0 + jnp.exp(-jnp.abs(forget_pre)))
-    square = (rows, rows)
-    diagonal = row_ids(square) == lane_ids(square)
-    old_m = jnp.sum(jnp.where(diagonal, jnp.broadcast_to(state_m[...], square), 0.0), axis=1, keepdims=True)
     carried = log_forget + old_m
     top = jnp.maximum(carried, log_input)
     keep = jnp.exp(carried - top)
@@ -158,7 +170,7 @@
     key_in = total[:, query_size : 2 * query_size] * (scale * admit)
     value = total[:, 2 * query_size : 2 * query_size + value_size] * scale
     out_pre = total[:, 2 * query_size + value_size : proj_width] * scale
-    later_n = keep * state_n[...].reshape(rows, query_size) + key_in
+    later_n = keep * packed[:, :query_size] + key_in
     normalizer = jnp.sum(later_n * query, axis=1, keepdims=True)
     denom = jnp.maximum(jnp.abs(normalizer), jnp.exp(-top))
     match = jnp.sum(key_in * query, axis=1, keepdims=True)
@@ -174,17 +186,28 @@
     short = head_out.astype(jnp.bfloat16)
     for i in range(sent.shape[0]):
         sent[i] = short
-    to_write[:, :lanes] = jnp.broadcast_to(keep, (rows, lanes))
-    to_write[:, lanes:] = key_in
+    lane = lane_ids((rows, lanes))
+    to_write[:, :lanes] = jnp.where(lane == 0, keep, top)
+    to_write[:, lanes : lanes + query_size] = key_in
+    to_write[:, lanes + query_size :] = later_n
     value_out[...] = value
-    new_n[...] = later_n.reshape(new_n.shape)
-    new_m[...] = jnp.sum(jnp.where(diagonal, jnp.broadcast_to(top, square), 0.0), axis=0, keepdims=True)
 
 
 def write_kernel(first, to_write, value, state, *refs):
-    new_c, order, held, sems_in, sems_out = refs[-5:]
-    order[...] = jnp.zeros_like(order)
-    count = held.shape[0]
+    outputs, held, sems_in, sems_out = refs[:-3], *refs[-3:]
+    count, _, query_size = held.shape
+    if first == 0:
+        new_c, order = outputs
+        order[...] = jnp.zeros_like(order)
+    else:
+        _, new_c, new_n, new_m = outputs
+        new_n[...] = to_write[:, lanes + query_size :].reshape(new_n.shape)
+        rows = to_write.shape[0]
+        square = (rows, rows)
+        top = jnp.broadcast_to(to_write[:, 1:2], square)
+        new_m[...] = jnp.sum(
+            jnp.where(row_ids(square) == lane_ids(square), top, 0.0), axis=0, keepdims=True
+        )
     into = [
         pltpu.make_async_copy(state.at[first + b, 0], held.at[b], sems_in.at[b])
         for b in range(count)
@@ -200,7 +223,7 @@
         row = first + b
         down = across[:, row : row + 1]
         keep = to_write[row : row + 1, :1]
-        key_in = to_write[row : row + 1, lanes:]
+        key_in = to_write[row : row + 1, lanes : lanes + query_size]
         into[b].wait()
         held[b] = keep * held[b] + down * key_in
         out[b].start()
@@ -274,49 +297,52 @@
         cost_estimate=cost(2 * batch * width_dev * proj_width, 2 * width_dev * proj_width),
         name="project",
     )(tokens, attn_gain.reshape(1, width_dev), w_query, w_key, w_value, w_outgate, w_gates.T)
-    state_short, w_output_near = pl.pallas_call(
-        shorten_kernel,
+    state_short, packed = pl.pallas_call(
+        near_kernel,
         out_shape=(
             jax.ShapeDtypeStruct((rows, value_size, query_size), bf16),
-            jax.ShapeDtypeStruct(w_output.shape, w_output.dtype),
+            jax.ShapeDtypeStruct((rows, query_size + lanes), f32),
         ),
-        in_specs=[hbm, hbm],
-        out_specs=(vmem, vmem),
+        in_specs=[hbm] * 4,
+        out_specs=[vmem] * 2,
         scratch_shapes=[
             pltpu.VMEM((rows, value_size, query_size), f32),
-            pltpu.SemaphoreType.DMA((rows + 1,)),
+            pltpu.VMEM(state_n.shape, f32),
+            pltpu.VMEM((1, rows), f32),
+            pltpu.VMEM((1, heads_all), f32),
+            pltpu.SemaphoreType.DMA((rows + 3,)),
         ],
         compiler_params=params(49),
         cost_estimate=cost(10**9, 6 * rows * value_size * query_size),
-        name="shorten_state",
-    )(state_c, w_output)
+        name="near",
+    )(
+        state_c,
+        state_n,
+        state_m.reshape(1, rows),
+        forget_bias.reshape(1, heads_all),
+    )
     arrived = exchange(sent.reshape(kv_count, rows, proj_width + lanes), kv)
-    head_copies, to_write, value, new_n, new_m = pl.pallas_call(
-        functools.partial(cell_kernel, width_all),
+    head_copies, to_write, value = pl.pallas_call(
+        functools.partial(cell_kernel, width_all, heads_all),
         out_shape=(
             jax.ShapeDtypeStruct((kv_count, rows, value_size), bf16),
-            jax.ShapeDtypeStruct((rows, lanes + query_size), f32),
+            jax.ShapeDtypeStruct((rows, lanes + 2 * query_size), f32),
             jax.ShapeDtypeStruct((rows, value_size), f32),
-            jax.ShapeDtypeStruct((rows, 1, query_size), f32),
-            jax.ShapeDtypeStruct((1, rows), f32),
         ),
-        in_specs=[vmem] * 4 + [smem],
-        out_specs=[vmem] * 5,
+        in_specs=[vmem] * 3,
+        out_specs=[vmem] * 3,
         compiler_params=params(8),
         cost_estimate=cost(10**8, 4 * rows * value_size * query_size),
         name="cell",
-    )(arrived, state_short, state_n, state_m.reshape(1, rows), forget_bias)
+    )(arrived, state_short, packed)
     half_rows = rows // 2
 
-    def written(first, *begun):
+    def written(first, extra, *begun):
         return pl.pallas_call(
             functools.partial(write_kernel, first),
-            out_shape=(
-                jax.ShapeDtypeStruct(state_c.shape, f32),
-                jax.ShapeDtypeStruct((8, lanes), f32),
-            ),
+            out_shape=(jax.ShapeDtypeStruct(state_c.shape, f32), *extra),
             in_specs=[vmem, vmem, hbm] + [hbm] * len(begun),
-            out_specs=(hbm, vmem),
+            out_specs=(hbm,) + (vmem,) * len(extra),
             input_output_aliases={3: 0} if begun else {},
             scratch_shapes=[
                 pltpu.VMEM((half_rows, value_size, query_size), f32),
@@ -328,10 +354,14 @@
             name="write_state",
         )(to_write, value, state_c, *begun)
 
-    begun_c, order = written(0)
-    new_c, _ = written(half_rows, begun_c)
+    begun_c, order = written(0, (jax.ShapeDtypeStruct((8, lanes), f32),))
+    new_c, new_n, new_m = written(
+        half_rows,
+        (jax.ShapeDtypeStruct(state_n.shape, f32), jax.ShapeDtypeStruct((1, rows), f32)),
+        begun_c,
+    )
     heads_rows = exchange(head_copies, kv).reshape(batch, value_size)
-    attn_part = jnp.dot(heads_rows, w_output_near, preferred_element_type=f32)
+    attn_part = jnp.dot(heads_rows, w_output, preferred_element_type=f32)
     hidden_dev = w_gateff.shape[1]
     hidden_pad = -(-(hidden_dev + 2) // lanes) * lanes
     sent, middle = pl.pallas_call(

time: 87.7 us -> 85.7 us (0.977)
  waiting for transfers between devices: 11.6 us -> 10.4 us
  local copies, waits for them, and re-layouts: 3.12 us -> 2.06 us
  matrix products: 0.46 us -> 1.41 us
    all_to_all x1, waiting for transfers between devices: 6.36 us -> 5.27 us  [exchange(): return lax.all_to_all(value, axis, split_axis=0, concat_axis=0, tiled=True)]
    unnamed x18 -> x16, local copies, waits for them, and re-layouts: 3.09 us -> 2.03 us
    dot_general x1, matrix products: 0.19 us -> 1.14 us  [per_device(): attn_part = jnp.dot(heads_rows, w_output, preferred_element_type=f32)]
where the time goes in v4:
time: 85.7 us; the launch traced here: 84.5 us
  blocking collectives  35.8 us (42%)
  starting transfers between devices  21.2 us (25%)
  Pallas kernels  11.7 us (14%)
  waiting for transfers between devices  10.4 us (12%)
  local copies, waits for them, and re-layouts  2.06 us (2%)
  matrix products  1.41 us (2%)
  other arithmetic  1.1 us (1%)
    all_to_all x3, blocking collectives, exchange(): return lax.all_to_all(value, axis, split_axis=0, concat_axis=0, tiled=True)  35.8 us
    ppermute x8, starting transfers between devices, shifted(): lax.ppermute(value, axis, [(i, (i + step) % size) for i in range(size)])  12.6 us
    all_to_all x1, starting transfers between devices, exchange(): return lax.all_to_all(value, axis, split_axis=0, concat_axis=0, tiled=True)  8.6 us
    pallas_call x2, Pallas kernels, written(): pl.pallas_call(functools.partial(write_kernel, first), out_shape=(jax.Sha...  5.72 us
    all_to_all x1, waiting for transfers between devices, exchange(): return lax.all_to_all(value, axis, split_axis=0, concat_axis=0, tiled=True)  5.27 us
    ppermute x8, waiting for transfers between devices, shifted(): lax.ppermute(value, axis, [(i, (i + step) % size) for i in range(size)])  5.18 us
    pallas_call x1, Pallas kernels, per_device(): pl.pallas_call(project_kernel, out_shape=jax.ShapeDtypeStruct((batch, pro...  2.4 us
    pallas_call x1, Pallas kernels, per_device(): pl.pallas_call(near_kernel, out_shape=(jax.ShapeDtypeStruct((rows, value_...  2.27 us
  transfers between devices with their start and end apart: 9, of which 6 were waited for; matrix products, arithmetic and copies ran while one was open for 0% of the time, Pallas kernels for 9%

profile of v4, /device:TPU:1, one launch (start us, length us, event | category | flops | bytes accessed | tf_op | source)
XLA Modules:
  0.0 84.5 jit_solution(12626547262657800951)
XLA Ops:
  0.6 2.4 %project.1 = bf16[128,1664]{1,0:T(8,128)(2,1)} custom-call(bf16[128,256]{1,0:T(8,128)(2,1)} %tok.1, f32[1,256]{1,0:T(1,128)} %bitcast.26, bf16[256,256]{1,0:T(8,128)(2,1)} %w_query.1, bf16[256,256]{1,0:T(8,128)(2,1)} %w_key.1, bf16[256,512]{1,0:T(8,128)(2,1)} %w_value.1, bf16[256,512]{1,0:T(8,128)(2,1)} %w_outgate.1, bf16[16,4096]{1,0:T(8,128)(2,1)} %bitcast.25), custom_call_target="tpu_custom_call" | custom-call | flops 100663296 | bytes 786432 | tf_op jit(solution)/shard_map/project/pallas_call | solution.py:284
  3.1 8.6 %all-to-all-start = ((bf16[16,8,1664]{2,1,0:T(8,128)(2,1)}), bf16[16,8,1664]{2,1,0:T(8,128)(2,1)S(1)}, u32[]{:S(2)}, u32[]{:S(2)}) async-start(bf16[16,8,1664]{2,1,0:T(8,128)(2,1)} %bitcast.24), calls=%async_computation | async-start | bytes 851968 | tf_op jit(solution)/shard_map/all_to_all | solution.py:51
  11.7 0.7 copy-done.4
  12.4 0.7 copy-done.6
  13.7 2.3 %near.1 = (bf16[8,512,256]{2,1,0:T(8,128)(2,1)S(1)}, f32[8,384]{1,0:T(8,128)S(1)}) custom-call(f32[8,1,512,256]{3,2,1,0:T(8,128)} %state.5, f32[8,1,256]{2,1,0:T(1,128)S(1)} %copy-done.4, f32[1,8]{1,0:T(1,128)S(1)} %bitcast.22, f32[1,8]{1,0:T(1,128)S(1)} %bitcast.23), custom_call_target="tpu_custom_call" | custom-call | flops 1000000000 | bytes 6291456 | tf_op jit(solution)/shard_map/near/pallas_call | solution.py:300
  16.0 5.3 %all-to-all-done.arrived = bf16[16,8,1664]{2,1,0:T(8,128)(2,1)S(1)} async-done(((bf16[16,8,1664]{2,1,0:T(8,128)(2,1)}), bf16[16,8,1664]{2,1,0:T(8,128)(2,1)S(1)}, u32[]{:S(2)}, u32[]{:S(2)}) %all-to-all-start) | async-done | bytes 426016 | tf_op jit(solution)/shard_map/all_to_all | solution.py:51
  21.2 0.7 cell.1
  22.0 9.8 %all_to_all.20 = bf16[16,8,512]{2,1,0:T(8,128)(2,1)S(1)} all-to-all(bf16[16,8,512]{2,1,0:T(8,128)(2,1)S(1)} %get-tuple-element.18), channel_id=1, replica_groups=mesh['z'=4,'y'=4,'x'=4,'core'=2] {'z','y'}, dimensions={0} | all-to-all | bytes 262144 | tf_op jit(solution)/shard_map/all_to_all | solution.py:51
  31.8 1.1 %convolution_convert_fusion.1 = bf16[128,256]{1,0:T(8,128)(2,1)S(1)} fusion(bf16[512,256]{1,0:T(8,128)(2,1)} %param.27, bf16[16,8,512]{2,1,0:T(8,128)(2,1)S(1)} %all_to_all.20), kind=kOutput, calls=%fused_computation.2 | convolution fusion | flops 33587200 | bytes 458752 | tf_op jit(solution)/shard_map/dot_general | solution.py:364
  32.9 3.0 %collective-permute-start = (bf16[128,256]{1,0:T(8,128)(2,1)S(1)}, bf16[128,256]{1,0:T(8,128)(2,1)S(1)}, u32[]{:S(2)}, u32[]{:S(2)}) collective-permute-start(bf16[128,256]{1,0:T(8,128)(2,1)S(1)} %convolution_convert_fusion.1), channel_id=1, source_target_pairs={{0,1},{1,0},{2,3},{3,2},{4,5},{5,4},{6,7},{7,6},{8,9},{9,8},{10,11... | collective-permute-start | bytes 196616 | tf_op jit(solution)/shard_map/ppermute | solution.py:61
  35.9 0.9 %collective-permute-done = bf16[128,256]{1,0:T(8,128)(2,1)S(1)} collective-permute-done((bf16[128,256]{1,0:T(8,128)(2,1)S(1)}, bf16[128,256]{1,0:T(8,128)(2,1)S(1)}, u32[]{:S(2)}, u32[]{:S(2)}) %collective-permute-start) | collective-permute-done | bytes 65568 | tf_op jit(solution)/shard_map/ppermute | solution.py:61
  36.9 2.5 %collective-permute-start.3 = (bf16[128,256]{1,0:T(8,128)(2,1)S(1)}, bf16[128,256]{1,0:T(8,128)(2,1)S(1)}, u32[]{:S(2)}, u32[]{:S(2)}) collective-permute-start(bf16[128,256]{1,0:T(8,128)(2,1)S(1)} %add_convert_fusion.2.term_0), channel_id=1, source_target_pairs={{0,6},{2,0},{4,2},{6,4},{1,7},{3,1},{5,3},{7,5},{8,14},{10,8},{12,... | collective-permute-start | bytes 196616 | tf_op jit(solution)/shard_map/ppermute | solution.py:61
  40.5 2.6 %write_state.2 = (f32[8,1,512,256]{3,2,1,0:T(8,128)}, f32[8,128]{1,0:T(8,128)S(1)}) custom-call(f32[8,640]{1,0:T(8,128)S(1)} %get-tuple-element.19.to_write, f32[8,512]{1,0:T(8,128)S(1)} %get-tuple-element.20.value, f32[8,1,512,256]{3,2,1,0:T(8,128)} %state.5), custom_call_target="tpu_custom_call" | custom-call | flops 1000000000 | bytes 4194304 | tf_op jit(solution)/shard_map/write_state/pallas_call | solution.py:341
  43.1 1.0 %collective-permute-done.2.term_2 = bf16[128,256]{1,0:T(8,128)(2,1)S(1)} collective-permute-done((bf16[128,256]{1,0:T(8,128)(2,1)S(1)}, bf16[128,256]{1,0:T(8,128)(2,1)S(1)}, u32[]{:S(2)}, u32[]{:S(2)}) %collective-permute-start.2) | collective-permute-done | bytes 65568 | tf_op jit(solution)/shard_map/ppermute | solution.py:61
  44.1 1.7 %collective-permute-done.1.term_1 = bf16[128,256]{1,0:T(8,128)(2,1)S(1)} collective-permute-done((bf16[128,256]{1,0:T(8,128)(2,1)S(1)}, bf16[128,256]{1,0:T(8,128)(2,1)S(1)}, u32[]{:S(2)}, u32[]{:S(2)}) %collective-permute-start.1) | collective-permute-done | bytes 65568 | tf_op jit(solution)/shard_map/ppermute | solution.py:61
  46.4 15.0 %all_to_all.21 = bf16[16,8,2816]{2,1,0:T(8,128)(2,1)S(1)} all-to-all(bf16[16,8,2816]{2,1,0:T(8,128)(2,1)S(1)} %bitcast.18), channel_id=1, replica_groups=mesh['z'=4,'y'=4,'x'=4,'core'=2] {'z','y'}, dimensions={0} | all-to-all | bytes 1441792 | tf_op jit(solution)/shard_map/all_to_all | solution.py:51
  61.8 11.1 %all_to_all.22 = bf16[16,8,1376]{2,1,0:T(8,128)(2,1)S(1)} all-to-all(bf16[16,8,1376]{2,1,0:T(8,128)(2,1)S(1)} %broadcast_in_dim.3), channel_id=1, replica_groups=mesh['z'=4,'y'=4,'x'=4,'core'=2] {'z','y'}, dimensions={0} | all-to-all | bytes 704512 | tf_op jit(solution)/shard_map/all_to_all | solution.py:51
  73.1 3.6 %collective-permute-start.4 = (bf16[128,256]{1,0:T(8,128)(2,1)S(1)}, bf16[128,256]{1,0:T(8,128)(2,1)S(1)}, u32[]{:S(2)}, u32[]{:S(2)}) collective-permute-start(bf16[128,256]{1,0:T(8,128)(2,1)S(1)} %convolution_convert_fusion), channel_id=1, source_target_pairs={{0,1},{1,0},{2,3},{3,2},{4,5},{5,4},{6,7},{7,6},{8,9},{9,8},{10,11... | collective-permute-start | bytes 196616 | tf_op jit(solution)/shard_map/ppermute | solution.py:61
  76.8 0.9 %collective-permute-done.4 = bf16[128,256]{1,0:T(8,128)(2,1)S(1)} collective-permute-done((bf16[128,256]{1,0:T(8,128)(2,1)S(1)}, bf16[128,256]{1,0:T(8,128)(2,1)S(1)}, u32[]{:S(2)}, u32[]{:S(2)}) %collective-permute-start.4) | collective-permute-done | bytes 65568 | tf_op jit(solution)/shard_map/ppermute | solution.py:61
  77.8 1.5 %collective-permute-start.6 = (bf16[128,256]{1,0:T(8,128)(2,1)S(1)}, bf16[128,256]{1,0:T(8,128)(2,1)S(1)}, u32[]{:S(2)}, u32[]{:S(2)}) collective-permute-start(bf16[128,256]{1,0:T(8,128)(2,1)S(1)} %add_convert_fusion.1), channel_id=1, source_target_pairs={{0,2},{2,4},{4,6},{6,0},{1,3},{3,5},{5,7},{7,1},{8,10},{10,12},{12... | collective-permute-start | bytes 196616 | tf_op jit(solution)/shard_map/ppermute | solution.py:61
  79.2 0.7 collective-permute-start.5
  80.0 3.2 %write_state.3 = (f32[8,1,512,256]{3,2,1,0:T(8,128)}, f32[8,1,256]{2,1,0:T(1,128)}, f32[1,8]{1,0:T(1,128)}) custom-call(f32[8,640]{1,0:T(8,128)S(1)} %get-tuple-element.19.to_write, f32[8,512]{1,0:T(8,128)S(1)} %get-tuple-element.20.value, f32[8,1,512,256]{3,2,1,0:T(8,128)} %state.5, ...), custom_call_target="tpu_custom_call", output_to_operand_aliasing={{0}: (3, {})} | custom-call | flops 1000000000 | bytes 4194304 | tf_op jit(solution)/shard_map/write_state/pallas_call | solution.py:341
  83.1 0.7 collective-permute-done.5
  83.8 0.7 add_convert_fusion
  (28 shorter events, 3.2 us)
Async XLA Ops:
  0.6 72.2 %copy-start = (bf16[1376,256]{1,0:T(8,128)(2,1)S(1)}, bf16[1376,256]{1,0:T(8,128)(2,1)}, u32[]{:S(2)}) copy-start(bf16[1376,256]{1,0:T(8,128)(2,1)} %param.31) | copy-start | bytes 2113540
  3.1 18.2 %all-to-all-start = ((bf16[16,8,1664]{2,1,0:T(8,128)(2,1)}), bf16[16,8,1664]{2,1,0:T(8,128)(2,1)S(1)}, u32[]{:S(2)}, u32[]{:S(2)}) async-start(bf16[16,8,1664]{2,1,0:T(8,128)(2,1)} %bitcast.24), calls=%async_computation | async-start | bytes 851968 | tf_op jit(solution)/shard_map/all_to_all | solution.py:51
  11.7 0.7 copy-start.4
  12.4 0.7 copy-start.6
  13.0 0.7 copy-start.7
  15.9 29.8 %copy-start.3 = (bf16[128,256]{1,0:T(8,128)(2,1)S(1)}, bf16[128,256]{1,0:T(8,128)(2,1)}, u32[]{:S(2)}) copy-start(bf16[128,256]{1,0:T(8,128)(2,1)} %tok.1) | copy-start | bytes 196612
  16.0 29.8 %copy-start.5 = (f32[256]{0:T(256)S(1)}, f32[256]{0:T(256)}, u32[]{:S(2)}) copy-start(f32[256]{0:T(256)} %param.28) | copy-start | bytes 3076
  21.2 24.5 %copy-start.1 = (bf16[256,1376]{0,1:T(8,128)(2,1)S(1)}, bf16[256,1376]{0,1:T(8,128)(2,1)}, u32[]{:S(2)}) copy-start(bf16[256,1376]{0,1:T(8,128)(2,1)} %param.29) | copy-start | bytes 2113540
  21.2 24.5 %copy-start.2 = (bf16[256,1376]{0,1:T(8,128)(2,1)S(1)}, bf16[256,1376]{0,1:T(8,128)(2,1)}, u32[]{:S(2)}) copy-start(bf16[256,1376]{0,1:T(8,128)(2,1)} %param.30) | copy-start | bytes 2113540
  32.9 3.9 %collective-permute-start = (bf16[128,256]{1,0:T(8,128)(2,1)S(1)}, bf16[128,256]{1,0:T(8,128)(2,1)S(1)}, u32[]{:S(2)}, u32[]{:S(2)}) collective-permute-start(bf16[128,256]{1,0:T(8,128)(2,1)S(1)} %convolution_convert_fusion.1), channel_id=1, source_target_pairs={{0,1},{1,0},{2,3},{3,2},{4,5},{5,4},{6,7},{7,6},{8,9},{9,8},{10,11... | collective-permute-start | bytes 196616 | tf_op jit(solution)/shard_map/ppermute | solution.py:61
  36.9 6.2 %collective-permute-start.3 = (bf16[128,256]{1,0:T(8,128)(2,1)S(1)}, bf16[128,256]{1,0:T(8,128)(2,1)S(1)}, u32[]{:S(2)}, u32[]{:S(2)}) collective-permute-start(bf16[128,256]{1,0:T(8,128)(2,1)S(1)} %add_convert_fusion.2.term_0), channel_id=1, source_target_pairs={{0,6},{2,0},{4,2},{6,4},{1,7},{3,1},{5,3},{7,5},{8,14},{10,8},{12,... | collective-permute-start | bytes 196616 | tf_op jit(solution)/shard_map/ppermute | solution.py:61
  39.4 4.7 %collective-permute-start.2 = (bf16[128,256]{1,0:T(8,128)(2,1)S(1)}, bf16[128,256]{1,0:T(8,128)(2,1)S(1)}, u32[]{:S(2)}, u32[]{:S(2)}) collective-permute-start(bf16[128,256]{1,0:T(8,128)(2,1)S(1)} %add_convert_fusion.2.term_0), channel_id=1, source_target_pairs={{0,4},{2,6},{4,0},{6,2},{1,5},{3,7},{5,1},{7,3},{8,12},{10,14},{12... | collective-permute-start | bytes 196616 | tf_op jit(solution)/shard_map/ppermute | solution.py:61
  39.9 5.9 %collective-permute-start.1 = (bf16[128,256]{1,0:T(8,128)(2,1)S(1)}, bf16[128,256]{1,0:T(8,128)(2,1)S(1)}, u32[]{:S(2)}, u32[]{:S(2)}) collective-permute-start(bf16[128,256]{1,0:T(8,128)(2,1)S(1)} %add_convert_fusion.2.term_0), channel_id=1, source_target_pairs={{0,2},{2,4},{4,6},{6,0},{1,3},{3,5},{5,7},{7,1},{8,10},{10,12},{12... | collective-permute-start | bytes 196616 | tf_op jit(solution)/shard_map/ppermute | solution.py:61
  73.1 4.5 %collective-permute-start.4 = (bf16[128,256]{1,0:T(8,128)(2,1)S(1)}, bf16[128,256]{1,0:T(8,128)(2,1)S(1)}, u32[]{:S(2)}, u32[]{:S(2)}) collective-permute-start(bf16[128,256]{1,0:T(8,128)(2,1)S(1)} %convolution_convert_fusion), channel_id=1, source_target_pairs={{0,1},{1,0},{2,3},{3,2},{4,5},{5,4},{6,7},{7,6},{8,9},{9,8},{10,11... | collective-permute-start | bytes 196616 | tf_op jit(solution)/shard_map/ppermute | solution.py:61
  77.7 5.4 %collective-permute-start.7 = (bf16[128,256]{1,0:T(8,128)(2,1)S(1)}, bf16[128,256]{1,0:T(8,128)(2,1)S(1)}, u32[]{:S(2)}, u32[]{:S(2)}) collective-permute-start(bf16[128,256]{1,0:T(8,128)(2,1)S(1)} %add_convert_fusion.1), channel_id=1, source_target_pairs={{0,6},{2,0},{4,2},{6,4},{1,7},{3,1},{5,3},{7,5},{8,14},{10,8},{12,... | collective-permute-start | bytes 196616 | tf_op jit(solution)/shard_map/ppermute | solution.py:61
  77.8 5.4 %collective-permute-start.6 = (bf16[128,256]{1,0:T(8,128)(2,1)S(1)}, bf16[128,256]{1,0:T(8,128)(2,1)S(1)}, u32[]{:S(2)}, u32[]{:S(2)}) collective-permute-start(bf16[128,256]{1,0:T(8,128)(2,1)S(1)} %add_convert_fusion.1), channel_id=1, source_target_pairs={{0,2},{2,4},{4,6},{6,0},{1,3},{3,5},{5,7},{7,1},{8,10},{10,12},{12... | collective-permute-start | bytes 196616 | tf_op jit(solution)/shard_map/ppermute | solution.py:61
  79.2 4.6 %collective-permute-start.5 = (bf16[128,256]{1,0:T(8,128)(2,1)S(1)}, bf16[128,256]{1,0:T(8,128)(2,1)S(1)}, u32[]{:S(2)}, u32[]{:S(2)}) collective-permute-start(bf16[128,256]{1,0:T(8,128)(2,1)S(1)} %add_convert_fusion.1), channel_id=1, source_target_pairs={{0,4},{2,6},{4,0},{6,2},{1,5},{3,7},{5,1},{7,3},{8,12},{10,14},{12... | collective-permute-start | bytes 196616 | tf_op jit(solution)/shard_map/ppermute | solution.py:61

commit v5 on v4

--- a/solution.py
+++ b/solution.py
@@ -15,6 +15,7 @@
 vmem = pl.BlockSpec(memory_space=pltpu.VMEM)
 hbm = pl.BlockSpec(memory_space=pltpu.HBM)
 low_at = 32
+extra_rows = 16
 nt_dims = (((1,), (1,)), ((), ()))
 
 
@@ -45,6 +46,15 @@
     high = value.astype(jnp.bfloat16)
     low = (value - high.astype(jnp.float32)).astype(jnp.bfloat16)
     return high, low
+
+
+def split_three(value):
+    parts = []
+    for _ in range(3):
+        part = value.astype(jnp.bfloat16).astype(jnp.float32)
+        parts.append(part)
+        value = value - part
+    return parts
 
 
 def exchange(value, axis):
@@ -117,15 +127,15 @@
 
 
 def near_kernel(
-    state, n_in, m_in, bias_in, short, packed, held, state_n, state_m, bias, sems
+    state, weight, n_in, m_in, bias_in, short, near, held, state_n, state_m, bias, sems
 ):
-    rows, _, query_size = held.shape
+    rows, value_size, query_size = held.shape
     moves = [(state.at[b, 0], held.at[b]) for b in range(rows)]
-    moves += [(n_in, state_n), (m_in, state_m), (bias_in, bias)]
+    moves += [(weight, near), (n_in, state_n), (m_in, state_m), (bias_in, bias)]
     copies = [pltpu.make_async_copy(*move, sems.at[i]) for i, move in enumerate(moves)]
     for copy in copies:
         copy.start()
-    for copy in copies[rows:]:
+    for copy in copies[rows + 1 :]:
         copy.wait()
     square = (rows, rows)
     diagonal = row_ids(square) == lane_ids(square)
@@ -133,18 +143,26 @@
     old_m = jnp.sum(old_m, axis=1, keepdims=True)
     mine = lane_ids(bias.shape) == index_of(tp)
     bias_here = jnp.sum(jnp.where(mine, bias[...], 0.0), axis=1, keepdims=True)
-    packed[:, :query_size] = state_n[...].reshape(rows, query_size)
-    packed[:, query_size:] = jnp.where(lane_ids((rows, lanes)) == 0, old_m, bias_here)
+    row = row_ids((extra_rows, query_size))
+    for b in range(rows):
+        block = jnp.zeros((extra_rows, query_size), jnp.float32)
+        for i, source in enumerate((state_n[b], old_m[b : b + 1], bias_here)):
+            for j, part in enumerate(split_three(source)):
+                block = jnp.where(row == 3 * i + j, part, block)
+        short[b, value_size:] = block.astype(jnp.bfloat16)
     for b in range(rows):
         copies[b].wait()
-        short[b] = held[b].astype(jnp.bfloat16)
+        short[b, :value_size] = held[b].astype(jnp.bfloat16)
+    copies[rows].wait()
 
 
 def cell_kernel(
-    width_all, heads, arrived, state_short, packed, sent, to_write, value_out
+    width_all, heads, arrived, state_short, sent, to_write, value_out
 ):
     rows = arrived.shape[1]
-    value_size, query_size = state_short.shape[1:]
+    value_size, query_size = state_short.shape[1] - extra_rows, state_short.shape[2]
+    kept = state_short[:, value_size:, :].astype(jnp.float32)
+    state_n, old_m, bias = (kept[:, i] + kept[:, i + 1] + kept[:, i + 2] for i in (0, 3, 6))
     proj_width = 2 * query_size + 2 * value_size
     total = arrived[0].astype(jnp.float32)
     for i in range(1, arrived.shape[0]):
@@ -159,10 +177,9 @@
     head = index_of(tp)
     scale = lax.rsqrt(column(2 * heads) / width_all + norm_floor)
     log_input = column(head) * scale
-    old_m = packed[:, query_size : query_size + 1]
-    forget_pre = column(heads + head) * scale + packed[:, query_size + 1 : query_size + 2]
+    forget_pre = column(heads + head) * scale + bias[:, :1]
     log_forget = jnp.minimum(forget_pre, 0.0) - jnp.log(1.0 + jnp.exp(-jnp.abs(forget_pre)))
-    carried = log_forget + old_m
+    carried = log_forget + old_m[:, :1]
     top = jnp.maximum(carried, log_input)
     keep = jnp.exp(carried - top)
     admit = jnp.exp(log_input - top)
@@ -170,7 +187,7 @@
     key_in = total[:, query_size : 2 * query_size] * (scale * admit)
     value = total[:, 2 * query_size : 2 * query_size + value_size] * scale
     out_pre = total[:, 2 * query_size + value_size : proj_width] * scale
-    later_n = keep * packed[:, :query_size] + key_in
+    later_n = keep * state_n + key_in
     normalizer = jnp.sum(later_n * query, axis=1, keepdims=True)
     denom = jnp.maximum(jnp.abs(normalizer), jnp.exp(-top))
     match = jnp.sum(key_in * query, axis=1, keepdims=True)
@@ -180,7 +197,7 @@
     reads = jnp.zeros((2 * rows, value_size), jnp.float32)
     for b in range(rows):
         one = jnp.where((row == b) | (row == b + rows), both, 0.0).astype(jnp.bfloat16)
-        reads += lax.dot_general(one, state_short[b], nt_dims, preferred_element_type=jnp.float32)
+        reads += lax.dot_general(one, state_short[b, :value_size], nt_dims, preferred_element_type=jnp.float32)
     numer = keep * (reads[:rows] + reads[rows:]) + match * value
     head_out = numer / ((1.0 + jnp.exp(-out_pre)) * denom)
     short = head_out.astype(jnp.bfloat16)
@@ -293,30 +310,31 @@
             pltpu.VMEM((lanes, width_dev), bf16),
             pltpu.SemaphoreType.DMA((8,)),
         ],
-        compiler_params=params(60),
+        compiler_params=params(63),
         cost_estimate=cost(2 * batch * width_dev * proj_width, 2 * width_dev * proj_width),
         name="project",
     )(tokens, attn_gain.reshape(1, width_dev), w_query, w_key, w_value, w_outgate, w_gates.T)
-    state_short, packed = pl.pallas_call(
+    state_short, w_output_near = pl.pallas_call(
         near_kernel,
         out_shape=(
-            jax.ShapeDtypeStruct((rows, value_size, query_size), bf16),
-            jax.ShapeDtypeStruct((rows, query_size + lanes), f32),
+            jax.ShapeDtypeStruct((rows, value_size + extra_rows, query_size), bf16),
+            jax.ShapeDtypeStruct(w_output.shape, w_output.dtype),
         ),
-        in_specs=[hbm] * 4,
+        in_specs=[hbm] * 5,
         out_specs=[vmem] * 2,
         scratch_shapes=[
             pltpu.VMEM((rows, value_size, query_size), f32),
             pltpu.VMEM(state_n.shape, f32),
             pltpu.VMEM((1, rows), f32),
             pltpu.VMEM((1, heads_all), f32),
-            pltpu.SemaphoreType.DMA((rows + 3,)),
+            pltpu.SemaphoreType.DMA((rows + 4,)),
         ],
         compiler_params=params(49),
         cost_estimate=cost(10**9, 6 * rows * value_size * query_size),
         name="near",
     )(
         state_c,
+        w_output,
         state_n,
         state_m.reshape(1, rows),
         forget_bias.reshape(1, heads_all),
@@ -329,12 +347,12 @@
             jax.ShapeDtypeStruct((rows, lanes + 2 * query_size), f32),
             jax.ShapeDtypeStruct((rows, value_size), f32),
         ),
-        in_specs=[vmem] * 3,
+        in_specs=[vmem] * 2,
         out_specs=[vmem] * 3,
         compiler_params=params(8),
         cost_estimate=cost(10**8, 4 * rows * value_size * query_size),
         name="cell",
-    )(arrived, state_short, packed)
+    )(arrived, state_short)
     half_rows = rows // 2
 
     def written(first, extra, *begun):
@@ -361,7 +379,7 @@
         begun_c,
     )
     heads_rows = exchange(head_copies, kv).reshape(batch, value_size)
-    attn_part = jnp.dot(heads_rows, w_output, preferred_element_type=f32)
+    attn_part = jnp.dot(heads_rows, w_output_near, preferred_element_type=f32)
     hidden_dev = w_gateff.shape[1]
     hidden_pad = -(-(hidden_dev + 2) // lanes) * lanes
     sent, middle = pl.pallas_call(

time: 85.7 us -> 86 us (level)
  Pallas kernels: 11.7 us -> 12.8 us
  matrix products: 1.41 us -> 0.46 us
  local copies, waits for them, and re-layouts: 2.06 us -> 3.01 us
    pallas_call x1, Pallas kernels: 0.72 us -> 1.84 us  [per_device(): pl.pallas_call(functools.partial(cell_kernel, width_all, heads_all), out_...]
    unnamed x16 -> x18, local copies, waits for them, and re-layouts: 2.03 us -> 2.98 us
    dot_general x1, matrix products: 1.14 us -> 0.19 us  [per_device(): attn_part = jnp.dot(heads_rows, w_output_near, preferred_element_type=f32)]
    all_to_all x1, waiting for transfers between devices: 5.27 us -> 4.37 us  [exchange(): return lax.all_to_all(value, axis, split_axis=0, concat_axis=0, tiled=True)]
where the time goes in v5:
time: 86 us; the launch traced here: 84.8 us
  blocking collectives  35.8 us (42%)
  starting transfers between devices  21.2 us (25%)
  Pallas kernels  12.8 us (15%)
  waiting for transfers between devices  9.55 us (11%)
  local copies, waits for them, and re-layouts  3.01 us (4%)
  other arithmetic  1.1 us (1%)
    all_to_all x3, blocking collectives, exchange(): return lax.all_to_all(value, axis, split_axis=0, concat_axis=0, tiled=True)  35.8 us
    ppermute x8, starting transfers between devices, shifted(): lax.ppermute(value, axis, [(i, (i + step) % size) for i in range(size)])  12.6 us
    all_to_all x1, starting transfers between devices, exchange(): return lax.all_to_all(value, axis, split_axis=0, concat_axis=0, tiled=True)  8.64 us
    pallas_call x2, Pallas kernels, written(): pl.pallas_call(functools.partial(write_kernel, first), out_shape=(jax.Sha...  5.72 us
    ppermute x8, waiting for transfers between devices, shifted(): lax.ppermute(value, axis, [(i, (i + step) % size) for i in range(size)])  5.18 us
    all_to_all x1, waiting for transfers between devices, exchange(): return lax.all_to_all(value, axis, split_axis=0, concat_axis=0, tiled=True)  4.37 us
    unnamed x18, local copies, waits for them, and re-layouts  2.98 us
    pallas_call x1, Pallas kernels, per_device(): pl.pallas_call(project_kernel, out_shape=jax.ShapeDtypeStruct((batch, pro...  2.4 us
  transfers between devices with their start and end apart: 9, of which 6 were waited for; matrix products, arithmetic and copies ran while one was open for 0% of the time, Pallas kernels for 9%

profile of v5, /device:TPU:1, one launch (start us, length us, event | category | flops | bytes accessed | tf_op | source)
XLA Modules:
  0.0 84.8 jit_solution(65631259112030961)
XLA Ops:
  0.6 2.4 %project.1 = bf16[128,1664]{1,0:T(8,128)(2,1)} custom-call(bf16[128,256]{1,0:T(8,128)(2,1)} %tok.1, f32[1,256]{1,0:T(1,128)} %bitcast.26, bf16[256,256]{1,0:T(8,128)(2,1)} %w_query.1, bf16[256,256]{1,0:T(8,128)(2,1)} %w_key.1, bf16[256,512]{1,0:T(8,128)(2,1)} %w_value.1, bf16[256,512]{1,0:T(8,128)(2,1)} %w_outgate.1, bf16[16,4096]{1,0:T(8,128)(2,1)} %bitcast.25), custom_call_target="tpu_custom_call" | custom-call | flops 100663296 | bytes 786432 | tf_op jit(solution)/shard_map/project/pallas_call | solution.py:301
  3.1 8.6 %all-to-all-start = ((bf16[16,8,1664]{2,1,0:T(8,128)(2,1)}), bf16[16,8,1664]{2,1,0:T(8,128)(2,1)}, u32[]{:S(2)}, u32[]{:S(2)}) async-start(bf16[16,8,1664]{2,1,0:T(8,128)(2,1)} %bitcast.24), calls=%async_computation | async-start | bytes 851968 | tf_op jit(solution)/shard_map/all_to_all | solution.py:61
  11.7 0.9 %copy-done.3 = bf16[512,256]{1,0:T(8,128)(2,1)S(1)} copy-done((bf16[512,256]{1,0:T(8,128)(2,1)S(1)}, bf16[512,256]{1,0:T(8,128)(2,1)}, u32[]{:S(2)}) %copy-start.3) | copy-done | bytes 262168
  12.7 0.7 copy-done.5
  13.4 0.7 copy-done.7
  14.7 2.3 %near.1 = (bf16[8,528,256]{2,1,0:T(8,128)(2,1)S(1)}, bf16[512,256]{1,0:T(8,128)(2,1)S(1)}) custom-call(f32[8,1,512,256]{3,2,1,0:T(8,128)} %state.5, bf16[512,256]{1,0:T(8,128)(2,1)S(1)} %copy-done.3, f32[8,1,256]{2,1,0:T(1,128)S(1)} %copy-done.5, f32[1,8]{1,0:T(1,128)S(1)} %bitcast.22, f32[1,8]{1,0:T(1,128)S(1)} %bitcast.23), custom_call_target="tpu_custom_call" | custom-call | flops 1000000000 | bytes 6291456 | tf_op jit(solution)/shard_map/near/pallas_call | solution.py:317
  17.0 4.4 %all-to-all-done.arrived = bf16[16,8,1664]{2,1,0:T(8,128)(2,1)} async-done(((bf16[16,8,1664]{2,1,0:T(8,128)(2,1)}), bf16[16,8,1664]{2,1,0:T(8,128)(2,1)}, u32[]{:S(2)}, u32[]{:S(2)}) %all-to-all-start) | async-done | bytes 426016 | tf_op jit(solution)/shard_map/all_to_all | solution.py:61
  21.4 1.8 %cell.1 = (bf16[16,8,512]{2,1,0:T(8,128)(2,1)S(1)}, f32[8,640]{1,0:T(8,128)S(1)}, f32[8,512]{1,0:T(8,128)S(1)}) custom-call(bf16[16,8,1664]{2,1,0:T(8,128)(2,1)} %all-to-all-done.arrived, bf16[8,528,256]{2,1,0:T(8,128)(2,1)S(1)} %get-tuple-element.16.state_short), custom_call_target="tpu_custom_call" | custom-call | flops 100000000 | bytes 4194304 | tf_op jit(solution)/shard_map/cell/pallas_call | solution.py:343
  23.2 9.8 %all_to_all.20 = bf16[16,8,512]{2,1,0:T(8,128)(2,1)S(1)} all-to-all(bf16[16,8,512]{2,1,0:T(8,128)(2,1)S(1)} %get-tuple-element.17), channel_id=1, replica_groups=mesh['z'=4,'y'=4,'x'=4,'core'=2] {'z','y'}, dimensions={0} | all-to-all | bytes 262144 | tf_op jit(solution)/shard_map/all_to_all | solution.py:61
  33.2 3.0 %collective-permute-start = (bf16[128,256]{1,0:T(8,128)(2,1)S(1)}, bf16[128,256]{1,0:T(8,128)(2,1)S(1)}, u32[]{:S(2)}, u32[]{:S(2)}) collective-permute-start(bf16[128,256]{1,0:T(8,128)(2,1)S(1)} %convolution_convert_fusion.1), channel_id=1, source_target_pairs={{0,1},{1,0},{2,3},{3,2},{4,5},{5,4},{6,7},{7,6},{8,9},{9,8},{10,11... | collective-permute-start | bytes 196616 | tf_op jit(solution)/shard_map/ppermute | solution.py:71
  36.2 0.9 %collective-permute-done = bf16[128,256]{1,0:T(8,128)(2,1)S(1)} collective-permute-done((bf16[128,256]{1,0:T(8,128)(2,1)S(1)}, bf16[128,256]{1,0:T(8,128)(2,1)S(1)}, u32[]{:S(2)}, u32[]{:S(2)}) %collective-permute-start) | collective-permute-done | bytes 65568 | tf_op jit(solution)/shard_map/ppermute | solution.py:71
  37.1 2.5 %collective-permute-start.3 = (bf16[128,256]{1,0:T(8,128)(2,1)S(1)}, bf16[128,256]{1,0:T(8,128)(2,1)S(1)}, u32[]{:S(2)}, u32[]{:S(2)}) collective-permute-start(bf16[128,256]{1,0:T(8,128)(2,1)S(1)} %add_convert_fusion.2.term_0), channel_id=1, source_target_pairs={{0,6},{2,0},{4,2},{6,4},{1,7},{3,1},{5,3},{7,5},{8,14},{10,8},{12,... | collective-permute-start | bytes 196616 | tf_op jit(solution)/shard_map/ppermute | solution.py:71
  40.8 2.6 %write_state.2 = (f32[8,1,512,256]{3,2,1,0:T(8,128)}, f32[8,128]{1,0:T(8,128)S(1)}) custom-call(f32[8,640]{1,0:T(8,128)S(1)} %get-tuple-element.19.to_write, f32[8,512]{1,0:T(8,128)S(1)} %get-tuple-element.20.value, f32[8,1,512,256]{3,2,1,0:T(8,128)} %state.5), custom_call_target="tpu_custom_call" | custom-call | flops 1000000000 | bytes 4194304 | tf_op jit(solution)/shard_map/write_state/pallas_call | solution.py:359
  43.4 1.0 %collective-permute-done.2.term_2 = bf16[128,256]{1,0:T(8,128)(2,1)S(1)} collective-permute-done((bf16[128,256]{1,0:T(8,128)(2,1)S(1)}, bf16[128,256]{1,0:T(8,128)(2,1)S(1)}, u32[]{:S(2)}, u32[]{:S(2)}) %collective-permute-start.2) | collective-permute-done | bytes 65568 | tf_op jit(solution)/shard_map/ppermute | solution.py:71
  44.3 1.7 %collective-permute-done.1.term_1 = bf16[128,256]{1,0:T(8,128)(2,1)S(1)} collective-permute-done((bf16[128,256]{1,0:T(8,128)(2,1)S(1)}, bf16[128,256]{1,0:T(8,128)(2,1)S(1)}, u32[]{:S(2)}, u32[]{:S(2)}) %collective-permute-start.1) | collective-permute-done | bytes 65568 | tf_op jit(solution)/shard_map/ppermute | solution.py:71
  46.6 15.0 %all_to_all.21 = bf16[16,8,2816]{2,1,0:T(8,128)(2,1)S(1)} all-to-all(bf16[16,8,2816]{2,1,0:T(8,128)(2,1)S(1)} %bitcast.18), channel_id=1, replica_groups=mesh['z'=4,'y'=4,'x'=4,'core'=2] {'z','y'}, dimensions={0} | all-to-all | bytes 1441792 | tf_op jit(solution)/shard_map/all_to_all | solution.py:61
  62.0 11.1 %all_to_all.22 = bf16[16,8,1376]{2,1,0:T(8,128)(2,1)S(1)} all-to-all(bf16[16,8,1376]{2,1,0:T(8,128)(2,1)S(1)} %broadcast_in_dim.3), channel_id=1, replica_groups=mesh['z'=4,'y'=4,'x'=4,'core'=2] {'z','y'}, dimensions={0} | all-to-all | bytes 704512 | tf_op jit(solution)/shard_map/all_to_all | solution.py:61
  73.4 3.6 %collective-permute-start.4 = (bf16[128,256]{1,0:T(8,128)(2,1)S(1)}, bf16[128,256]{1,0:T(8,128)(2,1)S(1)}, u32[]{:S(2)}, u32[]{:S(2)}) collective-permute-start(bf16[128,256]{1,0:T(8,128)(2,1)S(1)} %convolution_convert_fusion), channel_id=1, source_target_pairs={{0,1},{1,0},{2,3},{3,2},{4,5},{5,4},{6,7},{7,6},{8,9},{9,8},{10,11... | collective-permute-start | bytes 196616 | tf_op jit(solution)/shard_map/ppermute | solution.py:71
  77.0 0.9 %collective-permute-done.4 = bf16[128,256]{1,0:T(8,128)(2,1)S(1)} collective-permute-done((bf16[128,256]{1,0:T(8,128)(2,1)S(1)}, bf16[128,256]{1,0:T(8,128)(2,1)S(1)}, u32[]{:S(2)}, u32[]{:S(2)}) %collective-permute-start.4) | collective-permute-done | bytes 65568 | tf_op jit(solution)/shard_map/ppermute | solution.py:71
  78.0 1.5 %collective-permute-start.6 = (bf16[128,256]{1,0:T(8,128)(2,1)S(1)}, bf16[128,256]{1,0:T(8,128)(2,1)S(1)}, u32[]{:S(2)}, u32[]{:S(2)}) collective-permute-start(bf16[128,256]{1,0:T(8,128)(2,1)S(1)} %add_convert_fusion.1), channel_id=1, source_target_pairs={{0,2},{2,4},{4,6},{6,0},{1,3},{3,5},{5,7},{7,1},{8,10},{10,12},{12... | collective-permute-start | bytes 196616 | tf_op jit(solution)/shard_map/ppermute | solution.py:71
  79.5 0.7 collective-permute-start.5
  80.2 3.2 %write_state.3 = (f32[8,1,512,256]{3,2,1,0:T(8,128)}, f32[8,1,256]{2,1,0:T(1,128)}, f32[1,8]{1,0:T(1,128)}) custom-call(f32[8,640]{1,0:T(8,128)S(1)} %get-tuple-element.19.to_write, f32[8,512]{1,0:T(8,128)S(1)} %get-tuple-element.20.value, f32[8,1,512,256]{3,2,1,0:T(8,128)} %state.5, ...), custom_call_target="tpu_custom_call", output_to_operand_aliasing={{0}: (3, {})} | custom-call | flops 1000000000 | bytes 4194304 | tf_op jit(solution)/shard_map/write_state/pallas_call | solution.py:359
  83.4 0.7 collective-permute-done.5
  84.1 0.7 add_convert_fusion
  (30 shorter events, 3.4 us)
Async XLA Ops:
  0.6 72.5 %copy-start = (bf16[1376,256]{1,0:T(8,128)(2,1)S(1)}, bf16[1376,256]{1,0:T(8,128)(2,1)}, u32[]{:S(2)}) copy-start(bf16[1376,256]{1,0:T(8,128)(2,1)} %param.31) | copy-start | bytes 2113540
  3.1 18.3 %all-to-all-start = ((bf16[16,8,1664]{2,1,0:T(8,128)(2,1)}), bf16[16,8,1664]{2,1,0:T(8,128)(2,1)}, u32[]{:S(2)}, u32[]{:S(2)}) async-start(bf16[16,8,1664]{2,1,0:T(8,128)(2,1)} %bitcast.24), calls=%async_computation | async-start | bytes 851968 | tf_op jit(solution)/shard_map/all_to_all | solution.py:61
  11.7 1.0 %copy-start.3 = (bf16[512,256]{1,0:T(8,128)(2,1)S(1)}, bf16[512,256]{1,0:T(8,128)(2,1)}, u32[]{:S(2)}) copy-start(bf16[512,256]{1,0:T(8,128)(2,1)} %weight.1) | copy-start | bytes 786436
  12.7 0.7 copy-start.5
  13.4 0.7 copy-start.7
  14.0 0.7 copy-start.8
  17.0 29.1 %copy-start.4 = (bf16[128,256]{1,0:T(8,128)(2,1)S(1)}, bf16[128,256]{1,0:T(8,128)(2,1)}, u32[]{:S(2)}) copy-start(bf16[128,256]{1,0:T(8,128)(2,1)} %tok.1) | copy-start | bytes 196612
  17.0 29.1 %copy-start.6 = (f32[256]{0:T(256)S(1)}, f32[256]{0:T(256)}, u32[]{:S(2)}) copy-start(f32[256]{0:T(256)} %param.28) | copy-start | bytes 3076
  21.3 24.7 %copy-start.1 = (bf16[256,1376]{0,1:T(8,128)(2,1)S(1)}, bf16[256,1376]{0,1:T(8,128)(2,1)}, u32[]{:S(2)}) copy-start(bf16[256,1376]{0,1:T(8,128)(2,1)} %param.29) | copy-start | bytes 2113540
  21.4 24.7 %copy-start.2 = (bf16[256,1376]{0,1:T(8,128)(2,1)S(1)}, bf16[256,1376]{0,1:T(8,128)(2,1)}, u32[]{:S(2)}) copy-start(bf16[256,1376]{0,1:T(8,128)(2,1)} %param.30) | copy-start | bytes 2113540
  33.2 3.9 %collective-permute-start = (bf16[128,256]{1,0:T(8,128)(2,1)S(1)}, bf16[128,256]{1,0:T(8,128)(2,1)S(1)}, u32[]{:S(2)}, u32[]{:S(2)}) collective-permute-start(bf16[128,256]{1,0:T(8,128)(2,1)S(1)} %convolution_convert_fusion.1), channel_id=1, source_target_pairs={{0,1},{1,0},{2,3},{3,2},{4,5},{5,4},{6,7},{7,6},{8,9},{9,8},{10,11... | collective-permute-start | bytes 196616 | tf_op jit(solution)/shard_map/ppermute | solution.py:71
  37.1 6.2 %collective-permute-start.3 = (bf16[128,256]{1,0:T(8,128)(2,1)S(1)}, bf16[128,256]{1,0:T(8,128)(2,1)S(1)}, u32[]{:S(2)}, u32[]{:S(2)}) collective-permute-start(bf16[128,256]{1,0:T(8,128)(2,1)S(1)} %add_convert_fusion.2.term_0), channel_id=1, source_target_pairs={{0,6},{2,0},{4,2},{6,4},{1,7},{3,1},{5,3},{7,5},{8,14},{10,8},{12,... | collective-permute-start | bytes 196616 | tf_op jit(solution)/shard_map/ppermute | solution.py:71
  39.7 4.7 %collective-permute-start.2 = (bf16[128,256]{1,0:T(8,128)(2,1)S(1)}, bf16[128,256]{1,0:T(8,128)(2,1)S(1)}, u32[]{:S(2)}, u32[]{:S(2)}) collective-permute-start(bf16[128,256]{1,0:T(8,128)(2,1)S(1)} %add_convert_fusion.2.term_0), channel_id=1, source_target_pairs={{0,4},{2,6},{4,0},{6,2},{1,5},{3,7},{5,1},{7,3},{8,12},{10,14},{12... | collective-permute-start | bytes 196616 | tf_op jit(solution)/shard_map/ppermute | solution.py:71
  40.2 5.9 %collective-permute-start.1 = (bf16[128,256]{1,0:T(8,128)(2,1)S(1)}, bf16[128,256]{1,0:T(8,128)(2,1)S(1)}, u32[]{:S(2)}, u32[]{:S(2)}) collective-permute-start(bf16[128,256]{1,0:T(8,128)(2,1)S(1)} %add_convert_fusion.2.term_0), channel_id=1, source_target_pairs={{0,2},{2,4},{4,6},{6,0},{1,3},{3,5},{5,7},{7,1},{8,10},{10,12},{12... | collective-permute-start | bytes 196616 | tf_op jit(solution)/shard_map/ppermute | solution.py:71
  73.4 4.5 %collective-permute-start.4 = (bf16[128,256]{1,0:T(8,128)(2,1)S(1)}, bf16[128,256]{1,0:T(8,128)(2,1)S(1)}, u32[]{:S(2)}, u32[]{:S(2)}) collective-permute-start(bf16[128,256]{1,0:T(8,128)(2,1)S(1)} %convolution_convert_fusion), channel_id=1, source_target_pairs={{0,1},{1,0},{2,3},{3,2},{4,5},{5,4},{6,7},{7,6},{8,9},{9,8},{10,11... | collective-permute-start | bytes 196616 | tf_op jit(solution)/shard_map/ppermute | solution.py:71
  78.0 5.4 %collective-permute-start.7 = (bf16[128,256]{1,0:T(8,128)(2,1)S(1)}, bf16[128,256]{1,0:T(8,128)(2,1)S(1)}, u32[]{:S(2)}, u32[]{:S(2)}) collective-permute-start(bf16[128,256]{1,0:T(8,128)(2,1)S(1)} %add_convert_fusion.1), channel_id=1, source_target_pairs={{0,6},{2,0},{4,2},{6,4},{1,7},{3,1},{5,3},{7,5},{8,14},{10,8},{12,... | collective-permute-start | bytes 196616 | tf_op jit(solution)/shard_map/ppermute | solution.py:71
  78.0 5.4 %collective-permute-start.6 = (bf16[128,256]{1,0:T(8,128)(2,1)S(1)}, bf16[128,256]{1,0:T(8,128)(2,1)S(1)}, u32[]{:S(2)}, u32[]{:S(2)}) collective-permute-start(bf16[128,256]{1,0:T(8,128)(2,1)S(1)} %add_convert_fusion.1), channel_id=1, source_target_pairs={{0,2},{2,4},{4,6},{6,0},{1,3},{3,5},{5,7},{7,1},{8,10},{10,12},{12... | collective-permute-start | bytes 196616 | tf_op jit(solution)/shard_map/ppermute | solution.py:71
  79.5 4.6 %collective-permute-start.5 = (bf16[128,256]{1,0:T(8,128)(2,1)S(1)}, bf16[128,256]{1,0:T(8,128)(2,1)S(1)}, u32[]{:S(2)}, u32[]{:S(2)}) collective-permute-start(bf16[128,256]{1,0:T(8,128)(2,1)S(1)} %add_convert_fusion.1), channel_id=1, source_target_pairs={{0,4},{2,6},{4,0},{6,2},{1,5},{3,7},{5,1},{7,3},{8,12},{10,14},{12... | collective-permute-start | bytes 196616 | tf_op jit(solution)/shard_map/ppermute | solution.py:71

commit v6 on v5

--- a/solution.py
+++ b/solution.py
@@ -15,7 +15,6 @@
 vmem = pl.BlockSpec(memory_space=pltpu.VMEM)
 hbm = pl.BlockSpec(memory_space=pltpu.HBM)
 low_at = 32
-extra_rows = 16
 nt_dims = (((1,), (1,)), ((), ()))
 
 
@@ -51,9 +50,9 @@
 def split_three(value):
     parts = []
     for _ in range(3):
-        part = value.astype(jnp.bfloat16).astype(jnp.float32)
+        part = value.astype(jnp.bfloat16)
         parts.append(part)
-        value = value - part
+        value = value - part.astype(jnp.float32)
     return parts
 
 
@@ -143,16 +142,18 @@
     old_m = jnp.sum(old_m, axis=1, keepdims=True)
     mine = lane_ids(bias.shape) == index_of(tp)
     bias_here = jnp.sum(jnp.where(mine, bias[...], 0.0), axis=1, keepdims=True)
-    row = row_ids((extra_rows, query_size))
-    for b in range(rows):
-        block = jnp.zeros((extra_rows, query_size), jnp.float32)
-        for i, source in enumerate((state_n[b], old_m[b : b + 1], bias_here)):
-            for j, part in enumerate(split_three(source)):
-                block = jnp.where(row == 3 * i + j, part, block)
-        short[b, value_size:] = block.astype(jnp.bfloat16)
+    whole = (rows, query_size)
+    at = rows * value_size
+    for source in (
+        state_n[...].reshape(whole),
+        jnp.where(lane_ids(whole) < lanes, old_m, bias_here),
+    ):
+        for part in split_three(source):
+            short[at : at + rows] = part
+            at += rows
     for b in range(rows):
         copies[b].wait()
-        short[b, :value_size] = held[b].astype(jnp.bfloat16)
+        short[b * value_size : (b + 1) * value_size] = held[b].astype(jnp.bfloat16)
     copies[rows].wait()
 
 
@@ -160,9 +161,14 @@
     width_all, heads, arrived, state_short, sent, to_write, value_out
 ):
     rows = arrived.shape[1]
-    value_size, query_size = state_short.shape[1] - extra_rows, state_short.shape[2]
-    kept = state_short[:, value_size:, :].astype(jnp.float32)
-    state_n, old_m, bias = (kept[:, i] + kept[:, i + 1] + kept[:, i + 2] for i in (0, 3, 6))
+    query_size = state_short.shape[1]
+    value_size = value_out.shape[1]
+    at = rows * value_size
+    kept = [
+        state_short[at + i * rows : at + (i + 1) * rows].astype(jnp.float32) for i in range(6)
+    ]
+    state_n = kept[0] + kept[1] + kept[2]
+    others = kept[3] + kept[4] + kept[5]
     proj_width = 2 * query_size + 2 * value_size
     total = arrived[0].astype(jnp.float32)
     for i in range(1, arrived.shape[0]):
@@ -177,9 +183,9 @@
     head = index_of(tp)
     scale = lax.rsqrt(column(2 * heads) / width_all + norm_floor)
     log_input = column(head) * scale
-    forget_pre = column(heads + head) * scale + bias[:, :1]
+    forget_pre = column(heads + head) * scale + others[:, lanes : lanes + 1]
     log_forget = jnp.minimum(forget_pre, 0.0) - jnp.log(1.0 + jnp.exp(-jnp.abs(forget_pre)))
-    carried = log_forget + old_m[:, :1]
+    carried = log_forget + others[:, :1]
     top = jnp.maximum(carried, log_input)
     keep = jnp.exp(carried - top)
     admit = jnp.exp(log_input - top)
@@ -197,7 +203,8 @@
     reads = jnp.zeros((2 * rows, value_size), jnp.float32)
     for b in range(rows):
         one = jnp.where((row == b) | (row == b + rows), both, 0.0).astype(jnp.bfloat16)
-        reads += lax.dot_general(one, state_short[b, :value_size], nt_dims, preferred_element_type=jnp.float32)
+        block = state_short[b * value_size : (b + 1) * value_size]
+        reads += lax.dot_general(one, block, nt_dims, preferred_element_type=jnp.float32)
     numer = keep * (reads[:rows] + reads[rows:]) + match * value
     head_out = numer / ((1.0 + jnp.exp(-out_pre)) * denom)
     short = head_out.astype(jnp.bfloat16)
@@ -210,37 +217,22 @@
     value_out[...] = value
 
 
-def write_kernel(first, to_write, value, state, *refs):
-    outputs, held, sems_in, sems_out = refs[:-3], *refs[-3:]
-    count, _, query_size = held.shape
-    if first == 0:
-        new_c, order = outputs
-        order[...] = jnp.zeros_like(order)
-    else:
-        _, new_c, new_n, new_m = outputs
-        new_n[...] = to_write[:, lanes + query_size :].reshape(new_n.shape)
-        rows = to_write.shape[0]
-        square = (rows, rows)
-        top = jnp.broadcast_to(to_write[:, 1:2], square)
-        new_m[...] = jnp.sum(
-            jnp.where(row_ids(square) == lane_ids(square), top, 0.0), axis=0, keepdims=True
-        )
-    into = [
-        pltpu.make_async_copy(state.at[first + b, 0], held.at[b], sems_in.at[b])
-        for b in range(count)
-    ]
-    out = [
-        pltpu.make_async_copy(held.at[b], new_c.at[first + b, 0], sems_out.at[b])
-        for b in range(count)
-    ]
+def write_kernel(to_write, value, state, new_c, new_n, new_m, held, sems_in, sems_out):
+    rows, _, query_size = held.shape
+    into = [pltpu.make_async_copy(state.at[b, 0], held.at[b], sems_in.at[b]) for b in range(rows)]
+    out = [pltpu.make_async_copy(held.at[b], new_c.at[b, 0], sems_out.at[b]) for b in range(rows)]
     for copy in into:
         copy.start()
+    new_n[...] = to_write[:, lanes + query_size :].reshape(new_n.shape)
+    square = (rows, rows)
+    top = jnp.broadcast_to(to_write[:, 1:2], square)
+    diagonal = row_ids(square) == lane_ids(square)
+    new_m[...] = jnp.sum(jnp.where(diagonal, top, 0.0), axis=0, keepdims=True)
     across = value[...].T
-    for b in range(count):
-        row = first + b
-        down = across[:, row : row + 1]
-        keep = to_write[row : row + 1, :1]
-        key_in = to_write[row : row + 1, lanes : lanes + query_size]
+    for b in range(rows):
+        down = across[:, b : b + 1]
+        keep = to_write[b : b + 1, :1]
+        key_in = to_write[b : b + 1, lanes : lanes + query_size]
         into[b].wait()
         held[b] = keep * held[b] + down * key_in
         out[b].start()
@@ -248,9 +240,7 @@
         copy.wait()
 
 
-def widen_kernel(
-    term_0, term_1, term_2, term_3, tok, gain, gate_t, up_t, order, sent, middle
-):
+def widen_kernel(term_0, term_1, term_2, term_3, tok, gain, gate_t, up_t, sent, middle):
     attn_mix = in_order([term[...] for term in (term_0, term_1, term_2, term_3)])
     mid = (tok[...].astype(jnp.float32) + attn_mix).astype(jnp.bfloat16)
     middle[...] = mid
@@ -310,14 +300,14 @@
             pltpu.VMEM((lanes, width_dev), bf16),
             pltpu.SemaphoreType.DMA((8,)),
         ],
-        compiler_params=params(63),
+        compiler_params=params(60),
         cost_estimate=cost(2 * batch * width_dev * proj_width, 2 * width_dev * proj_width),
         name="project",
     )(tokens, attn_gain.reshape(1, width_dev), w_query, w_key, w_value, w_outgate, w_gates.T)
     state_short, w_output_near = pl.pallas_call(
         near_kernel,
         out_shape=(
-            jax.ShapeDtypeStruct((rows, value_size + extra_rows, query_size), bf16),
+            jax.ShapeDtypeStruct((rows * (value_size + 6), query_size), bf16),
             jax.ShapeDtypeStruct(w_output.shape, w_output.dtype),
         ),
         in_specs=[hbm] * 5,
@@ -350,34 +340,27 @@
         in_specs=[vmem] * 2,
         out_specs=[vmem] * 3,
         compiler_params=params(8),
-        cost_estimate=cost(10**8, 4 * rows * value_size * query_size),
+        cost_estimate=cost(10**10, 4 * rows * value_size * query_size),
         name="cell",
     )(arrived, state_short)
-    half_rows = rows // 2
-
-    def written(first, extra, *begun):
-        return pl.pallas_call(
-            functools.partial(write_kernel, first),
-            out_shape=(jax.ShapeDtypeStruct(state_c.shape, f32), *extra),
-            in_specs=[vmem, vmem, hbm] + [hbm] * len(begun),
-            out_specs=(hbm,) + (vmem,) * len(extra),
-            input_output_aliases={3: 0} if begun else {},
-            scratch_shapes=[
-                pltpu.VMEM((half_rows, value_size, query_size), f32),
-                pltpu.SemaphoreType.DMA((half_rows,)),
-                pltpu.SemaphoreType.DMA((half_rows,)),
-            ],
-            compiler_params=params(50),
-            cost_estimate=cost(10**9, 4 * rows * value_size * query_size),
-            name="write_state",
-        )(to_write, value, state_c, *begun)
-
-    begun_c, order = written(0, (jax.ShapeDtypeStruct((8, lanes), f32),))
-    new_c, new_n, new_m = written(
-        half_rows,
-        (jax.ShapeDtypeStruct(state_n.shape, f32), jax.ShapeDtypeStruct((1, rows), f32)),
-        begun_c,
-    )
+    new_c, new_n, new_m = pl.pallas_call(
+        write_kernel,
+        out_shape=(
+            jax.ShapeDtypeStruct(state_c.shape, f32),
+            jax.ShapeDtypeStruct(state_n.shape, f32),
+            jax.ShapeDtypeStruct((1, rows), f32),
+        ),
+        in_specs=[vmem, vmem, hbm],
+        out_specs=(hbm, vmem, vmem),
+        scratch_shapes=[
+            pltpu.VMEM((rows, value_size, query_size), f32),
+            pltpu.SemaphoreType.DMA((rows,)),
+            pltpu.SemaphoreType.DMA((rows,)),
+        ],
+        compiler_params=params(50),
+        cost_estimate=cost(10**9, 8 * rows * value_size * query_size),
+        name="write_state",
+    )(to_write, value, state_c)
     heads_rows = exchange(head_copies, kv).reshape(batch, value_size)
     attn_part = jnp.dot(heads_rows, w_output_near, preferred_element_type=f32)
     hidden_dev = w_gateff.shape[1]
@@ -388,7 +371,7 @@
             jax.ShapeDtypeStruct((batch, 2 * hidden_pad), bf16),
             jax.ShapeDtypeStruct((batch, width_dev), bf16),
         ),
-        in_specs=[vmem] * 9,
+        in_specs=[vmem] * 8,
         out_specs=[vmem] * 2,
         compiler_params=params(8),
         cost_estimate=cost(4 * batch * width_dev * hidden_dev, 4 * width_dev * hidden_dev),
@@ -399,7 +382,6 @@
         mlp_gain.reshape(1, width_dev),
         w_gateff.T,
         w_upff.T,
-        order,
     )
     mid_float = middle.astype(f32)
     arrived = exchange(sent.reshape(kv_count, rows, 2 * hidden_pad), kv)

time: 86 us -> 84.7 us (0.985)
  Pallas kernels: 12.8 us -> 9.93 us
  waiting for transfers between devices: 9.55 us -> 11.4 us
    ppermute x8, waiting for transfers between devices: 5.18 us -> 7.06 us  [shifted(): lax.ppermute(value, axis, [(i, (i + step) % size) for i in range(size)])]
    pallas_call x3 -> x2, Pallas kernels: 7.99 us -> 6.26 us  [the longest x1 3.98 us: per_device(): pl.pallas_call(write_kernel, out_shape=(jax.ShapeDtypeStruct(state_c.shap...]
    pallas_call x1, Pallas kernels: 1.84 us -> 0.72 us  [per_device(): pl.pallas_call(functools.partial(cell_kernel, width_all, heads_all), out_...]
  transfers between devices with their start and end apart: 9 -> 9, of which waited for: 6 -> 6; matrix products, arithmetic and copies ran while one was open for 0% -> 0% of each run, Pallas kernels for 9% -> 7%
where the time goes in v6:
time: 84.7 us; the launch traced here: 83.7 us
  blocking collectives  35.8 us (42%)
  starting transfers between devices  21.2 us (25%)
  waiting for transfers between devices  11.4 us (13%)
  Pallas kernels  9.93 us (12%)
  local copies, waits for them, and re-layouts  3 us (4%)
  other arithmetic  1.1 us (1%)
    all_to_all x3, blocking collectives, exchange(): return lax.all_to_all(value, axis, split_axis=0, concat_axis=0, tiled=True)  35.8 us
    ppermute x8, starting transfers between devices, shifted(): lax.ppermute(value, axis, [(i, (i + step) % size) for i in range(size)])  12.6 us
    all_to_all x1, starting transfers between devices, exchange(): return lax.all_to_all(value, axis, split_axis=0, concat_axis=0, tiled=True)  8.6 us
    ppermute x8, waiting for transfers between devices, shifted(): lax.ppermute(value, axis, [(i, (i + step) % size) for i in range(size)])  7.06 us
    all_to_all x1, waiting for transfers between devices, exchange(): return lax.all_to_all(value, axis, split_axis=0, concat_axis=0, tiled=True)  4.33 us
    pallas_call x1, Pallas kernels, per_device(): pl.pallas_call(write_kernel, out_shape=(jax.ShapeDtypeStruct(state_c.shap...  3.98 us
    unnamed x18, local copies, waits for them, and re-layouts  2.98 us
    pallas_call x1, Pallas kernels, per_device(): pl.pallas_call(project_kernel, out_shape=jax.ShapeDtypeStruct((batch, pro...  2.4 us
  transfers between devices with their start and end apart: 9, of which 6 were waited for; matrix products, arithmetic and copies ran while one was open for 0% of the time, Pallas kernels for 7%

profile of v6, /device:TPU:1, one launch (start us, length us, event | category | flops | bytes accessed | tf_op | source)
XLA Modules:
  0.0 83.7 jit_solution(14014413886094093428)
XLA Ops:
  0.6 2.4 %project.1 = bf16[128,1664]{1,0:T(8,128)(2,1)} custom-call(bf16[128,256]{1,0:T(8,128)(2,1)} %tok.1, f32[1,256]{1,0:T(1,128)} %bitcast.26, bf16[256,256]{1,0:T(8,128)(2,1)} %w_query.1, bf16[256,256]{1,0:T(8,128)(2,1)} %w_key.1, bf16[256,512]{1,0:T(8,128)(2,1)} %w_value.1, bf16[256,512]{1,0:T(8,128)(2,1)} %w_outgate.1, bf16[16,4096]{1,0:T(8,128)(2,1)} %bitcast.25), custom_call_target="tpu_custom_call" | custom-call | flops 100663296 | bytes 786432 | tf_op jit(solution)/shard_map/project/pallas_call | solution.py:291
  3.1 8.6 %all-to-all-start = ((bf16[16,8,1664]{2,1,0:T(8,128)(2,1)}), bf16[16,8,1664]{2,1,0:T(8,128)(2,1)S(1)}, u32[]{:S(2)}, u32[]{:S(2)}) async-start(bf16[16,8,1664]{2,1,0:T(8,128)(2,1)} %bitcast.24), calls=%async_computation | async-start | bytes 851968 | tf_op jit(solution)/shard_map/all_to_all | solution.py:60
  11.7 0.9 %copy-done.3 = bf16[512,256]{1,0:T(8,128)(2,1)S(1)} copy-done((bf16[512,256]{1,0:T(8,128)(2,1)S(1)}, bf16[512,256]{1,0:T(8,128)(2,1)}, u32[]{:S(2)}) %copy-start.3) | copy-done | bytes 262168
  12.6 0.7 copy-done.5
  13.3 0.7 copy-done.7
  14.0 0.7 copy-done.8
  14.6 2.3 %near.1 = (bf16[4144,256]{1,0:T(8,128)(2,1)S(1)}, bf16[512,256]{1,0:T(8,128)(2,1)S(1)}) custom-call(f32[8,1,512,256]{3,2,1,0:T(8,128)} %state.3, bf16[512,256]{1,0:T(8,128)(2,1)S(1)} %copy-done.3, f32[8,1,256]{2,1,0:T(1,128)S(1)} %copy-done.5, f32[1,8]{1,0:T(1,128)S(1)} %bitcast.22, f32[1,8]{1,0:T(1,128)S(1)} %bitcast.23), custom_call_target="tpu_custom_call" | custom-call | flops 1000000000 | bytes 6291456 | tf_op jit(solution)/shard_map/near/pallas_call | solution.py:307
  16.9 4.3 %all-to-all-done.arrived = bf16[16,8,1664]{2,1,0:T(8,128)(2,1)S(1)} async-done(((bf16[16,8,1664]{2,1,0:T(8,128)(2,1)}), bf16[16,8,1664]{2,1,0:T(8,128)(2,1)S(1)}, u32[]{:S(2)}, u32[]{:S(2)}) %all-to-all-start) | async-done | bytes 426016 | tf_op jit(solution)/shard_map/all_to_all | solution.py:60
  21.3 0.7 cell.1
  22.0 9.8 %all_to_all.20 = bf16[16,8,512]{2,1,0:T(8,128)(2,1)S(1)} all-to-all(bf16[16,8,512]{2,1,0:T(8,128)(2,1)S(1)} %get-tuple-element.15), channel_id=1, replica_groups=mesh['z'=4,'y'=4,'x'=4,'core'=2] {'z','y'}, dimensions={0} | all-to-all | bytes 262144 | tf_op jit(solution)/shard_map/all_to_all | solution.py:60
  31.9 3.0 %collective-permute-start = (bf16[128,256]{1,0:T(8,128)(2,1)S(1)}, bf16[128,256]{1,0:T(8,128)(2,1)S(1)}, u32[]{:S(2)}, u32[]{:S(2)}) collective-permute-start(bf16[128,256]{1,0:T(8,128)(2,1)S(1)} %convolution_convert_fusion.1), channel_id=1, source_target_pairs={{0,1},{1,0},{2,3},{3,2},{4,5},{5,4},{6,7},{7,6},{8,9},{9,8},{10,11... | collective-permute-start | bytes 196616 | tf_op jit(solution)/shard_map/ppermute | solution.py:70
  35.0 0.9 %collective-permute-done = bf16[128,256]{1,0:T(8,128)(2,1)S(1)} collective-permute-done((bf16[128,256]{1,0:T(8,128)(2,1)S(1)}, bf16[128,256]{1,0:T(8,128)(2,1)S(1)}, u32[]{:S(2)}, u32[]{:S(2)}) %collective-permute-start) | collective-permute-done | bytes 65568 | tf_op jit(solution)/shard_map/ppermute | solution.py:70
  35.9 2.5 %collective-permute-start.3 = (bf16[128,256]{1,0:T(8,128)(2,1)S(1)}, bf16[128,256]{1,0:T(8,128)(2,1)S(1)}, u32[]{:S(2)}, u32[]{:S(2)}) collective-permute-start(bf16[128,256]{1,0:T(8,128)(2,1)S(1)} %add_convert_fusion.2.term_0), channel_id=1, source_target_pairs={{0,6},{2,0},{4,2},{6,4},{1,7},{3,1},{5,3},{7,5},{8,14},{10,8},{12,... | collective-permute-start | bytes 196616 | tf_op jit(solution)/shard_map/ppermute | solution.py:70
  39.0 0.6 collective-permute-start.1
  39.8 3.3 %collective-permute-done.2.term_2 = bf16[128,256]{1,0:T(8,128)(2,1)S(1)} collective-permute-done((bf16[128,256]{1,0:T(8,128)(2,1)S(1)}, bf16[128,256]{1,0:T(8,128)(2,1)S(1)}, u32[]{:S(2)}, u32[]{:S(2)}) %collective-permute-start.2) | collective-permute-done | bytes 65568 | tf_op jit(solution)/shard_map/ppermute | solution.py:70
  43.1 1.7 %collective-permute-done.1.term_1 = bf16[128,256]{1,0:T(8,128)(2,1)S(1)} collective-permute-done((bf16[128,256]{1,0:T(8,128)(2,1)S(1)}, bf16[128,256]{1,0:T(8,128)(2,1)S(1)}, u32[]{:S(2)}, u32[]{:S(2)}) %collective-permute-start.1) | collective-permute-done | bytes 65568 | tf_op jit(solution)/shard_map/ppermute | solution.py:70
  45.4 15.0 %all_to_all.21 = bf16[16,8,2816]{2,1,0:T(8,128)(2,1)S(1)} all-to-all(bf16[16,8,2816]{2,1,0:T(8,128)(2,1)S(1)} %bitcast.18), channel_id=1, replica_groups=mesh['z'=4,'y'=4,'x'=4,'core'=2] {'z','y'}, dimensions={0} | all-to-all | bytes 1441792 | tf_op jit(solution)/shard_map/all_to_all | solution.py:60
  60.8 11.1 %all_to_all.22 = bf16[16,8,1376]{2,1,0:T(8,128)(2,1)S(1)} all-to-all(bf16[16,8,1376]{2,1,0:T(8,128)(2,1)S(1)} %broadcast_in_dim.3), channel_id=1, replica_groups=mesh['z'=4,'y'=4,'x'=4,'core'=2] {'z','y'}, dimensions={0} | all-to-all | bytes 704512 | tf_op jit(solution)/shard_map/all_to_all | solution.py:60
  72.2 3.6 %collective-permute-start.4 = (bf16[128,256]{1,0:T(8,128)(2,1)S(1)}, bf16[128,256]{1,0:T(8,128)(2,1)S(1)}, u32[]{:S(2)}, u32[]{:S(2)}) collective-permute-start(bf16[128,256]{1,0:T(8,128)(2,1)S(1)} %convolution_convert_fusion), channel_id=1, source_target_pairs={{0,1},{1,0},{2,3},{3,2},{4,5},{5,4},{6,7},{7,6},{8,9},{9,8},{10,11... | collective-permute-start | bytes 196616 | tf_op jit(solution)/shard_map/ppermute | solution.py:70
  75.8 0.9 %collective-permute-done.4 = bf16[128,256]{1,0:T(8,128)(2,1)S(1)} collective-permute-done((bf16[128,256]{1,0:T(8,128)(2,1)S(1)}, bf16[128,256]{1,0:T(8,128)(2,1)S(1)}, u32[]{:S(2)}, u32[]{:S(2)}) %collective-permute-start.4) | collective-permute-done | bytes 65568 | tf_op jit(solution)/shard_map/ppermute | solution.py:70
  76.8 1.5 %collective-permute-start.6 = (bf16[128,256]{1,0:T(8,128)(2,1)S(1)}, bf16[128,256]{1,0:T(8,128)(2,1)S(1)}, u32[]{:S(2)}, u32[]{:S(2)}) collective-permute-start(bf16[128,256]{1,0:T(8,128)(2,1)S(1)} %add_convert_fusion.1), channel_id=1, source_target_pairs={{0,2},{2,4},{4,6},{6,0},{1,3},{3,5},{5,7},{7,1},{8,10},{10,12},{12... | collective-permute-start | bytes 196616 | tf_op jit(solution)/shard_map/ppermute | solution.py:70
  78.3 0.7 collective-permute-start.5
  79.0 4.0 %write_state.1 = (f32[8,1,512,256]{3,2,1,0:T(8,128)}, f32[8,1,256]{2,1,0:T(1,128)}, f32[1,8]{1,0:T(1,128)}) custom-call(f32[8,640]{1,0:T(8,128)S(1)} %get-tuple-element.19.to_write, f32[8,512]{1,0:T(8,128)S(1)} %get-tuple-element.20.value, f32[8,1,512,256]{3,2,1,0:T(8,128)} %state.3), custom_call_target="tpu_custom_call" | custom-call | flops 1000000000 | bytes 8388608 | tf_op jit(solution)/shard_map/write_state/pallas_call | solution.py:346
  83.0 0.7 add_convert_fusion
  (29 shorter events, 2.3 us)
Async XLA Ops:
  0.6 71.3 %copy-start = (bf16[1376,256]{1,0:T(8,128)(2,1)S(1)}, bf16[1376,256]{1,0:T(8,128)(2,1)}, u32[]{:S(2)}) copy-start(bf16[1376,256]{1,0:T(8,128)(2,1)} %param.31) | copy-start | bytes 2113540
  3.1 18.2 %all-to-all-start = ((bf16[16,8,1664]{2,1,0:T(8,128)(2,1)}), bf16[16,8,1664]{2,1,0:T(8,128)(2,1)S(1)}, u32[]{:S(2)}, u32[]{:S(2)}) async-start(bf16[16,8,1664]{2,1,0:T(8,128)(2,1)} %bitcast.24), calls=%async_computation | async-start | bytes 851968 | tf_op jit(solution)/shard_map/all_to_all | solution.py:60
  11.7 1.0 %copy-start.3 = (bf16[512,256]{1,0:T(8,128)(2,1)S(1)}, bf16[512,256]{1,0:T(8,128)(2,1)}, u32[]{:S(2)}) copy-start(bf16[512,256]{1,0:T(8,128)(2,1)} %weight.1) | copy-start | bytes 786436
  12.6 0.7 copy-start.5
  13.3 0.7 copy-start.7
  14.0 0.7 copy-start.8
  21.2 23.6 %copy-start.1 = (bf16[256,1376]{0,1:T(8,128)(2,1)S(1)}, bf16[256,1376]{0,1:T(8,128)(2,1)}, u32[]{:S(2)}) copy-start(bf16[256,1376]{0,1:T(8,128)(2,1)} %param.29) | copy-start | bytes 2113540
  21.2 23.6 %copy-start.2 = (bf16[256,1376]{0,1:T(8,128)(2,1)S(1)}, bf16[256,1376]{0,1:T(8,128)(2,1)}, u32[]{:S(2)}) copy-start(bf16[256,1376]{0,1:T(8,128)(2,1)} %param.30) | copy-start | bytes 2113540
  21.2 23.6 %copy-start.4 = (bf16[128,256]{1,0:T(8,128)(2,1)S(1)}, bf16[128,256]{1,0:T(8,128)(2,1)}, u32[]{:S(2)}) copy-start(bf16[128,256]{1,0:T(8,128)(2,1)} %tok.1) | copy-start | bytes 196612
  21.2 23.6 %copy-start.6 = (f32[256]{0:T(256)S(1)}, f32[256]{0:T(256)}, u32[]{:S(2)}) copy-start(f32[256]{0:T(256)} %param.28) | copy-start | bytes 3076
  31.9 3.9 %collective-permute-start = (bf16[128,256]{1,0:T(8,128)(2,1)S(1)}, bf16[128,256]{1,0:T(8,128)(2,1)S(1)}, u32[]{:S(2)}, u32[]{:S(2)}) collective-permute-start(bf16[128,256]{1,0:T(8,128)(2,1)S(1)} %convolution_convert_fusion.1), channel_id=1, source_target_pairs={{0,1},{1,0},{2,3},{3,2},{4,5},{5,4},{6,7},{7,6},{8,9},{9,8},{10,11... | collective-permute-start | bytes 196616 | tf_op jit(solution)/shard_map/ppermute | solution.py:70
  35.9 3.9 %collective-permute-start.3 = (bf16[128,256]{1,0:T(8,128)(2,1)S(1)}, bf16[128,256]{1,0:T(8,128)(2,1)S(1)}, u32[]{:S(2)}, u32[]{:S(2)}) collective-permute-start(bf16[128,256]{1,0:T(8,128)(2,1)S(1)} %add_convert_fusion.2.term_0), channel_id=1, source_target_pairs={{0,6},{2,0},{4,2},{6,4},{1,7},{3,1},{5,3},{7,5},{8,14},{10,8},{12,... | collective-permute-start | bytes 196616 | tf_op jit(solution)/shard_map/ppermute | solution.py:70
  38.5 4.7 %collective-permute-start.2 = (bf16[128,256]{1,0:T(8,128)(2,1)S(1)}, bf16[128,256]{1,0:T(8,128)(2,1)S(1)}, u32[]{:S(2)}, u32[]{:S(2)}) collective-permute-start(bf16[128,256]{1,0:T(8,128)(2,1)S(1)} %add_convert_fusion.2.term_0), channel_id=1, source_target_pairs={{0,4},{2,6},{4,0},{6,2},{1,5},{3,7},{5,1},{7,3},{8,12},{10,14},{12... | collective-permute-start | bytes 196616 | tf_op jit(solution)/shard_map/ppermute | solution.py:70
  39.0 5.9 %collective-permute-start.1 = (bf16[128,256]{1,0:T(8,128)(2,1)S(1)}, bf16[128,256]{1,0:T(8,128)(2,1)S(1)}, u32[]{:S(2)}, u32[]{:S(2)}) collective-permute-start(bf16[128,256]{1,0:T(8,128)(2,1)S(1)} %add_convert_fusion.2.term_0), channel_id=1, source_target_pairs={{0,2},{2,4},{4,6},{6,0},{1,3},{3,5},{5,7},{7,1},{8,10},{10,12},{12... | collective-permute-start | bytes 196616 | tf_op jit(solution)/shard_map/ppermute | solution.py:70
  72.2 4.5 %collective-permute-start.4 = (bf16[128,256]{1,0:T(8,128)(2,1)S(1)}, bf16[128,256]{1,0:T(8,128)(2,1)S(1)}, u32[]{:S(2)}, u32[]{:S(2)}) collective-permute-start(bf16[128,256]{1,0:T(8,128)(2,1)S(1)} %convolution_convert_fusion), channel_id=1, source_target_pairs={{0,1},{1,0},{2,3},{3,2},{4,5},{5,4},{6,7},{7,6},{8,9},{9,8},{10,11... | collective-permute-start | bytes 196616 | tf_op jit(solution)/shard_map/ppermute | solution.py:70
  76.7 6.3 %collective-permute-start.7 = (bf16[128,256]{1,0:T(8,128)(2,1)S(1)}, bf16[128,256]{1,0:T(8,128)(2,1)S(1)}, u32[]{:S(2)}, u32[]{:S(2)}) collective-permute-start(bf16[128,256]{1,0:T(8,128)(2,1)S(1)} %add_convert_fusion.1), channel_id=1, source_target_pairs={{0,6},{2,0},{4,2},{6,4},{1,7},{3,1},{5,3},{7,5},{8,14},{10,8},{12,... | collective-permute-start | bytes 196616 | tf_op jit(solution)/shard_map/ppermute | solution.py:70
  76.8 6.2 %collective-permute-start.6 = (bf16[128,256]{1,0:T(8,128)(2,1)S(1)}, bf16[128,256]{1,0:T(8,128)(2,1)S(1)}, u32[]{:S(2)}, u32[]{:S(2)}) collective-permute-start(bf16[128,256]{1,0:T(8,128)(2,1)S(1)} %add_convert_fusion.1), channel_id=1, source_target_pairs={{0,2},{2,4},{4,6},{6,0},{1,3},{3,5},{5,7},{7,1},{8,10},{10,12},{12... | collective-permute-start | bytes 196616 | tf_op jit(solution)/shard_map/ppermute | solution.py:70
  78.3 4.8 %collective-permute-start.5 = (bf16[128,256]{1,0:T(8,128)(2,1)S(1)}, bf16[128,256]{1,0:T(8,128)(2,1)S(1)}, u32[]{:S(2)}, u32[]{:S(2)}) collective-permute-start(bf16[128,256]{1,0:T(8,128)(2,1)S(1)} %add_convert_fusion.1), channel_id=1, source_target_pairs={{0,4},{2,6},{4,0},{6,2},{1,5},{3,7},{5,1},{7,3},{8,12},{10,14},{12... | collective-permute-start | bytes 196616 | tf_op jit(solution)/shard_map/ppermute | solution.py:70

commit v7 on v5

--- a/solution.py
+++ b/solution.py
@@ -15,7 +15,6 @@
 vmem = pl.BlockSpec(memory_space=pltpu.VMEM)
 hbm = pl.BlockSpec(memory_space=pltpu.HBM)
 low_at = 32
-extra_rows = 16
 nt_dims = (((1,), (1,)), ((), ()))
 
 
@@ -51,9 +50,9 @@
 def split_three(value):
     parts = []
     for _ in range(3):
-        part = value.astype(jnp.bfloat16).astype(jnp.float32)
+        part = value.astype(jnp.bfloat16)
         parts.append(part)
-        value = value - part
+        value = value - part.astype(jnp.float32)
     return parts
 
 
@@ -66,18 +65,17 @@
     return exchange(copies, axis)
 
 
-def shifted(value, axis, step):
-    size = lax.axis_size(axis)
-    return lax.ppermute(value, axis, [(i, (i + step) % size) for i in range(size)])
+def swapped(value, axis, bits):
+    return lax.ppermute(value, axis, [(i, i ^ bits) for i in range(lax.axis_size(axis))])
 
 
 def over_tp(part):
     mine = part.astype(jnp.bfloat16)
-    theirs = shifted(mine, "core", 1)
+    theirs = swapped(mine, "core", 1)
     pair = (mine.astype(jnp.float32) + theirs.astype(jnp.float32)).astype(jnp.bfloat16)
     terms = [pair]
     for step in range(1, lax.axis_size("x")):
-        terms.append(shifted(pair, "x", step))
+        terms.append(swapped(pair, "x", step))
     return terms
 
 
@@ -143,16 +141,18 @@
     old_m = jnp.sum(old_m, axis=1, keepdims=True)
     mine = lane_ids(bias.shape) == index_of(tp)
     bias_here = jnp.sum(jnp.where(mine, bias[...], 0.0), axis=1, keepdims=True)
-    row = row_ids((extra_rows, query_size))
-    for b in range(rows):
-        block = jnp.zeros((extra_rows, query_size), jnp.float32)
-        for i, source in enumerate((state_n[b], old_m[b : b + 1], bias_here)):
-            for j, part in enumerate(split_three(source)):
-                block = jnp.where(row == 3 * i + j, part, block)
-        short[b, value_size:] = block.astype(jnp.bfloat16)
+    whole = (rows, query_size)
+    at = rows * value_size
+    for source in (
+        state_n[...].reshape(whole),
+        jnp.where(lane_ids(whole) < lanes, old_m, bias_here),
+    ):
+        for part in split_three(source):
+            short[at : at + rows] = part
+            at += rows
     for b in range(rows):
         copies[b].wait()
-        short[b, :value_size] = held[b].astype(jnp.bfloat16)
+        short[b * value_size : (b + 1) * value_size] = held[b].astype(jnp.bfloat16)
     copies[rows].wait()
 
 
@@ -160,9 +160,14 @@
     width_all, heads, arrived, state_short, sent, to_write, value_out
 ):
     rows = arrived.shape[1]
-    value_size, query_size = state_short.shape[1] - extra_rows, state_short.shape[2]
-    kept = state_short[:, value_size:, :].astype(jnp.float32)
-    state_n, old_m, bias = (kept[:, i] + kept[:, i + 1] + kept[:, i + 2] for i in (0, 3, 6))
+    query_size = state_short.shape[1]
+    value_size = value_out.shape[1]
+    at = rows * value_size
+    kept = [
+        state_short[at + i * rows : at + (i + 1) * rows].astype(jnp.float32) for i in range(6)
+    ]
+    state_n = kept[0] + kept[1] + kept[2]
+    others = kept[3] + kept[4] + kept[5]
     proj_width = 2 * query_size + 2 * value_size
     total = arrived[0].astype(jnp.float32)
     for i in range(1, arrived.shape[0]):
@@ -177,9 +182,9 @@
     head = index_of(tp)
     scale = lax.rsqrt(column(2 * heads) / width_all + norm_floor)
     log_input = column(head) * scale
-    forget_pre = column(heads + head) * scale + bias[:, :1]
+    forget_pre = column(heads + head) * scale + others[:, lanes : lanes + 1]
     log_forget = jnp.minimum(forget_pre, 0.0) - jnp.log(1.0 + jnp.exp(-jnp.abs(forget_pre)))
-    carried = log_forget + old_m[:, :1]
+    carried = log_forget + others[:, :1]
     top = jnp.maximum(carried, log_input)
     keep = jnp.exp(carried - top)
     admit = jnp.exp(log_input - top)
@@ -197,7 +202,8 @@
     reads = jnp.zeros((2 * rows, value_size), jnp.float32)
     for b in range(rows):
         one = jnp.where((row == b) | (row == b + rows), both, 0.0).astype(jnp.bfloat16)
-        reads += lax.dot_general(one, state_short[b, :value_size], nt_dims, preferred_element_type=jnp.float32)
+        block = state_short[b * value_size : (b + 1) * value_size]
+        reads += lax.dot_general(one, block, nt_dims, preferred_element_type=jnp.float32)
     numer = keep * (reads[:rows] + reads[rows:]) + match * value
     head_out = numer / ((1.0 + jnp.exp(-out_pre)) * denom)
     short = head_out.astype(jnp.bfloat16)
@@ -310,14 +316,14 @@
             pltpu.VMEM((lanes, width_dev), bf16),
             pltpu.SemaphoreType.DMA((8,)),
         ],
-        compiler_params=params(63),
+        compiler_params=params(60),
         cost_estimate=cost(2 * batch * width_dev * proj_width, 2 * width_dev * proj_width),
         name="project",
     )(tokens, attn_gain.reshape(1, width_dev), w_query, w_key, w_value, w_outgate, w_gates.T)
     state_short, w_output_near = pl.pallas_call(
         near_kernel,
         out_shape=(
-            jax.ShapeDtypeStruct((rows, value_size + extra_rows, query_size), bf16),
+            jax.ShapeDtypeStruct((rows * (value_size + 6), query_size), bf16),
             jax.ShapeDtypeStruct(w_output.shape, w_output.dtype),
         ),
         in_specs=[hbm] * 5,
@@ -350,7 +356,7 @@
         in_specs=[vmem] * 2,
         out_specs=[vmem] * 3,
         compiler_params=params(8),
-        cost_estimate=cost(10**8, 4 * rows * value_size * query_size),
+        cost_estimate=cost(10**10, 4 * rows * value_size * query_size),
         name="cell",
     )(arrived, state_short)
     half_rows = rows // 2

time: 86 us -> 83.7 us (0.973)
  waiting for transfers between devices: 9.55 us -> 7.48 us
  starting transfers between devices: 21.2 us -> 23 us
  Pallas kernels: 12.8 us -> 11.7 us
    ppermute x8, waiting for transfers between devices: 5.18 us -> 3.15 us  [swapped(): lax.ppermute(value, axis, [(i, i ^ bits) for i in range(lax.axis_size(axi...]
    ppermute x8, starting transfers between devices: 12.6 us -> 14.4 us  [swapped(): lax.ppermute(value, axis, [(i, i ^ bits) for i in range(lax.axis_size(axi...]
    pallas_call x1, Pallas kernels: 1.84 us -> 0.72 us  [per_device(): pl.pallas_call(functools.partial(cell_kernel, width_all, heads_all), out_...]
  transfers between devices with their start and end apart: 9 -> 9, of which waited for: 6 -> 5; matrix products, arithmetic and copies ran while one was open for 0% -> 0% of each run, Pallas kernels for 9% -> 10%
where the time goes in v7:
time: 83.7 us; the launch traced here: 83.1 us
  blocking collectives  35.5 us (42%)
  starting transfers between devices  23 us (27%)
  Pallas kernels  11.7 us (14%)
  waiting for transfers between devices  7.48 us (9%)
  local copies, waits for them, and re-layouts  3.01 us (4%)
  other arithmetic  1.1 us (1%)
    all_to_all x3, blocking collectives, exchange(): return lax.all_to_all(value, axis, split_axis=0, concat_axis=0, tiled=True)  35.5 us
    ppermute x8, starting transfers between devices, swapped(): lax.ppermute(value, axis, [(i, i ^ bits) for i in range(lax.axis_size(axi...  14.4 us
    all_to_all x1, starting transfers between devices, exchange(): return lax.all_to_all(value, axis, split_axis=0, concat_axis=0, tiled=True)  8.6 us
    pallas_call x2, Pallas kernels, written(): pl.pallas_call(functools.partial(write_kernel, first), out_shape=(jax.Sha...  5.72 us
    all_to_all x1, waiting for transfers between devices, exchange(): return lax.all_to_all(value, axis, split_axis=0, concat_axis=0, tiled=True)  4.33 us
    ppermute x8, waiting for transfers between devices, swapped(): lax.ppermute(value, axis, [(i, i ^ bits) for i in range(lax.axis_size(axi...  3.15 us
    unnamed x18, local copies, waits for them, and re-layouts  2.99 us
    pallas_call x1, Pallas kernels, per_device(): pl.pallas_call(project_kernel, out_shape=jax.ShapeDtypeStruct((batch, pro...  2.4 us
  transfers between devices with their start and end apart: 9, of which 5 were waited for; matrix products, arithmetic and copies ran while one was open for 0% of the time, Pallas kernels for 10%

profile of v7, /device:TPU:1, one launch (start us, length us, event | category | flops | bytes accessed | tf_op | source)
XLA Modules:
  0.0 83.1 jit_solution(1671606972235334362)
XLA Ops:
  0.6 2.4 %project.1 = bf16[128,1664]{1,0:T(8,128)(2,1)} custom-call(bf16[128,256]{1,0:T(8,128)(2,1)} %tok.1, f32[1,256]{1,0:T(1,128)} %bitcast.26, bf16[256,256]{1,0:T(8,128)(2,1)} %w_query.1, bf16[256,256]{1,0:T(8,128)(2,1)} %w_key.1, bf16[256,512]{1,0:T(8,128)(2,1)} %w_value.1, bf16[256,512]{1,0:T(8,128)(2,1)} %w_outgate.1, bf16[16,4096]{1,0:T(8,128)(2,1)} %bitcast.25), custom_call_target="tpu_custom_call" | custom-call | flops 100663296 | bytes 786432 | tf_op jit(solution)/shard_map/project/pallas_call | solution.py:307
  3.1 8.6 %all-to-all-start = ((bf16[16,8,1664]{2,1,0:T(8,128)(2,1)}), bf16[16,8,1664]{2,1,0:T(8,128)(2,1)S(1)}, u32[]{:S(2)}, u32[]{:S(2)}) async-start(bf16[16,8,1664]{2,1,0:T(8,128)(2,1)} %bitcast.24), calls=%async_computation | async-start | bytes 851968 | tf_op jit(solution)/shard_map/all_to_all | solution.py:60
  11.7 0.9 %copy-done.3 = bf16[512,256]{1,0:T(8,128)(2,1)S(1)} copy-done((bf16[512,256]{1,0:T(8,128)(2,1)S(1)}, bf16[512,256]{1,0:T(8,128)(2,1)}, u32[]{:S(2)}) %copy-start.3) | copy-done | bytes 262168
  12.6 0.7 copy-done.5
  13.3 0.7 copy-done.7
  14.0 0.7 copy-done.8
  14.6 2.3 %near.1 = (bf16[4144,256]{1,0:T(8,128)(2,1)S(1)}, bf16[512,256]{1,0:T(8,128)(2,1)S(1)}) custom-call(f32[8,1,512,256]{3,2,1,0:T(8,128)} %state.5, bf16[512,256]{1,0:T(8,128)(2,1)S(1)} %copy-done.3, f32[8,1,256]{2,1,0:T(1,128)S(1)} %copy-done.5, f32[1,8]{1,0:T(1,128)S(1)} %bitcast.22, f32[1,8]{1,0:T(1,128)S(1)} %bitcast.23), custom_call_target="tpu_custom_call" | custom-call | flops 1000000000 | bytes 6291456 | tf_op jit(solution)/shard_map/near/pallas_call | solution.py:323
  16.9 4.3 %all-to-all-done.arrived = bf16[16,8,1664]{2,1,0:T(8,128)(2,1)S(1)} async-done(((bf16[16,8,1664]{2,1,0:T(8,128)(2,1)}), bf16[16,8,1664]{2,1,0:T(8,128)(2,1)S(1)}, u32[]{:S(2)}, u32[]{:S(2)}) %all-to-all-start) | async-done | bytes 426016 | tf_op jit(solution)/shard_map/all_to_all | solution.py:60
  21.2 0.7 cell.1
  22.0 9.9 %all_to_all.20 = bf16[16,8,512]{2,1,0:T(8,128)(2,1)S(1)} all-to-all(bf16[16,8,512]{2,1,0:T(8,128)(2,1)S(1)} %get-tuple-element.17), channel_id=1, replica_groups=mesh['z'=4,'y'=4,'x'=4,'core'=2] {'z','y'}, dimensions={0} | all-to-all | bytes 262144 | tf_op jit(solution)/shard_map/all_to_all | solution.py:60
  32.1 3.0 %collective-permute-start = (bf16[128,256]{1,0:T(8,128)(2,1)S(1)}, bf16[128,256]{1,0:T(8,128)(2,1)S(1)}, u32[]{:S(2)}, u32[]{:S(2)}) collective-permute-start(bf16[128,256]{1,0:T(8,128)(2,1)S(1)} %convolution_convert_fusion.1), channel_id=1, source_target_pairs={{0,1},{1,0},{2,3},{3,2},{4,5},{5,4},{6,7},{7,6},{8,9},{9,8},{10,11... | collective-permute-start | bytes 196616 | tf_op jit(solution)/shard_map/ppermute | solution.py:69
  35.2 0.9 %collective-permute-done = bf16[128,256]{1,0:T(8,128)(2,1)S(1)} collective-permute-done((bf16[128,256]{1,0:T(8,128)(2,1)S(1)}, bf16[128,256]{1,0:T(8,128)(2,1)S(1)}, u32[]{:S(2)}, u32[]{:S(2)}) %collective-permute-start) | collective-permute-done | bytes 65568 | tf_op jit(solution)/shard_map/ppermute | solution.py:69
  36.1 2.6 %collective-permute-start.3 = (bf16[128,256]{1,0:T(8,128)(2,1)S(1)}, bf16[128,256]{1,0:T(8,128)(2,1)S(1)}, u32[]{:S(2)}, u32[]{:S(2)}) collective-permute-start(bf16[128,256]{1,0:T(8,128)(2,1)S(1)} %add_convert_fusion.2.term_0), channel_id=1, source_target_pairs={{0,6},{2,4},{4,2},{6,0},{1,7},{3,5},{5,3},{7,1},{8,14},{10,12},{12... | collective-permute-start | bytes 196616 | tf_op jit(solution)/shard_map/ppermute | solution.py:69
  39.4 2.6 %write_state.2 = (f32[8,1,512,256]{3,2,1,0:T(8,128)}, f32[8,128]{1,0:T(8,128)S(1)}) custom-call(f32[8,640]{1,0:T(8,128)S(1)} %get-tuple-element.19.to_write, f32[8,512]{1,0:T(8,128)S(1)} %get-tuple-element.20.value, f32[8,1,512,256]{3,2,1,0:T(8,128)} %state.5), custom_call_target="tpu_custom_call" | custom-call | flops 1000000000 | bytes 4194304 | tf_op jit(solution)/shard_map/write_state/pallas_call | solution.py:365
  42.0 1.3 %collective-permute-done.2.term_2 = bf16[128,256]{1,0:T(8,128)(2,1)S(1)} collective-permute-done((bf16[128,256]{1,0:T(8,128)(2,1)S(1)}, bf16[128,256]{1,0:T(8,128)(2,1)S(1)}, u32[]{:S(2)}, u32[]{:S(2)}) %collective-permute-start.2) | collective-permute-done | bytes 65568 | tf_op jit(solution)/shard_map/ppermute | solution.py:69
  43.3 0.6 widen.1
  43.9 14.2 %all_to_all.21 = bf16[16,8,2816]{2,1,0:T(8,128)(2,1)S(1)} all-to-all(bf16[16,8,2816]{2,1,0:T(8,128)(2,1)S(1)} %bitcast.18), channel_id=1, replica_groups=mesh['z'=4,'y'=4,'x'=4,'core'=2] {'z','y'}, dimensions={0} | all-to-all | bytes 1441792 | tf_op jit(solution)/shard_map/all_to_all | solution.py:60
  58.5 11.4 %all_to_all.22 = bf16[16,8,1376]{2,1,0:T(8,128)(2,1)S(1)} all-to-all(bf16[16,8,1376]{2,1,0:T(8,128)(2,1)S(1)} %broadcast_in_dim.3), channel_id=1, replica_groups=mesh['z'=4,'y'=4,'x'=4,'core'=2] {'z','y'}, dimensions={0} | all-to-all | bytes 704512 | tf_op jit(solution)/shard_map/all_to_all | solution.py:60
  70.2 4.1 %collective-permute-start.4 = (bf16[128,256]{1,0:T(8,128)(2,1)S(1)}, bf16[128,256]{1,0:T(8,128)(2,1)S(1)}, u32[]{:S(2)}, u32[]{:S(2)}) collective-permute-start(bf16[128,256]{1,0:T(8,128)(2,1)S(1)} %convolution_convert_fusion), channel_id=1, source_target_pairs={{0,1},{1,0},{2,3},{3,2},{4,5},{5,4},{6,7},{7,6},{8,9},{9,8},{10,11... | collective-permute-start | bytes 196616 | tf_op jit(solution)/shard_map/ppermute | solution.py:69
  74.3 0.9 %collective-permute-done.4 = bf16[128,256]{1,0:T(8,128)(2,1)S(1)} collective-permute-done((bf16[128,256]{1,0:T(8,128)(2,1)S(1)}, bf16[128,256]{1,0:T(8,128)(2,1)S(1)}, u32[]{:S(2)}, u32[]{:S(2)}) %collective-permute-start.4) | collective-permute-done | bytes 65568 | tf_op jit(solution)/shard_map/ppermute | solution.py:69
  75.2 1.7 %collective-permute-start.7 = (bf16[128,256]{1,0:T(8,128)(2,1)S(1)}, bf16[128,256]{1,0:T(8,128)(2,1)S(1)}, u32[]{:S(2)}, u32[]{:S(2)}) collective-permute-start(bf16[128,256]{1,0:T(8,128)(2,1)S(1)} %add_convert_fusion.1), channel_id=1, source_target_pairs={{0,6},{2,4},{4,2},{6,0},{1,7},{3,5},{5,3},{7,1},{8,14},{10,12},{12... | collective-permute-start | bytes 196616 | tf_op jit(solution)/shard_map/ppermute | solution.py:69
  77.2 2.0 %collective-permute-start.5 = (bf16[128,256]{1,0:T(8,128)(2,1)S(1)}, bf16[128,256]{1,0:T(8,128)(2,1)S(1)}, u32[]{:S(2)}, u32[]{:S(2)}) collective-permute-start(bf16[128,256]{1,0:T(8,128)(2,1)S(1)} %add_convert_fusion.1), channel_id=1, source_target_pairs={{0,4},{2,6},{4,0},{6,2},{1,5},{3,7},{5,1},{7,3},{8,12},{10,14},{12... | collective-permute-start | bytes 196616 | tf_op jit(solution)/shard_map/ppermute | solution.py:69
  79.2 3.2 %write_state.3 = (f32[8,1,512,256]{3,2,1,0:T(8,128)}, f32[8,1,256]{2,1,0:T(1,128)}, f32[1,8]{1,0:T(1,128)}) custom-call(f32[8,640]{1,0:T(8,128)S(1)} %get-tuple-element.19.to_write, f32[8,512]{1,0:T(8,128)S(1)} %get-tuple-element.20.value, f32[8,1,512,256]{3,2,1,0:T(8,128)} %state.5, ...), custom_call_target="tpu_custom_call", output_to_operand_aliasing={{0}: (3, {})} | custom-call | flops 1000000000 | bytes 4194304 | tf_op jit(solution)/shard_map/write_state/pallas_call | solution.py:365
  82.4 0.7 add_convert_fusion
  (30 shorter events, 2.1 us)
Async XLA Ops:
  0.6 69.3 %copy-start = (bf16[1376,256]{1,0:T(8,128)(2,1)S(1)}, bf16[1376,256]{1,0:T(8,128)(2,1)}, u32[]{:S(2)}) copy-start(bf16[1376,256]{1,0:T(8,128)(2,1)} %param.31) | copy-start | bytes 2113540
  3.1 18.2 %all-to-all-start = ((bf16[16,8,1664]{2,1,0:T(8,128)(2,1)}), bf16[16,8,1664]{2,1,0:T(8,128)(2,1)S(1)}, u32[]{:S(2)}, u32[]{:S(2)}) async-start(bf16[16,8,1664]{2,1,0:T(8,128)(2,1)} %bitcast.24), calls=%async_computation | async-start | bytes 851968 | tf_op jit(solution)/shard_map/all_to_all | solution.py:60
  11.7 1.0 %copy-start.3 = (bf16[512,256]{1,0:T(8,128)(2,1)S(1)}, bf16[512,256]{1,0:T(8,128)(2,1)}, u32[]{:S(2)}) copy-start(bf16[512,256]{1,0:T(8,128)(2,1)} %weight.1) | copy-start | bytes 786436
  12.6 0.7 copy-start.5
  13.3 0.7 copy-start.7
  14.0 0.7 copy-start.8
  22.0 21.3 %copy-start.1 = (bf16[256,1376]{0,1:T(8,128)(2,1)S(1)}, bf16[256,1376]{0,1:T(8,128)(2,1)}, u32[]{:S(2)}) copy-start(bf16[256,1376]{0,1:T(8,128)(2,1)} %param.29) | copy-start | bytes 2113540
  22.0 21.3 %copy-start.2 = (bf16[256,1376]{0,1:T(8,128)(2,1)S(1)}, bf16[256,1376]{0,1:T(8,128)(2,1)}, u32[]{:S(2)}) copy-start(bf16[256,1376]{0,1:T(8,128)(2,1)} %param.30) | copy-start | bytes 2113540
  22.0 21.3 %copy-start.4 = (bf16[128,256]{1,0:T(8,128)(2,1)S(1)}, bf16[128,256]{1,0:T(8,128)(2,1)}, u32[]{:S(2)}) copy-start(bf16[128,256]{1,0:T(8,128)(2,1)} %tok.1) | copy-start | bytes 196612
  22.0 21.3 %copy-start.6 = (f32[256]{0:T(256)S(1)}, f32[256]{0:T(256)}, u32[]{:S(2)}) copy-start(f32[256]{0:T(256)} %param.28) | copy-start | bytes 3076
  32.1 3.9 %collective-permute-start = (bf16[128,256]{1,0:T(8,128)(2,1)S(1)}, bf16[128,256]{1,0:T(8,128)(2,1)S(1)}, u32[]{:S(2)}, u32[]{:S(2)}) collective-permute-start(bf16[128,256]{1,0:T(8,128)(2,1)S(1)} %convolution_convert_fusion.1), channel_id=1, source_target_pairs={{0,1},{1,0},{2,3},{3,2},{4,5},{5,4},{6,7},{7,6},{8,9},{9,8},{10,11... | collective-permute-start | bytes 196616 | tf_op jit(solution)/shard_map/ppermute | solution.py:69
  36.1 5.9 %collective-permute-start.3 = (bf16[128,256]{1,0:T(8,128)(2,1)S(1)}, bf16[128,256]{1,0:T(8,128)(2,1)S(1)}, u32[]{:S(2)}, u32[]{:S(2)}) collective-permute-start(bf16[128,256]{1,0:T(8,128)(2,1)S(1)} %add_convert_fusion.2.term_0), channel_id=1, source_target_pairs={{0,6},{2,4},{4,2},{6,0},{1,7},{3,5},{5,3},{7,1},{8,14},{10,12},{12... | collective-permute-start | bytes 196616 | tf_op jit(solution)/shard_map/ppermute | solution.py:69
  38.6 4.6 %collective-permute-start.2 = (bf16[128,256]{1,0:T(8,128)(2,1)S(1)}, bf16[128,256]{1,0:T(8,128)(2,1)S(1)}, u32[]{:S(2)}, u32[]{:S(2)}) collective-permute-start(bf16[128,256]{1,0:T(8,128)(2,1)S(1)} %add_convert_fusion.2.term_0), channel_id=1, source_target_pairs={{0,4},{2,6},{4,0},{6,2},{1,5},{3,7},{5,1},{7,3},{8,12},{10,14},{12... | collective-permute-start | bytes 196616 | tf_op jit(solution)/shard_map/ppermute | solution.py:69
  39.2 4.1 %collective-permute-start.1 = (bf16[128,256]{1,0:T(8,128)(2,1)S(1)}, bf16[128,256]{1,0:T(8,128)(2,1)S(1)}, u32[]{:S(2)}, u32[]{:S(2)}) collective-permute-start(bf16[128,256]{1,0:T(8,128)(2,1)S(1)} %add_convert_fusion.2.term_0), channel_id=1, source_target_pairs={{0,2},{2,0},{4,6},{6,4},{1,3},{3,1},{5,7},{7,5},{8,10},{10,8},{12,... | collective-permute-start | bytes 196616 | tf_op jit(solution)/shard_map/ppermute | solution.py:69
  70.2 5.0 %collective-permute-start.4 = (bf16[128,256]{1,0:T(8,128)(2,1)S(1)}, bf16[128,256]{1,0:T(8,128)(2,1)S(1)}, u32[]{:S(2)}, u32[]{:S(2)}) collective-permute-start(bf16[128,256]{1,0:T(8,128)(2,1)S(1)} %convolution_convert_fusion), channel_id=1, source_target_pairs={{0,1},{1,0},{2,3},{3,2},{4,5},{5,4},{6,7},{7,6},{8,9},{9,8},{10,11... | collective-permute-start | bytes 196616 | tf_op jit(solution)/shard_map/ppermute | solution.py:69
  75.2 7.1 %collective-permute-start.7 = (bf16[128,256]{1,0:T(8,128)(2,1)S(1)}, bf16[128,256]{1,0:T(8,128)(2,1)S(1)}, u32[]{:S(2)}, u32[]{:S(2)}) collective-permute-start(bf16[128,256]{1,0:T(8,128)(2,1)S(1)} %add_convert_fusion.1), channel_id=1, source_target_pairs={{0,6},{2,4},{4,2},{6,0},{1,7},{3,5},{5,3},{7,1},{8,14},{10,12},{12... | collective-permute-start | bytes 196616 | tf_op jit(solution)/shard_map/ppermute | solution.py:69
  76.9 5.5 %collective-permute-start.6 = (bf16[128,256]{1,0:T(8,128)(2,1)S(1)}, bf16[128,256]{1,0:T(8,128)(2,1)S(1)}, u32[]{:S(2)}, u32[]{:S(2)}) collective-permute-start(bf16[128,256]{1,0:T(8,128)(2,1)S(1)} %add_convert_fusion.1), channel_id=1, source_target_pairs={{0,2},{2,0},{4,6},{6,4},{1,3},{3,1},{5,7},{7,5},{8,10},{10,8},{12,... | collective-permute-start | bytes 196616 | tf_op jit(solution)/shard_map/ppermute | solution.py:69
  77.2 5.2 %collective-permute-start.5 = (bf16[128,256]{1,0:T(8,128)(2,1)S(1)}, bf16[128,256]{1,0:T(8,128)(2,1)S(1)}, u32[]{:S(2)}, u32[]{:S(2)}) collective-permute-start(bf16[128,256]{1,0:T(8,128)(2,1)S(1)} %add_convert_fusion.1), channel_id=1, source_target_pairs={{0,4},{2,6},{4,0},{6,2},{1,5},{3,7},{5,1},{7,3},{8,12},{10,14},{12... | collective-permute-start | bytes 196616 | tf_op jit(solution)/shard_map/ppermute | solution.py:69

commit v8 on v7

--- a/solution.py
+++ b/solution.py
@@ -60,11 +60,6 @@
     return lax.all_to_all(value, axis, split_axis=0, concat_axis=0, tiled=True)
 
 
-def sent_to_all(value, axis):
-    copies = jnp.broadcast_to(value, (lax.axis_size(axis), *value.shape))
-    return exchange(copies, axis)
-
-
 def swapped(value, axis, bits):
     return lax.ppermute(value, axis, [(i, i ^ bits) for i in range(lax.axis_size(axis))])
 
@@ -88,22 +83,43 @@
 
 
 def project_kernel(
-    tokens, gain_in, w_query, w_key, w_value, w_outgate, gates_t, sent, tok, gain, weights, gate_rows, sems
+    tokens,
+    gain_in,
+    w_query,
+    w_key,
+    w_value,
+    w_outgate,
+    gates_t,
+    sent,
+    tok,
+    gain,
+    weights,
+    gate_rows,
+    held,
+    sems,
+    out_sems,
 ):
     width = tok.shape[1]
     gates = gates_t.shape[0]
     moves = [(tokens, tok), (gain_in, gain)]
-    at = 0
-    for source in (w_query, w_key, w_value, w_outgate):
-        columns = source.shape[1]
-        moves.append((source, weights.at[:, pl.ds(at, columns)]))
-        at += columns
     mine = pl.ds(pl.multiple_of(index_of(kv) * width, width), width)
     for row in (0, low_at):
         moves.append((gates_t.at[:, mine], gate_rows.at[pl.ds(row, gates), :]))
+    spans = []
+    at = 0
+    for source in (w_query, w_key, w_value, w_outgate):
+        span = pl.ds(at, source.shape[1])
+        moves.append((source, weights.at[:, span]))
+        spans.append(span)
+        at += source.shape[1]
+    spans.append(pl.ds(at, lanes))
     copies = [pltpu.make_async_copy(*move, sems.at[i]) for i, move in enumerate(moves)]
     for copy in copies:
         copy.start()
+    away = [
+        pltpu.make_async_copy(held.at[:, span], sent.at[:, span], out_sems.at[i])
+        for i, span in enumerate(spans)
+    ]
     for start, end in ((gates, low_at), (low_at + gates, lanes)):
         gate_rows[start:end, :] = jnp.zeros((end - start, width), gate_rows.dtype)
     for copy in copies[:2]:
@@ -111,17 +127,23 @@
     values = tok[...].astype(jnp.float32)
     squares = jnp.sum(values * values, axis=1, keepdims=True)
     normed = (values * gain[...]).astype(jnp.bfloat16)
-    for copy in copies[2:]:
+    for copy in copies[2:4]:
         copy.wait()
-    product = jnp.dot(normed, weights[...], preferred_element_type=jnp.float32)
-    sent[:, :at] = product.astype(jnp.bfloat16)
     extra = lax.dot_general(normed, gate_rows[...], nt_dims, preferred_element_type=jnp.float32)
     lane = lane_ids(extra.shape)
     extra = jnp.where((lane == gates) | (lane == low_at + gates), squares, extra)
     high, low = split_pair(extra)
-    sent[:, at:] = jnp.where(lane < low_at, high.astype(jnp.float32), low.astype(jnp.float32)).astype(
+    held[:, at:] = jnp.where(lane < low_at, high.astype(jnp.float32), low.astype(jnp.float32)).astype(
         jnp.bfloat16
     )
+    away[4].start()
+    for copy, span, leave in zip(copies[4:], spans, away):
+        copy.wait()
+        product = jnp.dot(normed, weights[:, span], preferred_element_type=jnp.float32)
+        held[:, span] = product.astype(jnp.bfloat16)
+        leave.start()
+    for leave in away:
+        leave.wait()
 
 
 def near_kernel(
@@ -217,20 +239,12 @@
 
 
 def write_kernel(first, to_write, value, state, *refs):
-    outputs, held, sems_in, sems_out = refs[:-3], *refs[-3:]
-    count, _, query_size = held.shape
     if first == 0:
-        new_c, order = outputs
+        new_c, order, held, sems_in, sems_out = refs
         order[...] = jnp.zeros_like(order)
     else:
-        _, new_c, new_n, new_m = outputs
-        new_n[...] = to_write[:, lanes + query_size :].reshape(new_n.shape)
-        rows = to_write.shape[0]
-        square = (rows, rows)
-        top = jnp.broadcast_to(to_write[:, 1:2], square)
-        new_m[...] = jnp.sum(
-            jnp.where(row_ids(square) == lane_ids(square), top, 0.0), axis=0, keepdims=True
-        )
+        _, new_c, new_n, new_m, held, sems_in, sems_out, held_n, held_m = refs
+    count, _, query_size = held.shape
     into = [
         pltpu.make_async_copy(state.at[first + b, 0], held.at[b], sems_in.at[b])
         for b in range(count)
@@ -241,6 +255,18 @@
     ]
     for copy in into:
         copy.start()
+    if first > 0:
+        held_n[...] = to_write[:, lanes + query_size :].reshape(held_n.shape)
+        rows = to_write.shape[0]
+        square = (rows, rows)
+        top = jnp.broadcast_to(to_write[:, 1:2], square)
+        held_m[...] = jnp.sum(
+            jnp.where(row_ids(square) == lane_ids(square), top, 0.0), axis=0, keepdims=True
+        )
+        out.append(pltpu.make_async_copy(held_n, new_n, sems_out.at[count]))
+        out.append(pltpu.make_async_copy(held_m, new_m, sems_out.at[count + 1]))
+        for copy in out[count:]:
+            copy.start()
     across = value[...].T
     for b in range(count):
         row = first + b
@@ -275,6 +301,23 @@
         product = lax.dot_general(normed, weight[...], nt_dims, preferred_element_type=jnp.float32)
         whole = jnp.concatenate([product, tail], axis=1)
         sent[:, at : at + half] = whole.astype(jnp.bfloat16)
+
+
+def hidden_kernel(width_all, hidden, arrived, sent):
+    half = arrived.shape[2] // 2
+    total = arrived[0].astype(jnp.float32)
+    for i in range(1, arrived.shape[0]):
+        total = total + arrived[i].astype(jnp.float32)
+    at = half + hidden
+    last = total[:, 2 * half - lanes :]
+    lane = lane_ids(last.shape) - (at - (2 * half - lanes))
+    squares = jnp.sum(jnp.where((lane == 0) | (lane == 1), last, 0.0), axis=1, keepdims=True)
+    scale = lax.rsqrt(squares / width_all + norm_floor)
+    gate = total[:, :half] * scale
+    up = total[:, half:] * scale
+    short = (gate / (1.0 + jnp.exp(-gate)) * up).astype(jnp.bfloat16)[:, :hidden]
+    for i in range(sent.shape[0]):
+        sent[i] = short
 
 
 def per_device(
@@ -308,13 +351,15 @@
         project_kernel,
         out_shape=jax.ShapeDtypeStruct((batch, proj_width + lanes), bf16),
         in_specs=[hbm] * 7,
-        out_specs=vmem,
+        out_specs=hbm,
         scratch_shapes=[
             pltpu.VMEM((batch, width_dev), bf16),
             pltpu.VMEM((1, width_dev), f32),
             pltpu.VMEM((width_dev, proj_width), bf16),
             pltpu.VMEM((lanes, width_dev), bf16),
+            pltpu.VMEM((batch, proj_width + lanes), bf16),
             pltpu.SemaphoreType.DMA((8,)),
+            pltpu.SemaphoreType.DMA((5,)),
         ],
         compiler_params=params(60),
         cost_estimate=cost(2 * batch * width_dev * proj_width, 2 * width_dev * proj_width),
@@ -361,27 +406,30 @@
     )(arrived, state_short)
     half_rows = rows // 2
 
-    def written(first, extra, *begun):
+    def written(first, extra, spec, scratch, *begun):
         return pl.pallas_call(
             functools.partial(write_kernel, first),
             out_shape=(jax.ShapeDtypeStruct(state_c.shape, f32), *extra),
             in_specs=[vmem, vmem, hbm] + [hbm] * len(begun),
-            out_specs=(hbm,) + (vmem,) * len(extra),
+            out_specs=(hbm,) + (spec,) * len(extra),
             input_output_aliases={3: 0} if begun else {},
             scratch_shapes=[
                 pltpu.VMEM((half_rows, value_size, query_size), f32),
                 pltpu.SemaphoreType.DMA((half_rows,)),
-                pltpu.SemaphoreType.DMA((half_rows,)),
+                pltpu.SemaphoreType.DMA((half_rows + len(scratch),)),
+                *scratch,
             ],
             compiler_params=params(50),
             cost_estimate=cost(10**9, 4 * rows * value_size * query_size),
             name="write_state",
         )(to_write, value, state_c, *begun)
 
-    begun_c, order = written(0, (jax.ShapeDtypeStruct((8, lanes), f32),))
+    begun_c, order = written(0, (jax.ShapeDtypeStruct((8, lanes), f32),), vmem, ())
     new_c, new_n, new_m = written(
         half_rows,
         (jax.ShapeDtypeStruct(state_n.shape, f32), jax.ShapeDtypeStruct((1, rows), f32)),
+        hbm,
+        (pltpu.VMEM(state_n.shape, f32), pltpu.VMEM((1, rows), f32)),
         begun_c,
     )
     heads_rows = exchange(head_copies, kv).reshape(batch, value_size)
@@ -409,15 +457,16 @@
     )
     mid_float = middle.astype(f32)
     arrived = exchange(sent.reshape(kv_count, rows, 2 * hidden_pad), kv)
-    summed = arrived.astype(jnp.float32).sum(axis=0)
-    at = hidden_pad + hidden_dev
-    rows_two = summed[:, at : at + 1] + summed[:, at + 1 : at + 2]
-    scale_two = lax.rsqrt(rows_two / width_all + norm_floor)
-    hidden_ff = (
-        jax.nn.silu(summed[:, :hidden_dev] * scale_two)
-        * (summed[:, hidden_pad : hidden_pad + hidden_dev] * scale_two)
-    ).astype(jnp.bfloat16)
-    hidden_rows = sent_to_all(hidden_ff, kv).reshape(batch, hidden_dev)
+    hidden_copies = pl.pallas_call(
+        functools.partial(hidden_kernel, width_all, hidden_dev),
+        out_shape=jax.ShapeDtypeStruct((kv_count, rows, hidden_dev), bf16),
+        in_specs=[vmem],
+        out_specs=vmem,
+        compiler_params=params(8),
+        cost_estimate=cost(10**6, 4 * kv_count * rows * hidden_pad),
+        name="hidden",
+    )(arrived)
+    hidden_rows = exchange(hidden_copies, kv).reshape(batch, hidden_dev)
     down_part = jnp.dot(hidden_rows, w_downff, preferred_element_type=jnp.float32)
     mixed = (mid_float + in_order(over_tp(down_part))).astype(jnp.bfloat16)
     return (mixed, new_c, new_n, new_m.reshape(rows, 1))

time: 83.7 us -> 83.8 us (level)
  transfers between devices with their start and end apart: 9 -> 9, of which waited for: 5 -> 5; matrix products, arithmetic and copies ran while one was open for 0% -> 0% of each run, Pallas kernels for 10% -> 9%
where the time goes in v8:
time: 83.8 us; the launch traced here: 83.1 us
  blocking collectives  35.5 us (42%)
  starting transfers between devices  23 us (27%)
  Pallas kernels  11.6 us (14%)
  waiting for transfers between devices  8.05 us (10%)
  local copies, waits for them, and re-layouts  2.99 us (4%)
    all_to_all x3, blocking collectives, exchange(): return lax.all_to_all(value, axis, split_axis=0, concat_axis=0, tiled=True)  35.5 us
    ppermute x8, starting transfers between devices, swapped(): lax.ppermute(value, axis, [(i, i ^ bits) for i in range(lax.axis_size(axi...  14.4 us
    all_to_all x1, starting transfers between devices, exchange(): return lax.all_to_all(value, axis, split_axis=0, concat_axis=0, tiled=True)  8.6 us
    pallas_call x2, Pallas kernels, written(): pl.pallas_call(functools.partial(write_kernel, first), out_shape=(jax.Sha...  5.15 us
    all_to_all x1, waiting for transfers between devices, exchange(): return lax.all_to_all(value, axis, split_axis=0, concat_axis=0, tiled=True)  4.33 us
    ppermute x8, waiting for transfers between devices, swapped(): lax.ppermute(value, axis, [(i, i ^ bits) for i in range(lax.axis_size(axi...  3.72 us
    unnamed x18, local copies, waits for them, and re-layouts  2.99 us
    pallas_call x1, Pallas kernels, per_device(): pl.pallas_call(project_kernel, out_shape=jax.ShapeDtypeStruct((batch, pro...  2.73 us
  transfers between devices with their start and end apart: 9, of which 5 were waited for; matrix products, arithmetic and copies ran while one was open for 0% of the time, Pallas kernels for 9%

profile of v8, /device:TPU:1, one launch (start us, length us, event | category | flops | bytes accessed | tf_op | source)
XLA Modules:
  0.0 83.1 jit_solution(11826891465559918105)
XLA Ops:
  0.6 2.7 %project.1 = bf16[128,1664]{1,0:T(8,128)(2,1)} custom-call(bf16[128,256]{1,0:T(8,128)(2,1)} %tok.1, f32[1,256]{1,0:T(1,128)} %bitcast.26, bf16[256,256]{1,0:T(8,128)(2,1)} %w_query.1, bf16[256,256]{1,0:T(8,128)(2,1)} %w_key.1, bf16[256,512]{1,0:T(8,128)(2,1)} %w_value.1, bf16[256,512]{1,0:T(8,128)(2,1)} %w_outgate.1, bf16[16,4096]{1,0:T(8,128)(2,1)} %bitcast.25), custom_call_target="tpu_custom_call" | custom-call | flops 100663296 | bytes 786432 | tf_op jit(solution)/shard_map/project/pallas_call | solution.py:350
  3.4 8.6 %all-to-all-start = ((bf16[16,8,1664]{2,1,0:T(8,128)(2,1)}), bf16[16,8,1664]{2,1,0:T(8,128)(2,1)S(1)}, u32[]{:S(2)}, u32[]{:S(2)}) async-start(bf16[16,8,1664]{2,1,0:T(8,128)(2,1)} %bitcast.24), calls=%async_computation | async-start | bytes 851968 | tf_op jit(solution)/shard_map/all_to_all | solution.py:60
  12.0 0.9 %copy-done.3 = bf16[512,256]{1,0:T(8,128)(2,1)S(1)} copy-done((bf16[512,256]{1,0:T(8,128)(2,1)S(1)}, bf16[512,256]{1,0:T(8,128)(2,1)}, u32[]{:S(2)}) %copy-start.3) | copy-done | bytes 262168
  12.9 0.7 copy-done.5
  13.6 0.7 copy-done.7
  14.3 0.7 copy-done.8
  15.0 2.3 %near.1 = (bf16[4144,256]{1,0:T(8,128)(2,1)S(1)}, bf16[512,256]{1,0:T(8,128)(2,1)S(1)}) custom-call(f32[8,1,512,256]{3,2,1,0:T(8,128)} %state.5, bf16[512,256]{1,0:T(8,128)(2,1)S(1)} %copy-done.3, f32[8,1,256]{2,1,0:T(1,128)S(1)} %copy-done.5, f32[1,8]{1,0:T(1,128)S(1)} %bitcast.22, f32[1,8]{1,0:T(1,128)S(1)} %bitcast.23), custom_call_target="tpu_custom_call" | custom-call | flops 1000000000 | bytes 6291456 | tf_op jit(solution)/shard_map/near/pallas_call | solution.py:368
  17.2 4.3 %all-to-all-done.arrived = bf16[16,8,1664]{2,1,0:T(8,128)(2,1)S(1)} async-done(((bf16[16,8,1664]{2,1,0:T(8,128)(2,1)}), bf16[16,8,1664]{2,1,0:T(8,128)(2,1)S(1)}, u32[]{:S(2)}, u32[]{:S(2)}) %all-to-all-start) | async-done | bytes 426016 | tf_op jit(solution)/shard_map/all_to_all | solution.py:60
  21.6 0.7 cell.1
  22.3 9.9 %all_to_all.20 = bf16[16,8,512]{2,1,0:T(8,128)(2,1)S(1)} all-to-all(bf16[16,8,512]{2,1,0:T(8,128)(2,1)S(1)} %get-tuple-element.17), channel_id=1, replica_groups=mesh['z'=4,'y'=4,'x'=4,'core'=2] {'z','y'}, dimensions={0} | all-to-all | bytes 262144 | tf_op jit(solution)/shard_map/all_to_all | solution.py:60
  32.4 3.0 %collective-permute-start = (bf16[128,256]{1,0:T(8,128)(2,1)S(1)}, bf16[128,256]{1,0:T(8,128)(2,1)S(1)}, u32[]{:S(2)}, u32[]{:S(2)}) collective-permute-start(bf16[128,256]{1,0:T(8,128)(2,1)S(1)} %convolution_convert_fusion.1), channel_id=1, source_target_pairs={{0,1},{1,0},{2,3},{3,2},{4,5},{5,4},{6,7},{7,6},{8,9},{9,8},{10,11... | collective-permute-start | bytes 196616 | tf_op jit(solution)/shard_map/ppermute | solution.py:64
  35.5 0.9 %collective-permute-done = bf16[128,256]{1,0:T(8,128)(2,1)S(1)} collective-permute-done((bf16[128,256]{1,0:T(8,128)(2,1)S(1)}, bf16[128,256]{1,0:T(8,128)(2,1)S(1)}, u32[]{:S(2)}, u32[]{:S(2)}) %collective-permute-start) | collective-permute-done | bytes 65568 | tf_op jit(solution)/shard_map/ppermute | solution.py:64
  36.4 2.6 %collective-permute-start.3 = (bf16[128,256]{1,0:T(8,128)(2,1)S(1)}, bf16[128,256]{1,0:T(8,128)(2,1)S(1)}, u32[]{:S(2)}, u32[]{:S(2)}) collective-permute-start(bf16[128,256]{1,0:T(8,128)(2,1)S(1)} %add_convert_fusion.2.term_0), channel_id=1, source_target_pairs={{0,6},{2,4},{4,2},{6,0},{1,7},{3,5},{5,3},{7,1},{8,14},{10,12},{12... | collective-permute-start | bytes 196616 | tf_op jit(solution)/shard_map/ppermute | solution.py:64
  39.7 2.6 %write_state.2 = (f32[8,1,512,256]{3,2,1,0:T(8,128)}, f32[8,128]{1,0:T(8,128)S(1)}) custom-call(f32[8,640]{1,0:T(8,128)S(1)} %get-tuple-element.19.to_write, f32[8,512]{1,0:T(8,128)S(1)} %get-tuple-element.20.value, f32[8,1,512,256]{3,2,1,0:T(8,128)} %state.5), custom_call_target="tpu_custom_call" | custom-call | flops 1000000000 | bytes 4194304 | tf_op jit(solution)/shard_map/write_state/pallas_call | solution.py:410
  42.3 1.3 %collective-permute-done.2.term_2 = bf16[128,256]{1,0:T(8,128)(2,1)S(1)} collective-permute-done((bf16[128,256]{1,0:T(8,128)(2,1)S(1)}, bf16[128,256]{1,0:T(8,128)(2,1)S(1)}, u32[]{:S(2)}, u32[]{:S(2)}) %collective-permute-start.2) | collective-permute-done | bytes 65568 | tf_op jit(solution)/shard_map/ppermute | solution.py:64
  44.2 14.2 %all_to_all.21.arrived = bf16[16,8,2816]{2,1,0:T(8,128)(2,1)S(1)} all-to-all(bf16[16,8,2816]{2,1,0:T(8,128)(2,1)S(1)} %bitcast.18), channel_id=1, replica_groups=mesh['z'=4,'y'=4,'x'=4,'core'=2] {'z','y'}, dimensions={0} | all-to-all | bytes 1441792 | tf_op jit(solution)/shard_map/all_to_all | solution.py:60
  58.6 11.4 %all_to_all.22 = bf16[16,8,1376]{2,1,0:T(8,128)(2,1)S(1)} all-to-all(bf16[16,8,1376]{2,1,0:T(8,128)(2,1)S(1)} %hidden.1), channel_id=1, replica_groups=mesh['z'=4,'y'=4,'x'=4,'core'=2] {'z','y'}, dimensions={0} | all-to-all | bytes 704512 | tf_op jit(solution)/shard_map/all_to_all | solution.py:60
  70.3 4.1 %collective-permute-start.4 = (bf16[128,256]{1,0:T(8,128)(2,1)S(1)}, bf16[128,256]{1,0:T(8,128)(2,1)S(1)}, u32[]{:S(2)}, u32[]{:S(2)}) collective-permute-start(bf16[128,256]{1,0:T(8,128)(2,1)S(1)} %convolution_convert_fusion), channel_id=1, source_target_pairs={{0,1},{1,0},{2,3},{3,2},{4,5},{5,4},{6,7},{7,6},{8,9},{9,8},{10,11... | collective-permute-start | bytes 196616 | tf_op jit(solution)/shard_map/ppermute | solution.py:64
  74.3 0.9 %collective-permute-done.4 = bf16[128,256]{1,0:T(8,128)(2,1)S(1)} collective-permute-done((bf16[128,256]{1,0:T(8,128)(2,1)S(1)}, bf16[128,256]{1,0:T(8,128)(2,1)S(1)}, u32[]{:S(2)}, u32[]{:S(2)}) %collective-permute-start.4) | collective-permute-done | bytes 65568 | tf_op jit(solution)/shard_map/ppermute | solution.py:64
  75.3 1.6 %collective-permute-start.7 = (bf16[128,256]{1,0:T(8,128)(2,1)S(1)}, bf16[128,256]{1,0:T(8,128)(2,1)S(1)}, u32[]{:S(2)}, u32[]{:S(2)}) collective-permute-start(bf16[128,256]{1,0:T(8,128)(2,1)S(1)} %add_convert_fusion.1), channel_id=1, source_target_pairs={{0,6},{2,4},{4,2},{6,0},{1,7},{3,5},{5,3},{7,1},{8,14},{10,12},{12... | collective-permute-start | bytes 196616 | tf_op jit(solution)/shard_map/ppermute | solution.py:64
  77.2 2.0 %collective-permute-start.5 = (bf16[128,256]{1,0:T(8,128)(2,1)S(1)}, bf16[128,256]{1,0:T(8,128)(2,1)S(1)}, u32[]{:S(2)}, u32[]{:S(2)}) collective-permute-start(bf16[128,256]{1,0:T(8,128)(2,1)S(1)} %add_convert_fusion.1), channel_id=1, source_target_pairs={{0,4},{2,6},{4,0},{6,2},{1,5},{3,7},{5,1},{7,3},{8,12},{10,14},{12... | collective-permute-start | bytes 196616 | tf_op jit(solution)/shard_map/ppermute | solution.py:64
  79.2 2.6 %write_state.3 = (f32[8,1,512,256]{3,2,1,0:T(8,128)}, f32[8,1,256]{2,1,0:T(1,128)}, f32[1,8]{1,0:T(1,128)}) custom-call(f32[8,640]{1,0:T(8,128)S(1)} %get-tuple-element.19.to_write, f32[8,512]{1,0:T(8,128)S(1)} %get-tuple-element.20.value, f32[8,1,512,256]{3,2,1,0:T(8,128)} %state.5, ...), custom_call_target="tpu_custom_call", output_to_operand_aliasing={{0}: (3, {})} | custom-call | flops 1000000000 | bytes 4194304 | tf_op jit(solution)/shard_map/write_state/pallas_call | solution.py:410
  81.8 0.6 collective-permute-done.5
  82.5 0.7 add_convert_fusion
  (27 shorter events, 2.4 us)
Async XLA Ops:
  0.6 69.3 %copy-start = (bf16[1376,256]{1,0:T(8,128)(2,1)S(1)}, bf16[1376,256]{1,0:T(8,128)(2,1)}, u32[]{:S(2)}) copy-start(bf16[1376,256]{1,0:T(8,128)(2,1)} %param.31) | copy-start | bytes 2113540
  3.4 18.2 %all-to-all-start = ((bf16[16,8,1664]{2,1,0:T(8,128)(2,1)}), bf16[16,8,1664]{2,1,0:T(8,128)(2,1)S(1)}, u32[]{:S(2)}, u32[]{:S(2)}) async-start(bf16[16,8,1664]{2,1,0:T(8,128)(2,1)} %bitcast.24), calls=%async_computation | async-start | bytes 851968 | tf_op jit(solution)/shard_map/all_to_all | solution.py:60
  12.0 1.0 %copy-start.3 = (bf16[512,256]{1,0:T(8,128)(2,1)S(1)}, bf16[512,256]{1,0:T(8,128)(2,1)}, u32[]{:S(2)}) copy-start(bf16[512,256]{1,0:T(8,128)(2,1)} %weight.1) | copy-start | bytes 786436
  12.9 0.7 copy-start.5
  13.6 0.7 copy-start.7
  14.3 0.7 copy-start.8
  22.3 21.3 %copy-start.1 = (bf16[256,1376]{0,1:T(8,128)(2,1)S(1)}, bf16[256,1376]{0,1:T(8,128)(2,1)}, u32[]{:S(2)}) copy-start(bf16[256,1376]{0,1:T(8,128)(2,1)} %param.29) | copy-start | bytes 2113540
  22.3 21.3 %copy-start.2 = (bf16[256,1376]{0,1:T(8,128)(2,1)S(1)}, bf16[256,1376]{0,1:T(8,128)(2,1)}, u32[]{:S(2)}) copy-start(bf16[256,1376]{0,1:T(8,128)(2,1)} %param.30) | copy-start | bytes 2113540
  22.3 21.3 %copy-start.4 = (bf16[128,256]{1,0:T(8,128)(2,1)S(1)}, bf16[128,256]{1,0:T(8,128)(2,1)}, u32[]{:S(2)}) copy-start(bf16[128,256]{1,0:T(8,128)(2,1)} %tok.1) | copy-start | bytes 196612
  22.3 21.3 %copy-start.6 = (f32[256]{0:T(256)S(1)}, f32[256]{0:T(256)}, u32[]{:S(2)}) copy-start(f32[256]{0:T(256)} %param.28) | copy-start | bytes 3076
  32.4 3.9 %collective-permute-start = (bf16[128,256]{1,0:T(8,128)(2,1)S(1)}, bf16[128,256]{1,0:T(8,128)(2,1)S(1)}, u32[]{:S(2)}, u32[]{:S(2)}) collective-permute-start(bf16[128,256]{1,0:T(8,128)(2,1)S(1)} %convolution_convert_fusion.1), channel_id=1, source_target_pairs={{0,1},{1,0},{2,3},{3,2},{4,5},{5,4},{6,7},{7,6},{8,9},{9,8},{10,11... | collective-permute-start | bytes 196616 | tf_op jit(solution)/shard_map/ppermute | solution.py:64
  36.4 5.9 %collective-permute-start.3 = (bf16[128,256]{1,0:T(8,128)(2,1)S(1)}, bf16[128,256]{1,0:T(8,128)(2,1)S(1)}, u32[]{:S(2)}, u32[]{:S(2)}) collective-permute-start(bf16[128,256]{1,0:T(8,128)(2,1)S(1)} %add_convert_fusion.2.term_0), channel_id=1, source_target_pairs={{0,6},{2,4},{4,2},{6,0},{1,7},{3,5},{5,3},{7,1},{8,14},{10,12},{12... | collective-permute-start | bytes 196616 | tf_op jit(solution)/shard_map/ppermute | solution.py:64
  39.0 4.6 %collective-permute-start.2 = (bf16[128,256]{1,0:T(8,128)(2,1)S(1)}, bf16[128,256]{1,0:T(8,128)(2,1)S(1)}, u32[]{:S(2)}, u32[]{:S(2)}) collective-permute-start(bf16[128,256]{1,0:T(8,128)(2,1)S(1)} %add_convert_fusion.2.term_0), channel_id=1, source_target_pairs={{0,4},{2,6},{4,0},{6,2},{1,5},{3,7},{5,1},{7,3},{8,12},{10,14},{12... | collective-permute-start | bytes 196616 | tf_op jit(solution)/shard_map/ppermute | solution.py:64
  39.5 4.1 %collective-permute-start.1 = (bf16[128,256]{1,0:T(8,128)(2,1)S(1)}, bf16[128,256]{1,0:T(8,128)(2,1)S(1)}, u32[]{:S(2)}, u32[]{:S(2)}) collective-permute-start(bf16[128,256]{1,0:T(8,128)(2,1)S(1)} %add_convert_fusion.2.term_0), channel_id=1, source_target_pairs={{0,2},{2,0},{4,6},{6,4},{1,3},{3,1},{5,7},{7,5},{8,10},{10,8},{12,... | collective-permute-start | bytes 196616 | tf_op jit(solution)/shard_map/ppermute | solution.py:64
  70.3 5.0 %collective-permute-start.4 = (bf16[128,256]{1,0:T(8,128)(2,1)S(1)}, bf16[128,256]{1,0:T(8,128)(2,1)S(1)}, u32[]{:S(2)}, u32[]{:S(2)}) collective-permute-start(bf16[128,256]{1,0:T(8,128)(2,1)S(1)} %convolution_convert_fusion), channel_id=1, source_target_pairs={{0,1},{1,0},{2,3},{3,2},{4,5},{5,4},{6,7},{7,6},{8,9},{9,8},{10,11... | collective-permute-start | bytes 196616 | tf_op jit(solution)/shard_map/ppermute | solution.py:64
  75.3 6.5 %collective-permute-start.7 = (bf16[128,256]{1,0:T(8,128)(2,1)S(1)}, bf16[128,256]{1,0:T(8,128)(2,1)S(1)}, u32[]{:S(2)}, u32[]{:S(2)}) collective-permute-start(bf16[128,256]{1,0:T(8,128)(2,1)S(1)} %add_convert_fusion.1), channel_id=1, source_target_pairs={{0,6},{2,4},{4,2},{6,0},{1,7},{3,5},{5,3},{7,1},{8,14},{10,12},{12... | collective-permute-start | bytes 196616 | tf_op jit(solution)/shard_map/ppermute | solution.py:64
  76.9 4.9 %collective-permute-start.6 = (bf16[128,256]{1,0:T(8,128)(2,1)S(1)}, bf16[128,256]{1,0:T(8,128)(2,1)S(1)}, u32[]{:S(2)}, u32[]{:S(2)}) collective-permute-start(bf16[128,256]{1,0:T(8,128)(2,1)S(1)} %add_convert_fusion.1), channel_id=1, source_target_pairs={{0,2},{2,0},{4,6},{6,4},{1,3},{3,1},{5,7},{7,5},{8,10},{10,8},{12,... | collective-permute-start | bytes 196616 | tf_op jit(solution)/shard_map/ppermute | solution.py:64
  77.2 5.2 %collective-permute-start.5 = (bf16[128,256]{1,0:T(8,128)(2,1)S(1)}, bf16[128,256]{1,0:T(8,128)(2,1)S(1)}, u32[]{:S(2)}, u32[]{:S(2)}) collective-permute-start(bf16[128,256]{1,0:T(8,128)(2,1)S(1)} %add_convert_fusion.1), channel_id=1, source_target_pairs={{0,4},{2,6},{4,0},{6,2},{1,5},{3,7},{5,1},{7,3},{8,12},{10,14},{12... | collective-permute-start | bytes 196616 | tf_op jit(solution)/shard_map/ppermute | solution.py:64
